TPU v7x, 512 devices: a whole 4x8x8 slice. The times are simulated.
512 devices in a mesh: sp: 128 (over z, y, core), tp: 4 (over x).
Axes of the slice: x: 4, y: 8, z: 8, core: 2. Of those that a mesh axis runs over, the one named last changes fastest.
Arguments:
- tokens: bfloat16 [65536, 2048], P(('sp', 'tp')), may hold values from -6 to 6
- pooling_input_weight: bfloat16 [2048, 1024], P('sp', 'tp'), may hold values from -0.125 to 0.125
- query_matrix: bfloat16 [2048, 512], P('sp', 'tp'), may hold values from -0.125 to 0.125
- key_matrix: bfloat16 [2048, 512], P('sp', 'tp'), may hold values from -0.125 to 0.125
- value_matrix: bfloat16 [2048, 1024], P('sp', 'tp'), may hold values from -0.125 to 0.125
- decay_inner_weight: bfloat16 [2048, 64], replicated, may hold values from -0.125 to 0.125
- decay_outer_weight: bfloat16 [2, 32, 512], replicated, may hold values from -1 to 1
- channel_decay_bias: float32 [2, 512], replicated, may hold values from -0.3 to 12
- spike_log_decay: float32 [8, 65536], P('tp', 'sp'), may hold values from -0.72 to 0
- starting_state: float32 [2, 8, 64, 128], P(None, 'tp'), may hold values from -1536 to 1536
- pooling_group_map: bfloat16 [4, 256, 256], replicated, may hold values from -0.375 to 0.375
- pooling_output_weight: bfloat16 [1024, 2048], P('tp', 'sp'), may hold values from -0.125 to 0.125
- attention_output_weight: bfloat16 [1024, 2048], P('tp', 'sp'), may hold values from -0.125 to 0.125
Outputs:
- mixed: bfloat16 [65536, 2048], P(('sp', 'tp'))
All inputs are finite; a program needn't handle non-finite values.
Results may differ from a plain program's by a relative error of at most 0.015.
Values may be sent and summed in bfloat16 or wider, within the bound.
No kernel may reach another device: no remote copies, remote signals or barrier semaphores. Data moves between devices by JAX's collectives and lax.ppermute only.
A program may use at most 64 MiB of HBM per device.

v0:
```python
import jax
import jax.numpy as jnp
from jax import lax
from jax.sharding import Mesh
from jax.sharding import PartitionSpec as P

KEY_CHANNELS = 64
DV = 128
RANK = 32
BLOCK = 64
SP = ("sp_0", "sp_1", "sp_2")
SP_TP = ("sp_0", "sp_1", "sp_2", "tp")


eps_value = 1e-06
gate_norm_factor = 16.0
rim_width = 8


def from_everyone(value, axis):
    copies = jnp.broadcast_to(value, (lax.axis_size(axis), *value.shape))
    return lax.all_to_all(copies, axis, split_axis=0, concat_axis=0, tiled=True)


def laid_out(tiles, dim):
    tiles = jnp.moveaxis(tiles, 0, dim)
    lengths = tiles.shape
    return tiles.reshape(*lengths[:dim], lengths[dim] * lengths[dim + 1], *lengths[dim + 2 :])


def gathered_copies(value, axis, dim):
    tiles = from_everyone(value, axis)
    return laid_out(tiles, dim)


def extended(value, sides, width):
    for axis, dim in sides:
        devices, length = (lax.axis_size(axis), value.shape[dim])
        up = [(i, (i + 1) % devices) for i in range(devices - 1)]
        down = [(j, i) for i, j in up]
        last = lax.slice_in_dim(value, length - width, length, axis=dim)
        leading = lax.slice_in_dim(value, 0, width, axis=dim)
        before = lax.ppermute(last, axis, up)
        after = lax.ppermute(leading, axis, down)
        value = jnp.concatenate([before, value, after], axis=dim)
    return value


def neutral_like(value, identity):
    return jax.tree.map(
        lambda a, e: jnp.broadcast_to(jnp.asarray(e, a.dtype), a.shape), value, identity
    )


def carried_in(value, axes, combine, identity):
    before = start = neutral_like(value, identity)
    total = value
    for axis in reversed(axes):
        devices, mine = (lax.axis_size(axis), lax.axis_index(axis))
        pieces = jax.tree.map(
            lambda part, kind: lax.all_gather(part.astype(kind), axis),
            total,
            jax.tree.map(lambda a: jnp.bfloat16 if a.dtype == jnp.float32 else a.dtype, value),
        )
        inside, total = (start, start)
        for k in range(devices):
            passed = k < mine
            total = combine(
                total, jax.tree.map(lambda part, own: part[k].astype(own.dtype), pieces, value)
            )
            inside = jax.tree.map(lambda new, old: jnp.where(passed, new, old), total, inside)
        before = combine(inside, before)
    return before


def gathered_once(value, axis):
    leaves = jax.tree.leaves(value)
    order = sorted(range(len(leaves)), key=lambda k: -leaves[k].size)
    width = (1, *leaves[order[0]].shape)[-1]
    lines = [
        jnp.pad(leaves[k].reshape(-1), (0, -leaves[k].size % width)).reshape(-1, width)
        for k in order
    ]
    both, at, found = (lax.all_gather(jnp.concatenate(lines), axis), 0, {})
    for k, line in zip(order, lines):
        section = both[:, at : at + len(line)].reshape(len(both), -1)
        found[k] = section[:, : leaves[k].size].reshape(-1, *leaves[k].shape)
        at += len(line)
    numbers = iter(range(len(leaves)))
    return jax.tree.map(lambda _: found[next(numbers)], value)


def carried_in_2(value, axes, combine, identity):
    before = start = neutral_like(value, identity)
    total = value
    for axis in reversed(axes):
        devices, mine = (lax.axis_size(axis), lax.axis_index(axis))
        pieces = gathered_once(
            jax.tree.map(
                lambda part, kind: part.astype(kind),
                total,
                jax.tree.map(lambda a: jnp.bfloat16 if a.dtype == jnp.float32 else a.dtype, value),
            ),
            axis,
        )
        inside, total = (start, start)
        for k in reversed(range(devices)):
            passed = k > mine
            total = combine(
                total, jax.tree.map(lambda part, own: part[k].astype(own.dtype), pieces, value)
            )
            inside = jax.tree.map(lambda new, old: jnp.where(passed, new, old), total, inside)
        before = combine(inside, before)
    return before


def gather_turned(arrays, axis, dims):
    turned = [jnp.moveaxis(a, dim, 0) for a, dim in zip(arrays, dims)]
    both = jnp.concatenate([t.reshape(len(t), -1) for t in turned], axis=1)
    filled, at, finished = (lax.all_gather(both, axis, axis=0, tiled=True), 0, [])
    for t, dim in zip(turned, dims):
        section = filled[:, at : at + t[0].size].reshape(-1, *t.shape[1:])
        finished.append(jnp.moveaxis(section, 0, dim))
        at += t[0].size
    return tuple(finished)


def cut_along(value, dim, devices):
    lengths = value.shape
    tiles = value.reshape(*lengths[:dim], devices, lengths[dim] // devices, *lengths[dim + 1 :])
    return jnp.moveaxis(tiles, dim, 0)


def sum_at_owner(value, axis, dim):
    devices = lax.axis_size(axis)
    tiles = lax.all_to_all(cut_along(value, dim, devices), axis, 0, 0, tiled=True)
    return jnp.sum(tiles.astype(jnp.float32), axis=0)


def normalize(token_rows):
    floats = token_rows.astype(jnp.float32)
    scaled = floats * lax.rsqrt(jnp.mean(floats * floats, axis=-1, keepdims=True) + eps_value)
    return scaled.astype(jnp.bfloat16)


def chain_combine(earlier, later):
    return (earlier[0] + later[0], jnp.exp(later[0])[..., None] * earlier[1] + later[1])


def local_chain(decays, updates, backward):

    def advance(carried, element):
        log_total, memory = carried
        decay_now, update_now = element
        return (
            (log_total + decay_now, jnp.exp(decay_now)[..., None] * memory + update_now),
            (log_total, memory),
        )

    begin = (jnp.zeros_like(decays[0]), jnp.zeros_like(updates[0]))
    return lax.scan(advance, begin, (decays, updates), reverse=backward)


def within_blocks(queries, cumulative, key_rows, value_rows, lower):
    row_ids = lax.broadcasted_iota(jnp.int32, (BLOCK, BLOCK), 0)
    col_ids = lax.broadcasted_iota(jnp.int32, (BLOCK, BLOCK), 1)
    allowed = col_ids <= row_ids if lower else col_ids > row_ids
    scaled_q = queries * jnp.exp(cumulative)
    scaled_k = key_rows * jnp.exp(-cumulative)
    scores = jnp.einsum("hnid,hnjd->hnij", scaled_q, scaled_k)
    scores = jnp.where(allowed, scores, 0.0)
    return (scaled_q, jnp.einsum("hnij,hnjv->hniv", scores, value_rows))


def block_updates(key_rows, value_rows, cumulative, edge):
    weighted = key_rows * jnp.exp(edge[:, :, None, :] - cumulative)
    return jnp.einsum("hncd,hncv->hndv", weighted, value_rows)


def carried_term(scaled_q, before, entering):
    log_before, memory_before = before
    block_memory = jnp.exp(log_before)[..., None] * entering[None] + memory_before
    return jnp.einsum("hnid,nhdv->hniv", scaled_q, block_memory)


def shards(
    tokens,
    pooling_input_weight,
    query_matrix,
    key_matrix,
    value_matrix,
    decay_inner_weight,
    decay_outer_weight,
    channel_decay_bias,
    spike_log_decay,
    starting_state,
    pooling_group_map,
    pooling_output_weight,
    attention_output_weight,
):
    sp_index = lax.axis_index(SP)
    tp_index = lax.axis_index("tp")
    normed = normalize(tokens)
    pool_cols = pooling_input_weight.shape[1]
    qk_cols = query_matrix.shape[1]
    value_cols = value_matrix.shape[1]
    local_weight = jnp.concatenate(
        [pooling_input_weight, query_matrix, key_matrix, value_matrix], axis=1
    )
    all_rows = gathered_copies(normed, "tp", 0)
    summed = jnp.dot(
        all_rows,
        lax.all_gather(local_weight, SP, axis=0, tiled=True),
        preferred_element_type=jnp.float32,
    )
    rank_part = jnp.dot(all_rows, decay_inner_weight, preferred_element_type=jnp.float32).astype(
        jnp.bfloat16
    )
    projected = jnp.concatenate([summed.astype(jnp.bfloat16), rank_part], axis=1)
    sequence_length = projected.shape[0]
    blocks = sequence_length // BLOCK
    heads_here = qk_cols // KEY_CHANNELS
    pool_input = projected[:, :pool_cols]
    query_part = projected[:, pool_cols : pool_cols + qk_cols]
    key_part = projected[:, pool_cols + qk_cols : pool_cols + 2 * qk_cols]
    value_part = projected[:, pool_cols + 2 * qk_cols : pool_cols + 2 * qk_cols + value_cols]
    low_rank = projected[:, pool_cols + 2 * qk_cols + value_cols :]
    window = jnp.left_shift(jnp.int32(2), tp_index)
    half_width = window // 2
    padded = extended(pool_input, ((SP, 0),), rim_width)
    floats = padded.astype(jnp.float32)
    window_sum = jnp.zeros((sequence_length, pool_cols), jnp.float32)
    for offset in range(-rim_width, rim_width):
        inside = ((offset >= -half_width) & (offset < window - half_width)).astype(jnp.float32)
        window_sum = (
            window_sum + inside * floats[rim_width + offset : rim_width + offset + sequence_length]
        )
    seq_length = sequence_length * lax.axis_size(SP)
    position = sp_index * sequence_length + jnp.arange(sequence_length, dtype=jnp.int32)
    low_end = jnp.clip(position - half_width, 0, seq_length - 1)
    high_end = jnp.clip(position - half_width + window - 1, 0, seq_length - 1)
    counted = (high_end - low_end + 1).astype(jnp.float32)[:, None]
    pooled = (window_sum / counted - floats[rim_width : rim_width + sequence_length]).astype(
        jnp.bfloat16
    )
    mix_here = lax.dynamic_index_in_dim(pooling_group_map, tp_index, 0, keepdims=False)
    pool_output = jnp.dot(pooled, mix_here, preferred_element_type=jnp.float32).astype(jnp.bfloat16)

    def split_heads(token_level, width):
        return (
            token_level.astype(jnp.float32)
            .reshape(blocks, BLOCK, heads_here, width)
            .transpose(2, 0, 1, 3)
        )

    queries = split_heads(query_part, KEY_CHANNELS) * KEY_CHANNELS ** (-0.5)
    key_rows = split_heads(key_part, KEY_CHANNELS)
    value_rows = split_heads(value_part, DV)
    up_here = lax.dynamic_slice_in_dim(decay_outer_weight, tp_index * qk_cols, qk_cols, 2)
    bias_here = lax.dynamic_slice_in_dim(channel_decay_bias, tp_index * qk_cols, qk_cols, 1)
    spike_amounts = spike_log_decay.T[:, :, None]

    def log_decay(direction):
        preactivation = (
            jnp.dot(
                low_rank[:, direction * RANK : (direction + 1) * RANK],
                up_here[direction],
                preferred_element_type=jnp.float32,
            )
            + bias_here[direction]
        )
        token_level = (jax.nn.log_sigmoid(preactivation) / gate_norm_factor).reshape(
            sequence_length, heads_here, KEY_CHANNELS
        ) + spike_amounts
        return token_level.reshape(blocks, BLOCK, heads_here, KEY_CHANNELS).transpose(2, 0, 1, 3)

    cum_fwd = jnp.cumsum(log_decay(0), axis=2)
    cum_bwd = jnp.flip(jnp.cumsum(jnp.flip(log_decay(1), 2), axis=2), 2)
    scaled_fwd, inner_fwd = within_blocks(queries, cum_fwd, key_rows, value_rows, True)
    scaled_bwd, inner_bwd = within_blocks(queries, cum_bwd, key_rows, value_rows, False)
    edge_fwd = cum_fwd[:, :, -1, :]
    edge_bwd = cum_bwd[:, :, 0, :]
    updates_fwd = block_updates(key_rows, value_rows, cum_fwd, edge_fwd)
    updates_bwd = block_updates(key_rows, value_rows, cum_bwd, edge_bwd)
    total_fwd, before_fwd = local_chain(
        jnp.moveaxis(edge_fwd, 1, 0), jnp.moveaxis(updates_fwd, 1, 0), False
    )
    total_bwd, before_bwd = local_chain(
        jnp.moveaxis(edge_bwd, 1, 0), jnp.moveaxis(updates_bwd, 1, 0), True
    )
    neutral = (jnp.zeros_like(total_fwd[0]), jnp.zeros_like(total_fwd[1]))
    prefix_fwd = carried_in(total_fwd, SP, chain_combine, neutral)
    prefix_bwd = carried_in_2(total_bwd, SP, chain_combine, neutral)
    entering_fwd = jnp.exp(prefix_fwd[0])[..., None] * starting_state[0] + prefix_fwd[1]
    entering_bwd = jnp.exp(prefix_bwd[0])[..., None] * starting_state[1] + prefix_bwd[1]
    out_fwd = inner_fwd + carried_term(scaled_fwd, before_fwd, entering_fwd)
    out_bwd = inner_bwd + carried_term(scaled_bwd, before_bwd, entering_bwd)
    joined = out_fwd + out_bwd
    normal_scale = lax.rsqrt(jnp.mean(joined * joined, axis=-1, keepdims=True) + eps_value)
    attention_output = (
        (joined * normal_scale)
        .astype(jnp.bfloat16)
        .transpose(1, 2, 0, 3)
        .reshape(sequence_length, heads_here * DV)
    )
    whole_pool, whole_attention = gather_turned(
        (pooling_output_weight, attention_output_weight), SP, (1, 1)
    )
    part_one = jnp.dot(pool_output, whole_pool, preferred_element_type=jnp.float32)
    part_two = jnp.dot(attention_output, whole_attention, preferred_element_type=jnp.float32)
    mixed = sum_at_owner((part_one + part_two).astype(jnp.bfloat16), "tp", 0)
    return mixed.astype(jnp.bfloat16)


def solution(mesh):
    split = Mesh(mesh.devices.reshape(8, 8, 2, mesh.shape["tp"]), ("sp_0", "sp_1", "sp_2", "tp"))
    in_specs = (
        P(SP_TP, None),
        P(SP, "tp"),
        P(SP, "tp"),
        P(SP, "tp"),
        P(SP, "tp"),
        P(),
        P(),
        P(),
        P("tp", SP),
        P(None, "tp", None, None),
        P(),
        P("tp", SP),
        P("tp", SP),
    )
    out_specs = P(SP_TP, None)
    return jax.shard_map(
        shards, mesh=split, in_specs=in_specs, out_specs=out_specs, check_vma=False
    )
```

profile of v0, /device:TPU:2, one launch (start us, length us, event | category | flops | bytes accessed | tf_op | source)
XLA Modules:
  0.0 326.1 jit_solution(17219555616986555512)
XLA Ops:
  12.0 9.6 %all-to-all-start = ((bf16[4,128,2048]{2,1,0:T(8,128)(2,1)}), bf16[4,128,2048]{2,1,0:T(8,128)(2,1)S(1)}, u32[]{:S(2)}, u32[]{:S(2)}) async-start(bf16[4,128,2048]{2,1,0:T(8,128)(2,1)} %broadcast_in_dim.42), calls=%async_computation | async-start | bytes 4194304 | tf_op jit(solution)/shard_map/all_to_all | solution.py:22
  24.8 17.1 %all-to-all-done = bf16[4,128,2048]{2,1,0:T(8,128)(2,1)S(1)} async-done(((bf16[4,128,2048]{2,1,0:T(8,128)(2,1)}), bf16[4,128,2048]{2,1,0:T(8,128)(2,1)S(1)}, u32[]{:S(2)}, u32[]{:S(2)}) %all-to-all-start) | async-done | bytes 2097184 | tf_op jit(solution)/shard_map/all_to_all | solution.py:22
  46.8 1.9 rev.7
  51.6 2.1 reshape.1391
  56.3 42.6 %all-gather.12.cloned.1.call-done = bf16[2048,768]{1,0:T(8,128)(2,1)} async-done(((bf16[16,768]{1,0:T(8,128)(2,1)}), bf16[2048,768]{1,0:T(8,128)(2,1)}) %all-gather.12.cloned.1.call-update) | async-done | bytes 3145744 | tf_op jit(solution)/shard_map/all_gather | solution.py:213
  98.9 3.7 %convolution_convert_fusion = bf16[512,768]{1,0:T(8,128)(2,1)S(1)} fusion(bf16[512,2048]{1,0:T(8,128)(2,1)S(1)} %bitcast.287, bf16[2048,768]{1,0:T(8,128)(2,1)} %all-gather.12.cloned.1.call-done), kind=kOutput, calls=%fused_computation.13 | convolution fusion | flops 1611005952 | bytes 6029312 | tf_op jit(solution)/shard_map/dot_general | solution.py:211
  105.5 2.8 bitcast_multiply_fusion.1
  108.6 7.0 %while.39 = (s32[]{:T(128)}, f32[2,64]{1,0:T(2,128)S(1)}, f32[2,64,128]{2,1,0:T(8,128)S(1)}, f32[8,2,64]{2,1,0:T(2,128)S(1)}, f32[8,2,64,128]{3,2,1,0:T(8,128)S(...) while((s32[]{:T(128)}, f32[2,64]{1,0:T(2,128)S(1)}, ...), condition=%wide.region_6.7_spmd.clone, body=%wide.region_5.6_spmd.clone.sunk | while | flops 65924 | bytes 333454 | solution.py:161
  115.7 1.8 all-gather.6
  117.7 24.9 %all-gather.7 = bf16[8,129,128]{2,1,0:T(8,128)(2,1)S(1)} all-gather(bf16[1,129,128]{2,1,0:T(8,128)(2,1)S(1)} %maximum_bitcast_fusion.1), channel_id=5, replica_groups=mesh['sp_0'=8,'sp_1'=8,'sp_2'=2,'tp'=4] {'sp_1'}, dimensions={0}, use_global_device_ids=true | all-gather | bytes 297216 | tf_op jit(solution)/shard_map/all_gather | solution.py:84
  142.9 25.0 %all-gather.8 = bf16[8,129,128]{2,1,0:T(8,128)(2,1)S(1)} all-gather(bf16[1,129,128]{2,1,0:T(8,128)(2,1)S(1)} %maximum_bitcast_fusion.2), channel_id=6, replica_groups=mesh['sp_0'=8,'sp_1'=8,'sp_2'=2,'tp'=4] {'sp_0'}, dimensions={0}, use_global_device_ids=true | all-gather | bytes 297216 | tf_op jit(solution)/shard_map/all_gather | solution.py:84
  181.8 7.0 %while.38 = (s32[]{:T(128)}, f32[2,64]{1,0:T(2,128)S(1)}, f32[2,64,128]{2,1,0:T(8,128)S(1)}, f32[8,2,64]{2,1,0:T(2,128)S(1)}, f32[8,2,64,128]{3,2,1,0:T(8,128)S(...) while((s32[]{:T(128)}, f32[2,64]{1,0:T(2,128)S(1)}, ...), condition=%wide.region_3.4_spmd.clone, body=%wide.region_2.3_spmd.clone.sunk | while | flops 65923 | bytes 333434 | solution.py:161
  189.0 1.8 all-gather.5
  190.8 15.0 %all_gather.56 = bf16[8,2,64]{2,1,0:T(2,128)(2,1)S(1)} all-gather(bf16[1,2,64]{2,1,0:T(2,128)(2,1)S(1)} %get-tuple-element.410), channel_id=1, replica_groups=mesh['sp_0'=8,'sp_1'=8,'sp_2'=2,'tp'=4] {'sp_1'}, dimensions={0}, use_global_device_ids=true | all-gather | bytes 2304 | tf_op jit(solution)/shard_map/all_gather | solution.py:61
  205.9 14.8 %all_gather.57 = bf16[8,2,64]{2,1,0:T(2,128)(2,1)S(1)} all-gather(bf16[1,2,64]{2,1,0:T(2,128)(2,1)S(1)} %get-tuple-element.398), channel_id=1, replica_groups=mesh['sp_0'=8,'sp_1'=8,'sp_2'=2,'tp'=4] {'sp_0'}, dimensions={0}, use_global_device_ids=true | all-gather | bytes 2304 | tf_op jit(solution)/shard_map/all_gather | solution.py:61
  220.7 1.8 all-gather.1
  222.5 2.1 collective-permute-start
  226.0 28.0 %all_gather.60 = bf16[8,2,64,128]{3,2,1,0:T(8,128)(2,1)S(1)} all-gather(bf16[1,2,64,128]{3,2,1,0:T(8,128)(2,1)S(1)} %fusion.138), channel_id=1, replica_groups=mesh['sp_0'=8,'sp_1'=8,'sp_2'=2,'tp'=4] {'sp_1'}, dimensions={0}, use_global_device_ids=true | all-gather | bytes 294912 | tf_op jit(solution)/shard_map/all_gather | solution.py:61
  254.2 26.6 %all_gather.61 = bf16[8,2,64,128]{3,2,1,0:T(8,128)(2,1)S(1)} all-gather(bf16[1,2,64,128]{3,2,1,0:T(8,128)(2,1)S(1)} %fusion.137), channel_id=1, replica_groups=mesh['sp_0'=8,'sp_1'=8,'sp_2'=2,'tp'=4] {'sp_0'}, dimensions={0}, use_global_device_ids=true | all-gather | bytes 294912 | tf_op jit(solution)/shard_map/all_gather | solution.py:61
  281.7 1.9 fusion.126
  285.7 2.1 fusion.3
  290.3 5.1 %fusion.5 = f32[512,2048]{1,0:T(8,128)} fusion(bf16[2048,512]{1,0:T(8,128)(2,1)} %all-gather.14.cloned.1.call-done, f32[528,256]{1,0:T(8,128)S(1)} %maximum_convert_fusion, f32[512]{0:T(512)S(1)} %copy-done.15, f32[]{:T(128)S(6)} %convert_element_type.1186, f32[]{:T(128)S(6)} %convert_element_type.1185, f32[]{:T(128)S(6)} %convert_element_type.1184, ...), kind=kOutput, calls=%fused_computation.26 | convolution fusion | flops 608567296 | bytes 13764676 | tf_op jit(solution)/shard_map/dot_general | solution.py:309
  295.4 2.9 add_convert_fusion
  298.3 19.7 %all_to_all.10 = bf16[4,128,2048]{2,1,0:T(8,128)(2,1)S(1)} all-to-all(bf16[4,128,2048]{2,1,0:T(8,128)(2,1)S(1)} %bitcast.288), channel_id=1, replica_groups=mesh['sp_0'=8,'sp_1'=8,'sp_2'=2,'tp'=4] {'tp'}, dimensions={0} | all-to-all | bytes 4194304 | tf_op jit(solution)/shard_map/all_to_all | solution.py:136
  (258 shorter events, 57.8 us)
Async XLA Ops:
  6.5 283.8 %copy-start = (bf16[4,256,256]{2,1,0:T(8,128)(2,1)S(1)}, bf16[4,256,256]{2,1,0:T(8,128)(2,1)}, u32[]{:S(2)}) copy-start(bf16[4,256,256]{2,1,0:T(8,128)(2,1)} %param.27) | copy-start | bytes 1572868
  6.5 92.3 %all-gather.12.cloned.1.call-start = ((), (), s32[]{:S(2)}) async-start(), calls=%async_computation.2 | async-start | bytes 3170304 | tf_op jit(solution)/shard_map/all_gather | solution.py:213
  12.0 29.8 %all-to-all-start = ((bf16[4,128,2048]{2,1,0:T(8,128)(2,1)}), bf16[4,128,2048]{2,1,0:T(8,128)(2,1)S(1)}, u32[]{:S(2)}, u32[]{:S(2)}) async-start(bf16[4,128,2048]{2,1,0:T(8,128)(2,1)} %broadcast_in_dim.42), calls=%async_computation | async-start | bytes 4194304 | tf_op jit(solution)/shard_map/all_to_all | solution.py:22
  21.6 268.7 %all-gather.14.cloned.1.call-start = ((), (), s32[]{:S(2)}) async-start(), calls=%async_computation.3 | async-start | bytes 2113536 | tf_op jit(solution)/shard_map/all_gather | solution.py:120
  188.8 94.9 %copy-start.8 = (f32[2,2,64,128]{3,2,1,0:T(8,128)S(1)}, f32[2,2,64,128]{3,2,1,0:T(8,128)}, u32[]{:S(2)}) copy-start(f32[2,2,64,128]{3,2,1,0:T(8,128)} %param.26) | copy-start | bytes 393220
  188.8 94.9 %copy-start.16 = (f32[2,64]{1,0:T(2,128)S(1)}, f32[2,64]{1,0:T(2,128)}, u32[]{:S(2)}) copy-start(f32[2,64]{1,0:T(2,128)} %reshape.1519) | copy-start | bytes 1540
  188.8 94.9 %copy-start.17 = (f32[2,64]{1,0:T(2,128)S(1)}, f32[2,64]{1,0:T(2,128)}, u32[]{:S(2)}) copy-start(f32[2,64]{1,0:T(2,128)} %reshape.1557) | copy-start | bytes 1540
  188.8 94.9 %copy-start.18 = (f32[2,64]{1,0:T(2,128)S(1)}, f32[2,64]{1,0:T(2,128)}, u32[]{:S(2)}) copy-start(f32[2,64]{1,0:T(2,128)} %reshape.1568) | copy-start | bytes 1540
  188.8 94.9 %copy-start.19 = (f32[2,64]{1,0:T(2,128)S(1)}, f32[2,64]{1,0:T(2,128)}, u32[]{:S(2)}) copy-start(f32[2,64]{1,0:T(2,128)} %exp.501) | copy-start | bytes 1540
  188.8 94.9 %copy-start.20 = (f32[2,64]{1,0:T(2,128)S(1)}, f32[2,64]{1,0:T(2,128)}, u32[]{:S(2)}) copy-start(f32[2,64]{1,0:T(2,128)} %exp.503) | copy-start | bytes 1540
  188.9 94.9 %copy-start.21 = (f32[2,64]{1,0:T(2,128)S(1)}, f32[2,64]{1,0:T(2,128)}, u32[]{:S(2)}) copy-start(f32[2,64]{1,0:T(2,128)} %exp.505) | copy-start | bytes 1540
  188.9 94.9 %copy-start.22 = (f32[2,64]{1,0:T(2,128)S(1)}, f32[2,64]{1,0:T(2,128)}, u32[]{:S(2)}) copy-start(f32[2,64]{1,0:T(2,128)} %mul.911) | copy-start | bytes 1540
  188.9 94.9 %copy-start.23 = (f32[2,64]{1,0:T(2,128)S(1)}, f32[2,64]{1,0:T(2,128)}, u32[]{:S(2)}) copy-start(f32[2,64]{1,0:T(2,128)} %reshape.1462) | copy-start | bytes 1540
  188.9 94.9 %copy-start.24 = (f32[2,64]{1,0:T(2,128)S(1)}, f32[2,64]{1,0:T(2,128)}, u32[]{:S(2)}) copy-start(f32[2,64]{1,0:T(2,128)} %reshape.1480) | copy-start | bytes 1540
  188.9 94.9 %copy-start.25 = (f32[2,64]{1,0:T(2,128)S(1)}, f32[2,64]{1,0:T(2,128)}, u32[]{:S(2)}) copy-start(f32[2,64]{1,0:T(2,128)} %reshape.1497) | copy-start | bytes 1540
  188.9 94.9 %copy-start.26 = (f32[2,64]{1,0:T(2,128)S(1)}, f32[2,64]{1,0:T(2,128)}, u32[]{:S(2)}) copy-start(f32[2,64]{1,0:T(2,128)} %exp.512) | copy-start | bytes 1540
  188.9 94.9 %copy-start.27 = (f32[2,64]{1,0:T(2,128)S(1)}, f32[2,64]{1,0:T(2,128)}, u32[]{:S(2)}) copy-start(f32[2,64]{1,0:T(2,128)} %exp.513) | copy-start | bytes 1540
  188.9 94.9 %copy-start.28 = (f32[2,64]{1,0:T(2,128)S(1)}, f32[2,64]{1,0:T(2,128)}, u32[]{:S(2)}) copy-start(f32[2,64]{1,0:T(2,128)} %exp.514) | copy-start | bytes 1540
  188.9 94.9 %copy-start.29 = (f32[2,64]{1,0:T(2,128)S(1)}, f32[2,64]{1,0:T(2,128)}, u32[]{:S(2)}) copy-start(f32[2,64]{1,0:T(2,128)} %mul.929) | copy-start | bytes 1540
  188.9 94.9 %copy-start.30 = (f32[2,64]{1,0:T(2,128)S(1)}, f32[2,64]{1,0:T(2,128)}, u32[]{:S(2)}) copy-start(f32[2,64]{1,0:T(2,128)} %reshape.1463) | copy-start | bytes 1540
  189.0 94.9 %copy-start.31 = (f32[2,64]{1,0:T(2,128)S(1)}, f32[2,64]{1,0:T(2,128)}, u32[]{:S(2)}) copy-start(f32[2,64]{1,0:T(2,128)} %reshape.1481) | copy-start | bytes 1540
  189.0 94.9 %copy-start.32 = (f32[2,64]{1,0:T(2,128)S(1)}, f32[2,64]{1,0:T(2,128)}, u32[]{:S(2)}) copy-start(f32[2,64]{1,0:T(2,128)} %reshape.1498) | copy-start | bytes 1540
  222.5 67.7 %collective-permute-start = (bf16[8,256]{1,0:T(8,128)(2,1)}, bf16[8,256]{1,0:T(8,128)(2,1)S(1)}, u32[]{:S(2)}, u32[]{:S(2)}) collective-permute-start(bf16[8,256]{1,0:T(8,128)(2,1)} %get-tuple-element.350), channel_id=1, source_target_pairs={{0,4},{4,8},{8,12},{12,16},{16,20},{20,24},{24,28},{28,32},{32,36}... | collective-permute-start | bytes 12296 | tf_op jit(solution)/shard_map/ppermute | solution.py:43
  224.6 65.6 %collective-permute-start.1 = (bf16[8,256]{1,0:T(8,128)(2,1)}, bf16[8,256]{1,0:T(8,128)(2,1)S(1)}, u32[]{:S(2)}, u32[]{:S(2)}) collective-permute-start(bf16[8,256]{1,0:T(8,128)(2,1)} %get-tuple-element.351), channel_id=1, source_target_pairs={{4,0},{8,4},{12,8},{16,12},{20,16},{24,20},{28,24},{32,28},{36,32}... | collective-permute-start | bytes 12296 | tf_op jit(solution)/shard_map/ppermute | solution.py:44
  (18 other events, 554.5 us)
Sparse Core Ops, SparseCore 0:
  10.5 88.3 all-gather.11
  102.0 80.1 all-gather.13
where the time goes:
time: 328 us; the launch traced here: 326 us
  blocking collectives  159 us (48%)
  waiting for transfers between devices  59.8 us (18%)
  local copies, waits for them, and re-layouts  37.4 us (11%)
  matrix products  21.7 us (7%)
  other arithmetic  19.6 us (6%)
  between operations  14.6 us (4%)
  starting transfers between devices  13 us (4%)
    all_gather x6, blocking collectives, carried_in(): lax.all_gather(part.astype(kind), axis)  88 us
    all_gather x3, blocking collectives, gathered_once(): both, at, found = (lax.all_gather(jnp.concatenate(lines), axis), 0, {})  51.7 us
    all_gather x1, waiting for transfers between devices, shards(): lax.all_gather(local_weight, SP, axis=0, tiled=True)  42.6 us
    all_to_all x1, blocking collectives, sum_at_owner(): lax.all_to_all(cut_along(value, dim, devices), axis, 0, 0, tiled=True)  19.7 us
    all_to_all x1, waiting for transfers between devices, from_everyone(): return lax.all_to_all(copies, axis, split_axis=0, concat_axis=0, tiled=True)  17.1 us
    dynamic_slice x16, local copies, waits for them, and re-layouts, local_chain(): return lax.scan(advance, begin, (decays, updates), reverse=backward)  11.3 us
    exp x19, local copies, waits for them, and re-layouts, chain_combine(): jnp.exp(later[0])[..., None] * earlier[1] + later[1]  11 us
    all_to_all x1, starting transfers between devices, from_everyone(): return lax.all_to_all(copies, axis, split_axis=0, concat_axis=0, tiled=True)  9.6 us
  transfers between devices with their start and end apart: 5, of which 2 were waited for; matrix products, arithmetic and copies ran while one was open for 21% of the time, Pallas kernels for 0%

commit v1 on v0

--- a/solution.py
+++ b/solution.py
@@ -1,6 +1,8 @@
 import jax
 import jax.numpy as jnp
 from jax import lax
+from jax.experimental import pallas as pl
+from jax.experimental.pallas import tpu as pltpu
 from jax.sharding import Mesh
 from jax.sharding import PartitionSpec as P
 
@@ -15,6 +17,7 @@
 eps_value = 1e-06
 gate_norm_factor = 16.0
 rim_width = 8
+LANES = 128
 
 
 def from_everyone(value, axis):
@@ -46,83 +49,84 @@
     return value
 
 
-def neutral_like(value, identity):
-    return jax.tree.map(
-        lambda a, e: jnp.broadcast_to(jnp.asarray(e, a.dtype), a.shape), value, identity
-    )
-
-
-def carried_in(value, axes, combine, identity):
-    before = start = neutral_like(value, identity)
-    total = value
-    for axis in reversed(axes):
-        devices, mine = (lax.axis_size(axis), lax.axis_index(axis))
-        pieces = jax.tree.map(
-            lambda part, kind: lax.all_gather(part.astype(kind), axis),
-            total,
-            jax.tree.map(lambda a: jnp.bfloat16 if a.dtype == jnp.float32 else a.dtype, value),
-        )
-        inside, total = (start, start)
-        for k in range(devices):
-            passed = k < mine
-            total = combine(
-                total, jax.tree.map(lambda part, own: part[k].astype(own.dtype), pieces, value)
-            )
-            inside = jax.tree.map(lambda new, old: jnp.where(passed, new, old), total, inside)
-        before = combine(inside, before)
-    return before
-
-
-def gathered_once(value, axis):
-    leaves = jax.tree.leaves(value)
-    order = sorted(range(len(leaves)), key=lambda k: -leaves[k].size)
-    width = (1, *leaves[order[0]].shape)[-1]
-    lines = [
-        jnp.pad(leaves[k].reshape(-1), (0, -leaves[k].size % width)).reshape(-1, width)
-        for k in order
-    ]
-    both, at, found = (lax.all_gather(jnp.concatenate(lines), axis), 0, {})
-    for k, line in zip(order, lines):
-        section = both[:, at : at + len(line)].reshape(len(both), -1)
-        found[k] = section[:, : leaves[k].size].reshape(-1, *leaves[k].shape)
-        at += len(line)
-    numbers = iter(range(len(leaves)))
-    return jax.tree.map(lambda _: found[next(numbers)], value)
-
-
-def carried_in_2(value, axes, combine, identity):
-    before = start = neutral_like(value, identity)
-    total = value
-    for axis in reversed(axes):
-        devices, mine = (lax.axis_size(axis), lax.axis_index(axis))
-        pieces = gathered_once(
-            jax.tree.map(
-                lambda part, kind: part.astype(kind),
-                total,
-                jax.tree.map(lambda a: jnp.bfloat16 if a.dtype == jnp.float32 else a.dtype, value),
-            ),
-            axis,
-        )
-        inside, total = (start, start)
-        for k in reversed(range(devices)):
-            passed = k > mine
-            total = combine(
-                total, jax.tree.map(lambda part, own: part[k].astype(own.dtype), pieces, value)
-            )
-            inside = jax.tree.map(lambda new, old: jnp.where(passed, new, old), total, inside)
-        before = combine(inside, before)
-    return before
-
-
-def gather_turned(arrays, axis, dims):
-    turned = [jnp.moveaxis(a, dim, 0) for a, dim in zip(arrays, dims)]
-    both = jnp.concatenate([t.reshape(len(t), -1) for t in turned], axis=1)
-    filled, at, finished = (lax.all_gather(both, axis, axis=0, tiled=True), 0, [])
-    for t, dim in zip(turned, dims):
-        section = filled[:, at : at + t[0].size].reshape(-1, *t.shape[1:])
-        finished.append(jnp.moveaxis(section, 0, dim))
-        at += t[0].size
-    return tuple(finished)
+def scan_kernel(place_ref, received_ref, start_ref, out_ref):
+    place = place_ref[0]
+    devices = received_ref.shape[0]
+    packed = received_ref[:, 2, :].astype(jnp.float32)
+    logs = packed + pltpu.roll(packed, LANES - 2, 1)
+    row = lax.broadcasted_iota(jnp.int32, (devices, devices), 0)
+    col = lax.broadcasted_iota(jnp.int32, (devices, devices), 1)
+    earlier = (col < row).astype(jnp.float32)
+    later = (row < col).astype(jnp.float32)
+    exact = lax.Precision.HIGHEST
+    before_col = jnp.dot(earlier, logs, precision=exact, preferred_element_type=jnp.float32)
+    dims = (((0,), (0,)), ((), ()))
+    before_row = lax.dot_general(
+        logs, later, dims, precision=exact, preferred_element_type=jnp.float32
+    )
+    own_row = lax.dot_general(
+        logs,
+        (row == col).astype(jnp.float32),
+        dims,
+        precision=exact,
+        preferred_element_type=jnp.float32,
+    )
+    total = jnp.sum(logs, axis=0, keepdims=True)
+    forward = place < devices // 2
+    for r in range(2):
+        at_col = before_col[:, r : r + 1]
+        past_col = at_col + logs[:, r : r + 1]
+        at_row = before_row[r : r + 1, :]
+        past_row = at_row + own_row[r : r + 1, :]
+        between = jnp.where(forward, at_col - past_row, at_row - past_col)
+        allowed = jnp.where(forward, row - col, col - row) > 0
+        weights = jnp.where(allowed, jnp.exp(jnp.minimum(between, 0.0)), 0.0)
+        outside = jnp.where(forward, at_col, total[:, r : r + 1] - past_col)
+        updates = received_ref[:, r, :].astype(jnp.float32)
+        first = start_ref[pl.ds(2 * place + r, 1), :]
+        entering = jnp.dot(
+            weights, updates, precision=exact, preferred_element_type=jnp.float32
+        ) + jnp.exp(jnp.minimum(outside, 0.0)) * first
+        out_ref[:, r, :] = entering.astype(out_ref.dtype)
+
+
+def entering_states(total_fwd, total_bwd, starting_state, place):
+    logs = jnp.stack([total_fwd[0], total_bwd[0]])
+    updates = jnp.stack([total_fwd[1], total_bwd[1]])
+    devices = logs.size // 2
+    high = logs.astype(jnp.bfloat16)
+    low = (logs - high.astype(jnp.float32)).astype(jnp.bfloat16)
+    edge = jnp.concatenate([high.reshape(devices, 2), low.reshape(devices, 2)], axis=1)
+    edge = jnp.pad(edge, ((0, 0), (0, LANES - 4)))
+    packed = jnp.concatenate(
+        [updates.astype(jnp.bfloat16).reshape(devices, 2, DV), edge[:, None]], axis=1
+    )
+    received = lax.all_to_all(packed, SP, 0, 0, tiled=True)
+    entering = pl.pallas_call(
+        scan_kernel,
+        in_specs=[
+            pl.BlockSpec(memory_space=pltpu.SMEM),
+            pl.BlockSpec(memory_space=pltpu.VMEM),
+            pl.BlockSpec(memory_space=pltpu.VMEM),
+        ],
+        out_specs=pl.BlockSpec(memory_space=pltpu.VMEM),
+        out_shape=jax.ShapeDtypeStruct((devices, 2, DV), jnp.bfloat16),
+        name="scan_states",
+    )(place.reshape(1).astype(jnp.int32), received, starting_state.reshape(2 * devices, DV))
+    entering = lax.all_to_all(entering, SP, 0, 0, tiled=True)
+    return entering.reshape(starting_state.shape).astype(jnp.float32)
+
+
+def spread(value, axes):
+    for axis in axes:
+        copies = jnp.broadcast_to(value, (lax.axis_size(axis), *value.shape))
+        value = lax.all_to_all(copies, axis, split_axis=0, concat_axis=0, tiled=True)
+    return value
+
+
+def in_order(tiles):
+    whole = tiles.transpose(1, 2, 0, 3, 4)
+    return whole.reshape(-1, tiles.shape[-1])
 
 
 def cut_along(value, dim, devices):
@@ -141,10 +145,6 @@
     floats = token_rows.astype(jnp.float32)
     scaled = floats * lax.rsqrt(jnp.mean(floats * floats, axis=-1, keepdims=True) + eps_value)
     return scaled.astype(jnp.bfloat16)
-
-
-def chain_combine(earlier, later):
-    return (earlier[0] + later[0], jnp.exp(later[0])[..., None] * earlier[1] + later[1])
 
 
 def local_chain(decays, updates, backward):
@@ -207,10 +207,15 @@
     local_weight = jnp.concatenate(
         [pooling_input_weight, query_matrix, key_matrix, value_matrix], axis=1
     )
+    local_out = jnp.concatenate([pooling_output_weight, attention_output_weight], axis=0).T
+    some = spread(jnp.concatenate([local_weight, local_out], axis=1), ("sp_1",))
+    in_cols = local_weight.shape[1]
+    whole_in = in_order(spread(some[..., :in_cols], ("sp_0", "sp_2")))
+    whole_out = in_order(spread(some[..., in_cols:], ("sp_0", "sp_2")))
     all_rows = gathered_copies(normed, "tp", 0)
     summed = jnp.dot(
         all_rows,
-        lax.all_gather(local_weight, SP, axis=0, tiled=True),
+        whole_in,
         preferred_element_type=jnp.float32,
     )
     rank_part = jnp.dot(all_rows, decay_inner_weight, preferred_element_type=jnp.float32).astype(
@@ -288,11 +293,8 @@
     total_bwd, before_bwd = local_chain(
         jnp.moveaxis(edge_bwd, 1, 0), jnp.moveaxis(updates_bwd, 1, 0), True
     )
-    neutral = (jnp.zeros_like(total_fwd[0]), jnp.zeros_like(total_fwd[1]))
-    prefix_fwd = carried_in(total_fwd, SP, chain_combine, neutral)
-    prefix_bwd = carried_in_2(total_bwd, SP, chain_combine, neutral)
-    entering_fwd = jnp.exp(prefix_fwd[0])[..., None] * starting_state[0] + prefix_fwd[1]
-    entering_bwd = jnp.exp(prefix_bwd[0])[..., None] * starting_state[1] + prefix_bwd[1]
+    entering = entering_states(total_fwd, total_bwd, starting_state, sp_index)
+    entering_fwd, entering_bwd = entering[0], entering[1]
     out_fwd = inner_fwd + carried_term(scaled_fwd, before_fwd, entering_fwd)
     out_bwd = inner_bwd + carried_term(scaled_bwd, before_bwd, entering_bwd)
     joined = out_fwd + out_bwd
@@ -303,12 +305,11 @@
         .transpose(1, 2, 0, 3)
         .reshape(sequence_length, heads_here * DV)
     )
-    whole_pool, whole_attention = gather_turned(
-        (pooling_output_weight, attention_output_weight), SP, (1, 1)
-    )
-    part_one = jnp.dot(pool_output, whole_pool, preferred_element_type=jnp.float32)
-    part_two = jnp.dot(attention_output, whole_attention, preferred_element_type=jnp.float32)
-    mixed = sum_at_owner((part_one + part_two).astype(jnp.bfloat16), "tp", 0)
+    activations = jnp.concatenate([pool_output, attention_output], axis=1)
+    partial = lax.dot_general(
+        activations, whole_out, (((1,), (1,)), ((), ())), preferred_element_type=jnp.float32
+    )
+    mixed = sum_at_owner(partial.astype(jnp.bfloat16), "tp", 0)
     return mixed.astype(jnp.bfloat16)
 
 

time: 328 us -> 262 us (0.80)
  the two profiles are of different devices: /device:TPU:2 before, /device:TPU:1 now
where the time goes in v1:
time: 262 us; the launch traced here: 260 us
  waiting for transfers between devices  92.2 us (35%)
  starting transfers between devices  46.7 us (18%)
  blocking collectives  46.5 us (18%)
  local copies, waits for them, and re-layouts  35.9 us (14%)
  matrix products  18.1 us (7%)
  other arithmetic  17 us (6%)
    all_to_all x3, waiting for transfers between devices, spread(): lax.all_to_all(copies, axis, split_axis=0, concat_axis=0, tiled=True)  55.4 us
    all_to_all x1, blocking collectives, sum_at_owner(): lax.all_to_all(cut_along(value, dim, devices), axis, 0, 0, tiled=True)  28.3 us
    all_to_all x1, waiting for transfers between devices, from_everyone(): return lax.all_to_all(copies, axis, split_axis=0, concat_axis=0, tiled=True)  24 us
    all_to_all x3, starting transfers between devices, spread(): lax.all_to_all(copies, axis, split_axis=0, concat_axis=0, tiled=True)  22.1 us
    all_to_all x2, blocking collectives, spread(): lax.all_to_all(copies, axis, split_axis=0, concat_axis=0, tiled=True)  18.2 us
    dynamic_slice x16, local copies, waits for them, and re-layouts, local_chain(): return lax.scan(advance, begin, (decays, updates), reverse=backward)  11.3 us
    all_to_all x1, waiting for transfers between devices, entering_states(): received = lax.all_to_all(packed, SP, 0, 0, tiled=True)  8.74 us
    all_to_all x1, starting transfers between devices, entering_states(): received = lax.all_to_all(packed, SP, 0, 0, tiled=True)  8.15 us
  transfers between devices with their start and end apart: 8, of which 6 were waited for; matrix products, arithmetic and copies ran while one was open for 19% of the time, Pallas kernels for 0%

profile of v1, /device:TPU:1, one launch (start us, length us, event | category | flops | bytes accessed | tf_op | source)
XLA Modules:
  0.0 260.2 jit_solution(8667297334891006236)
XLA Ops:
  4.3 7.6 %all-to-all-start.1 = ((bf16[8,16,1280]{2,1,0:T(8,128)(2,1)}), bf16[8,16,1280]{2,1,0:T(8,128)(2,1)S(1)}, u32[]{:S(2)}, u32[]{:S(2)}) async-start(bf16[8,16,1280]{2,1,0:T(8,128)(2,1)} %broadcast_in_dim.68), calls=%async_computation.1 | async-start | bytes 655360 | tf_op jit(solution)/shard_map/all_to_all | solution.py:123
  14.4 7.7 %all-to-all-done.1 = bf16[8,16,1280]{2,1,0:T(8,128)(2,1)S(1)} async-done(((bf16[8,16,1280]{2,1,0:T(8,128)(2,1)}), bf16[8,16,1280]{2,1,0:T(8,128)(2,1)S(1)}, u32[]{:S(2)}, u32[]{:S(2)}) %all-to-all-start.1) | async-done | bytes 327712 | tf_op jit(solution)/shard_map/all_to_all | solution.py:123
  23.7 6.0 %all-to-all-start = ((bf16[4,128,2048]{2,1,0:T(8,128)(2,1)}), bf16[4,128,2048]{2,1,0:T(8,128)(2,1)S(1)}, u32[]{:S(2)}, u32[]{:S(2)}) async-start(bf16[4,128,2048]{2,1,0:T(8,128)(2,1)} %broadcast_in_dim.67), calls=%async_computation | async-start | bytes 4194304 | tf_op jit(solution)/shard_map/all_to_all | solution.py:25
  29.7 24.0 %all-to-all-done = bf16[4,128,2048]{2,1,0:T(8,128)(2,1)S(1)} async-done(((bf16[4,128,2048]{2,1,0:T(8,128)(2,1)}), bf16[4,128,2048]{2,1,0:T(8,128)(2,1)S(1)}, u32[]{:S(2)}, u32[]{:S(2)}) %all-to-all-start) | async-done | bytes 2097184 | tf_op jit(solution)/shard_map/all_to_all | solution.py:25
  54.8 10.0 %all-to-all-start.6 = ((bf16[8,8,16,512]{3,2,1,0:T(8,128)(2,1)}), bf16[8,8,16,512]{3,2,1,0:T(8,128)(2,1)}, u32[]{:S(2)}, u32[]{:S(2)}) async-start(bf16[8,8,16,512]{3,2,1,0:T(8,128)(2,1)} %broadcast_in_dim.75), calls=%async_computation.6 | async-start | bytes 2097152 | tf_op jit(solution)/shard_map/all_to_all | solution.py:123
  64.8 26.3 %all-to-all-done.6 = bf16[8,8,16,512]{3,2,1,0:T(8,128)(2,1)} async-done(((bf16[8,8,16,512]{3,2,1,0:T(8,128)(2,1)}), bf16[8,8,16,512]{3,2,1,0:T(8,128)(2,1)}, u32[]{:S(2)}, u32[]{:S(2)}) %all-to-all-start.6) | async-done | bytes 1048608 | tf_op jit(solution)/shard_map/all_to_all | solution.py:123
  92.6 9.6 %all_to_all.45 = bf16[2,8,8,16,512]{4,3,2,1,0:T(8,128)(2,1)} all-to-all(bf16[2,8,8,16,512]{4,3,2,1,0:T(8,128)(2,1)S(1)} %broadcast_in_dim.76), channel_id=1, replica_groups=mesh['sp_0'=8,'sp_1'=8,'sp_2'=2,'tp'=4] {'sp_2'}, dimensions={0} | all-to-all | bytes 4194304 | tf_op jit(solution)/shard_map/all_to_all | solution.py:123
  103.6 4.4 %all-to-all-start.2 = ((bf16[8,8,16,768]{3,2,1,0:T(8,128)(2,1)}), bf16[8,8,16,768]{3,2,1,0:T(8,128)(2,1)}, u32[]{:S(2)}, u32[]{:S(2)}) async-start(bf16[8,8,16,768]{3,2,1,0:T(8,128)(2,1)} %broadcast_in_dim.69), calls=%async_computation.2 | async-start | bytes 3145728 | tf_op jit(solution)/shard_map/all_to_all | solution.py:123
  115.3 1.9 rev.7
  124.8 21.5 %all-to-all-done.2 = bf16[8,8,16,768]{3,2,1,0:T(8,128)(2,1)} async-done(((bf16[8,8,16,768]{3,2,1,0:T(8,128)(2,1)}), bf16[8,8,16,768]{3,2,1,0:T(8,128)(2,1)}, u32[]{:S(2)}, u32[]{:S(2)}) %all-to-all-start.2) | async-done | bytes 1572896 | tf_op jit(solution)/shard_map/all_to_all | solution.py:123
  148.0 8.5 %all_to_all.46 = bf16[2,8,8,16,768]{4,3,2,1,0:T(8,128)(2,1)S(1)} all-to-all(bf16[2,8,8,16,768]{4,3,2,1,0:T(8,128)(2,1)S(1)} %broadcast_in_dim.70), channel_id=1, replica_groups=mesh['sp_0'=8,'sp_1'=8,'sp_2'=2,'tp'=4] {'sp_2'}, dimensions={0} | all-to-all | bytes 6291456 | tf_op jit(solution)/shard_map/all_to_all | solution.py:123
  160.1 1.9 collective-permute-start
  162.1 3.0 %collective-permute-start.1 = (bf16[8,256]{1,0:T(8,128)(2,1)}, bf16[8,256]{1,0:T(8,128)(2,1)}, u32[]{:S(2)}, u32[]{:S(2)}) collective-permute-start(bf16[8,256]{1,0:T(8,128)(2,1)} %get-tuple-element.354), channel_id=1, source_target_pairs={{4,0},{8,4},{12,8},{16,12},{20,16},{24,20},{28,24},{32,28},{36,32}... | collective-permute-start | bytes 12296 | tf_op jit(solution)/shard_map/ppermute | solution.py:47
  166.6 2.7 %bitcast_multiply_fusion.1 = (bf16[2,8,64,64]{3,1,2,0:T(8,128)(2,1)S(1)}, bf16[2,8,64,64]{3,1,2,0:T(8,128)(2,1)S(1)}, bf16[2,8,64,64]{3,1,2,0:T(8,128)(2,1)S(1)}...) fusion(f32[2,8,64,64]{3,1,2,0:T(8,128)S(1)} %fusion.86, ...), kind=kLoop, calls=%fused_computation.72 | loop fusion | flops 1048576 | bytes 1843200 | tf_op jit(solution)/shard_map/mul | solution.py:169
  169.6 7.0 %while.39 = (s32[]{:T(128)}, f32[2,64]{1,0:T(2,128)S(1)}, f32[2,64,128]{2,1,0:T(8,128)S(1)}, f32[8,2,64]{2,1,0:T(2,128)S(1)}, f32[8,2,64,128]{3,2,1,0:T(8,128)S(...) while((s32[]{:T(128)}, f32[2,64]{1,0:T(2,128)S(1)}, ...), condition=%wide.region_6.7_spmd.clone, body=%wide.region_5.6_spmd.clone.sunk | while | flops 65924 | bytes 333454 | solution.py:161
  177.5 7.0 %while.38 = (s32[]{:T(128)}, f32[2,64]{1,0:T(2,128)S(1)}, f32[2,64,128]{2,1,0:T(8,128)S(1)}, f32[8,2,64]{2,1,0:T(2,128)S(1)}, f32[8,2,64,128]{3,2,1,0:T(8,128)S(...) while((s32[]{:T(128)}, f32[2,64]{1,0:T(2,128)S(1)}, ...), condition=%wide.region_3.4_spmd.clone, body=%wide.region_2.3_spmd.clone.sunk | while | flops 65923 | bytes 333434 | solution.py:161
  185.7 8.1 %all-to-all-start.4 = ((bf16[128,3,128]{2,1,0:T(4,128)(2,1)}), bf16[128,3,128]{2,1,0:T(4,128)(2,1)}, u32[]{:S(2)}, u32[]{:S(2)}) async-start(bf16[128,3,128]{2,1,0:T(4,128)(2,1)} %pad_maximum_fusion), calls=%async_computation.4 | async-start | bytes 262144 | tf_op jit(solution)/shard_map/all_to_all | solution.py:104
  197.4 8.7 %all-to-all-done.4.received_ref = bf16[128,3,128]{2,1,0:T(4,128)(2,1)} async-done(((bf16[128,3,128]{2,1,0:T(4,128)(2,1)}), bf16[128,3,128]{2,1,0:T(4,128)(2,1)}, u32[]{:S(2)}, u32[]{:S(2)}) %all-to-all-start.4) | async-done | bytes 98336 | tf_op jit(solution)/shard_map/all_to_all | solution.py:104
  206.2 2.6 scan_states.1
  208.7 5.6 %all-to-all-start.5 = ((bf16[128,2,128]{2,1,0:T(2,128)(2,1)}), bf16[128,2,128]{2,1,0:T(2,128)(2,1)S(1)}, u32[]{:S(2)}, u32[]{:S(2)}) async-start(bf16[128,2,128]{2,1,0:T(2,128)(2,1)} %scan_states.1), calls=%async_computation.5 | async-start | bytes 131072 | tf_op jit(solution)/shard_map/all_to_all | solution.py:116
  214.3 7.5 %convolution_convert_fusion.2 = bf16[512,256]{0,1:T(8,128)(2,1)} fusion(f32[528,256]{1,0:T(8,128)} %maximum_convert_fusion, f32[512]{0:T(512)S(1)} %copy-done.11, f32[]{:T(128)S(6)} %convert_element_type.133, f32[]{:T(128)S(6)} %convert_element_type.132, f32[]{:T(128)S(6)} %convert_element_type.131, f32[]{:T(128)S(6)} %convert_element_type.130, ...), kind=kOutput, calls=%fused_computation.25 | convolution fusion | flops 71696384 | bytes 8783940 | tf_op jit(solution)/shard_map/dot_general | solution.py:252
  221.8 4.1 %all-to-all-done.5 = bf16[128,2,128]{2,1,0:T(2,128)(2,1)S(1)} async-done(((bf16[128,2,128]{2,1,0:T(2,128)(2,1)}), bf16[128,2,128]{2,1,0:T(2,128)(2,1)S(1)}, u32[]{:S(2)}, u32[]{:S(2)}) %all-to-all-start.5) | async-done | bytes 65568 | tf_op jit(solution)/shard_map/all_to_all | solution.py:116
  228.3 2.3 convolution_convert_fusion
  230.6 28.3 %all_to_all.47 = bf16[4,128,2048]{2,1,0:T(8,128)(2,1)S(1)} all-to-all(bf16[4,128,2048]{2,1,0:T(8,128)(2,1)S(1)} %bitcast.135), channel_id=1, replica_groups=mesh['sp_0'=8,'sp_1'=8,'sp_2'=2,'tp'=4] {'tp'}, dimensions={0} | all-to-all | bytes 4194304 | tf_op jit(solution)/shard_map/all_to_all | solution.py:140
  (182 shorter events, 56.7 us)
Async XLA Ops:
  0.0 214.3 %copy-start = (bf16[4,256,256]{2,1,0:T(8,128)(2,1)S(1)}, bf16[4,256,256]{2,1,0:T(8,128)(2,1)}, u32[]{:S(2)}) copy-start(bf16[4,256,256]{2,1,0:T(8,128)(2,1)} %param.27) | copy-start | bytes 1572868
  4.3 17.8 %all-to-all-start.1 = ((bf16[8,16,1280]{2,1,0:T(8,128)(2,1)}), bf16[8,16,1280]{2,1,0:T(8,128)(2,1)S(1)}, u32[]{:S(2)}, u32[]{:S(2)}) async-start(bf16[8,16,1280]{2,1,0:T(8,128)(2,1)} %broadcast_in_dim.68), calls=%async_computation.1 | async-start | bytes 655360 | tf_op jit(solution)/shard_map/all_to_all | solution.py:123
  22.1 42.7 %copy-start.5 = (bf16[8,16,1280]{2,1,0:T(8,128)(2,1)}, bf16[8,16,1280]{2,1,0:T(8,128)(2,1)S(1)}, u32[]{:S(2)}) copy-start(bf16[8,16,1280]{2,1,0:T(8,128)(2,1)S(1)} %all-to-all-done.1) | copy-start | bytes 983044
  23.7 30.0 %all-to-all-start = ((bf16[4,128,2048]{2,1,0:T(8,128)(2,1)}), bf16[4,128,2048]{2,1,0:T(8,128)(2,1)S(1)}, u32[]{:S(2)}, u32[]{:S(2)}) async-start(bf16[4,128,2048]{2,1,0:T(8,128)(2,1)} %broadcast_in_dim.67), calls=%async_computation | async-start | bytes 4194304 | tf_op jit(solution)/shard_map/all_to_all | solution.py:25
  54.8 36.3 %all-to-all-start.6 = ((bf16[8,8,16,512]{3,2,1,0:T(8,128)(2,1)}), bf16[8,8,16,512]{3,2,1,0:T(8,128)(2,1)}, u32[]{:S(2)}, u32[]{:S(2)}) async-start(bf16[8,8,16,512]{3,2,1,0:T(8,128)(2,1)} %broadcast_in_dim.75), calls=%async_computation.6 | async-start | bytes 2097152 | tf_op jit(solution)/shard_map/all_to_all | solution.py:123
  92.6 9.6 %slice-start = ((bf16[8,16,1280]{2,1,0:T(8,128)(2,1)}), bf16[8,16,768]{2,1,0:T(8,128)(2,1)S(1)}, s32[]{:S(2)}) async-start(bf16[8,16,1280]{2,1,0:T(8,128)(2,1)} %copy-done.5), calls=%async_computation.9 | async-start | bytes 393216 | tf_op jit(solution)/shard_map/slice | solution.py:213
  103.6 4.7 %copy-start.10 = (f32[2,512]{1,0:T(2,128)S(1)}, f32[2,512]{1,0:T(2,128)}, u32[]{:S(2)}) copy-start(f32[2,512]{1,0:T(2,128)} %param.25) | copy-start | bytes 12292
  103.6 6.8 %copy-start.6 = (bf16[2048,64]{0,1:T(8,128)(2,1)S(1)}, bf16[2048,64]{0,1:T(8,128)(2,1)}, u32[]{:S(2)}) copy-start(bf16[2048,64]{0,1:T(8,128)(2,1)} %param.22) | copy-start | bytes 786436
  103.6 42.7 %all-to-all-start.2 = ((bf16[8,8,16,768]{3,2,1,0:T(8,128)(2,1)}), bf16[8,8,16,768]{3,2,1,0:T(8,128)(2,1)}, u32[]{:S(2)}, u32[]{:S(2)}) async-start(bf16[8,8,16,768]{3,2,1,0:T(8,128)(2,1)} %broadcast_in_dim.69), calls=%async_computation.2 | async-start | bytes 3145728 | tf_op jit(solution)/shard_map/all_to_all | solution.py:123
  119.3 3.9 %copy-start.1 = (bf16[2,8,8,16,512]{4,3,2,1,0:T(8,128)(2,1)S(1)}, bf16[2,8,8,16,512]{4,3,2,1,0:T(8,128)(2,1)}, u32[]{:S(2)}) copy-start(bf16[2,8,8,16,512]{4,3,2,1,0:T(8,128)(2,1)} %all_to_all.45) | copy-start | bytes 6291460
  121.8 0.8 copy-start.2
  158.7 7.8 %copy-start.3 = (f32[2,8,64,64]{3,1,2,0:T(8,128)S(1)}, f32[2,8,64,64]{3,1,2,0:T(8,128)}, u32[]{:S(2)}) copy-start(f32[2,8,64,64]{3,1,2,0:T(8,128)} %copy-done.2) | copy-start | bytes 786436
  160.1 35.5 %collective-permute-start = (bf16[8,256]{1,0:T(8,128)(2,1)}, bf16[8,256]{1,0:T(8,128)(2,1)}, u32[]{:S(2)}, u32[]{:S(2)}) collective-permute-start(bf16[8,256]{1,0:T(8,128)(2,1)} %get-tuple-element.353), channel_id=1, source_target_pairs={{0,4},{4,8},{8,12},{12,16},{16,20},{20,24},{24,28},{28,32},{32,36}... | collective-permute-start | bytes 12296 | tf_op jit(solution)/shard_map/ppermute | solution.py:46
  162.1 33.6 %collective-permute-start.1 = (bf16[8,256]{1,0:T(8,128)(2,1)}, bf16[8,256]{1,0:T(8,128)(2,1)}, u32[]{:S(2)}, u32[]{:S(2)}) collective-permute-start(bf16[8,256]{1,0:T(8,128)(2,1)} %get-tuple-element.354), channel_id=1, source_target_pairs={{4,0},{8,4},{12,8},{16,12},{20,16},{24,20},{28,24},{32,28},{36,32}... | collective-permute-start | bytes 12296 | tf_op jit(solution)/shard_map/ppermute | solution.py:47
  176.6 0.6 copy-start.8
  177.2 16.7 %copy-start.7 = (pred[64,64]{1,0:T(8,128)(4,1)S(1)}, pred[64,64]{1,0:T(8,128)(4,1)}, u32[]{:S(2)}) copy-start(pred[64,64]{1,0:T(8,128)(4,1)} %iota_compare_fusion.1) | copy-start | bytes 12292
  184.5 11.1 %copy-start.9 = (f32[8,2,64]{2,1,0:T(2,128)S(1)}, f32[8,2,64]{2,1,0:T(2,128)}, u32[]{:S(2)}) copy-start(f32[8,2,64]{2,1,0:T(2,128)} %copy-done.8) | copy-start | bytes 12292
  185.7 28.6 %copy-start.11 = (f32[512]{0:T(512)S(1)}, f32[512]{0:T(512)}, u32[]{:S(2)}) copy-start(f32[512]{0:T(512)} %add_convert_fusion) | copy-start | bytes 6148
  185.7 20.5 %all-to-all-start.4 = ((bf16[128,3,128]{2,1,0:T(4,128)(2,1)}), bf16[128,3,128]{2,1,0:T(4,128)(2,1)}, u32[]{:S(2)}, u32[]{:S(2)}) async-start(bf16[128,3,128]{2,1,0:T(4,128)(2,1)} %pad_maximum_fusion), calls=%async_computation.4 | async-start | bytes 262144 | tf_op jit(solution)/shard_map/all_to_all | solution.py:104
  208.7 17.1 %all-to-all-start.5 = ((bf16[128,2,128]{2,1,0:T(2,128)(2,1)}), bf16[128,2,128]{2,1,0:T(2,128)(2,1)S(1)}, u32[]{:S(2)}, u32[]{:S(2)}) async-start(bf16[128,2,128]{2,1,0:T(2,128)(2,1)} %scan_states.1), calls=%async_computation.5 | async-start | bytes 131072 | tf_op jit(solution)/shard_map/all_to_all | solution.py:116
  226.7 1.6 copy-start.4

commit v2 on v0

v2 whole, which is shorter than its diff:
```python
import jax
import jax.numpy as jnp
from jax import lax
from jax.experimental import pallas as pl
from jax.experimental.pallas import tpu as pltpu
from jax.sharding import Mesh
from jax.sharding import PartitionSpec as P


KEY_CHANNELS = 64
DV = 128
RANK = 32
BLOCK = 64
LANES = 128
SP = ("sp_0", "sp_1", "sp_2")
CHIPS = ("sp_0", "sp_1")
SP_TP = ("sp_0", "sp_1", "sp_2", "tp")

eps_value = 1e-06
gate_norm_factor = 16.0
rim_width = 8
interpreted = False

bf16 = jnp.bfloat16
f32 = jnp.float32
exact = lax.Precision.HIGHEST


def matmul(a, b, dims=((1,), (0,)), precision=None):
    return lax.dot_general(a, b, (dims, ((), ())), precision=precision, preferred_element_type=f32)


def call(kernel, out_shapes, operands, scalars=1, scratch=(), flops=0, moved=0):
    smem = pl.BlockSpec(memory_space=pltpu.SMEM)
    vmem = pl.BlockSpec(memory_space=pltpu.VMEM)
    return pl.pallas_call(
        kernel,
        in_specs=[smem if i < scalars else vmem for i in range(len(operands))],
        out_specs=jax.tree.map(lambda _: vmem, out_shapes),
        out_shape=out_shapes,
        scratch_shapes=list(scratch),
        cost_estimate=pl.CostEstimate(flops=flops, bytes_accessed=moved, transcendentals=0),
        interpret=interpreted,
    )(*operands)


def shifted(value, axis, step):
    devices = lax.axis_size(axis)
    return lax.ppermute(value, axis, [(i, (i + step) % devices) for i in range(devices)])


def neighbours(value, axes, step):
    devices = lax.axis_size(axes)
    pairs = [(i, i + step) for i in range(devices) if 0 <= i + step < devices]
    return lax.ppermute(value, axes, pairs)


def normalize(token_rows):
    floats = token_rows.astype(f32)
    scaled = floats * lax.rsqrt(jnp.mean(floats * floats, axis=-1, keepdims=True) + eps_value)
    return scaled.astype(bf16)


def place_tokens(tp, pieces, whole_ref, first):
    own, before, after, far_top, far_end = pieces
    rows = own.shape[0]
    half = rows // 2

    def at(step):
        return pl.multiple_of(first + lax.rem(tp + step, 4) * rows, 8)

    whole_ref[pl.ds(at(0), rows), :] = own[...]
    whole_ref[pl.ds(at(3), rows), :] = before[...]
    whole_ref[pl.ds(at(1), rows), :] = after[...]
    far = at(2)
    whole_ref[pl.ds(far, half), :] = far_top[...]
    whole_ref[pl.ds(pl.multiple_of(far + half, 8), half), :] = far_end[...]


def split_dot(ones, values):
    high = values.astype(bf16)
    low = (values - high.astype(f32)).astype(bf16)
    return matmul(ones, high) + matmul(ones, low)


def project_kernel(
    place,
    own,
    before,
    after,
    far_top,
    far_end,
    weight_own,
    weight_other,
    inner,
    outer,
    bias,
    spike,
    qkv_out,
    pool_out,
    logs_out,
    packed_out,
    tokens_ref,
    weight_ref,
):
    tp, core = (place[0], place[1])
    place_tokens(tp, (own, before, after, far_top, far_end), tokens_ref, 0)
    weight_ref[:, pl.ds(core, 1)] = weight_own[...][:, None]
    weight_ref[:, pl.ds(1 - core, 1)] = weight_other[...][:, None]
    rows, width = tokens_ref.shape
    tokens = tokens_ref[...]
    low_rank = matmul(tokens, inner[...]).astype(bf16)
    projected = matmul(tokens, weight_ref[...].reshape(width, -1)).astype(bf16)
    qkv = projected[:, : 4 * LANES]
    qkv_out[...] = qkv
    pool_out[...] = projected[:, 4 * LANES :]
    here = pl.ds(pl.multiple_of(tp * LANES, LANES), LANES)
    blank = jnp.zeros((RANK, LANES), bf16)
    outer_both = jnp.concatenate(
        [
            jnp.concatenate([outer[0, :, here], blank], axis=1),
            jnp.concatenate([blank, outer[1, :, here]], axis=1),
        ],
        axis=0,
    )
    bias_both = jnp.concatenate([bias[0:1, here], bias[1:2, here]], axis=1)
    pre = matmul(low_rank, outer_both) + bias_both
    gate = jnp.minimum(pre, 0.0) - jnp.log1p(jnp.exp(-jnp.abs(pre)))
    lane = lax.broadcasted_iota(jnp.int32, (rows, LANES), 1)
    spikes = jnp.where(lane < KEY_CHANNELS, spike[:, 0:1], spike[:, 1:2])
    decay = gate * (1.0 / gate_norm_factor) + jnp.concatenate([spikes, spikes], axis=1)
    size = LANES
    row_ids = lax.broadcasted_iota(jnp.int32, (size, size), 0)
    col_ids = lax.broadcasted_iota(jnp.int32, (size, size), 1)
    upto = (col_ids <= row_ids).astype(bf16)
    onward = (col_ids >= row_ids).astype(bf16)
    tiles = rows // size
    carry = jnp.zeros((1, LANES), f32)
    for n in range(tiles):
        found = split_dot(upto, decay[n * size : (n + 1) * size, :LANES]) + carry
        logs_out[0, n * size : (n + 1) * size, :] = found
        carry = found[size - 1 : size, :]
    total_fwd = carry
    carry = jnp.zeros((1, LANES), f32)
    for n in reversed(range(tiles)):
        found = split_dot(onward, decay[n * size : (n + 1) * size, LANES:]) + carry
        logs_out[1, n * size : (n + 1) * size, :] = found
        carry = found[0:1, :]
    total_bwd = carry
    keys = qkv[:, LANES : 2 * LANES].astype(f32)
    weighted = jnp.concatenate(
        [
            (keys * jnp.exp(total_fwd - logs_out[0])).astype(bf16),
            (keys * jnp.exp(total_bwd - logs_out[1])).astype(bf16),
        ],
        axis=1,
    )
    updates = matmul(weighted, qkv[:, 2 * LANES :], ((0,), (0,)))
    first = lax.broadcasted_iota(jnp.int32, (LANES, LANES), 0) < KEY_CHANNELS
    for d in range(2):
        mine = updates[d * LANES : (d + 1) * LANES]
        packed_out[:, 0, d * LANES : (d + 1) * LANES] = jnp.where(
            first, mine[:, :LANES], mine[:, LANES:]
        )
    totals = jnp.concatenate([total_fwd, total_bwd], axis=0)
    stacked = jnp.concatenate([totals, jnp.zeros((LANES - 2, LANES), f32)], axis=0)
    packed_out[:, 0, 2 * LANES :] = stacked.T


def scan_kernel(place, received, start, out):
    devices = received.shape[0]
    here = place[0]
    logs = received[:, 0, 2 * LANES :]
    row = lax.broadcasted_iota(jnp.int32, (devices, devices), 0)
    col = lax.broadcasted_iota(jnp.int32, (devices, devices), 1)
    earlier = (col < row).astype(f32)
    upto = (row <= col).astype(f32)
    strictly = (row < col).astype(f32)
    before_col = matmul(earlier, logs, precision=exact)
    before_row = matmul(logs, strictly, ((0,), (0,)), precision=exact)
    past_row = matmul(logs, upto, ((0,), (0,)), precision=exact)
    past_col = before_col + logs
    total = jnp.sum(logs, axis=0, keepdims=True)
    for r in range(2):
        if r == 0:
            between = before_col[:, 0:1] - past_row[0:1, :]
            allowed = col < row
            outside = before_col[:, 0:1]
        else:
            between = before_row[1:2, :] - past_col[:, 1:2]
            allowed = col > row
            outside = total[:, 1:2] - past_col[:, 1:2]
        weights = jnp.where(allowed, jnp.exp(jnp.minimum(between, 0.0)), 0.0)
        high = weights.astype(bf16)
        low = (weights - high.astype(f32)).astype(bf16)
        updates = received[:, 0, r * LANES : (r + 1) * LANES].astype(bf16)
        first = start[r, pl.ds(here, 1), :]
        entering = matmul(high, updates) + matmul(low, updates)
        entering = entering + jnp.exp(jnp.minimum(outside, 0.0)) * first
        out[:, 0, r * LANES : (r + 1) * LANES] = entering


def inner_kernel(qkv, logs, part_out, query_out):
    rows = qkv.shape[0]
    blocks = rows // BLOCK
    lane = lax.broadcasted_iota(jnp.int32, (BLOCK, LANES), 1)
    row = lax.broadcasted_iota(jnp.int32, (BLOCK, LANES), 0)
    head_one = lane < KEY_CHANNELS
    lower = lax.rem(lane, KEY_CHANNELS) <= row
    value_lane = lax.broadcasted_iota(jnp.int32, (BLOCK, 2 * DV), 1)
    value_one = value_lane < DV
    diagonal = (
        lax.rem(lax.broadcasted_iota(jnp.int32, (4 * KEY_CHANNELS, 2 * DV), 0), LANES)
        < KEY_CHANNELS
    ) == (lax.broadcasted_iota(jnp.int32, (4 * KEY_CHANNELS, 2 * DV), 1) < DV)
    zero = jnp.zeros((), bf16)
    scale = KEY_CHANNELS ** (-0.5)
    edges, updates, scaled, scored = [], [], [], []
    nothing = jnp.zeros((1, LANES), f32)
    for n in range(blocks):
        at = slice(n * BLOCK, (n + 1) * BLOCK)
        base_fwd = logs[0, n * BLOCK - 1 : n * BLOCK, :] if n else nothing
        base_bwd = logs[1, (n + 1) * BLOCK : (n + 1) * BLOCK + 1, :] if n + 1 < blocks else nothing
        cum_fwd = logs[0, at, :] - base_fwd
        cum_bwd = logs[1, at, :] - base_bwd
        edge_fwd = cum_fwd[BLOCK - 1 : BLOCK, :]
        edge_bwd = cum_bwd[0:1, :]
        queries = qkv[at, :LANES].astype(f32) * scale
        keys = qkv[at, LANES : 2 * LANES].astype(f32)
        values = qkv[at, 2 * LANES :]
        query_out[at, :LANES] = (queries * jnp.exp(logs[0, at, :])).astype(bf16)
        query_out[at, LANES:] = (queries * jnp.exp(logs[1, at, :])).astype(bf16)
        query_fwd = (queries * jnp.exp(cum_fwd)).astype(bf16)
        query_bwd = (queries * jnp.exp(cum_bwd)).astype(bf16)
        key_fwd = (keys * jnp.exp(-cum_fwd)).astype(bf16)
        key_bwd = (keys * jnp.exp(-cum_bwd)).astype(bf16)

        def by_head(key):
            return jnp.concatenate(
                [jnp.where(head_one, key, zero), jnp.where(head_one, zero, key)], axis=0
            )

        across = ((1,), (1,))
        scores = jnp.where(
            lower,
            matmul(query_fwd, by_head(key_fwd), across),
            matmul(query_bwd, by_head(key_bwd), across),
        ).astype(bf16)
        spread = jnp.concatenate(
            [jnp.where(value_one, values, zero), jnp.where(value_one, zero, values)], axis=0
        )
        scored.append(matmul(scores, spread))
        scaled.append(jnp.concatenate([query_fwd, query_bwd], axis=1))
        weighted = jnp.concatenate(
            [
                (keys * jnp.exp(edge_fwd - cum_fwd)).astype(bf16),
                (keys * jnp.exp(edge_bwd - cum_bwd)).astype(bf16),
            ],
            axis=1,
        )
        update = matmul(weighted, values, ((0,), (0,)))
        updates.append(jnp.where(diagonal, update, 0.0))
        edges.append((edge_fwd, edge_bwd))
    stacked = jnp.concatenate(
        [e[0] for e in edges]
        + [e[1] for e in edges]
        + [jnp.zeros((LANES - 2 * blocks, LANES), f32)],
        axis=0,
    )
    factors = jnp.exp(stacked.T)
    start_fwd, start_bwd = [None] * blocks, [None] * blocks
    memory = jnp.zeros((LANES, 2 * DV), f32)
    for n in range(blocks):
        start_fwd[n] = memory.astype(bf16)
        memory = factors[:, n : n + 1] * memory + updates[n][:LANES]
    memory = jnp.zeros((LANES, 2 * DV), f32)
    for n in reversed(range(blocks)):
        start_bwd[n] = memory.astype(bf16)
        memory = factors[:, blocks + n : blocks + n + 1] * memory + updates[n][LANES:]
    for n in range(blocks):
        entering = jnp.concatenate([start_fwd[n], start_bwd[n]], axis=0)
        part_out[n * BLOCK : (n + 1) * BLOCK, :] = scored[n] + matmul(scaled[n], entering)


def pool_kernel(place, pool_input, rim_before, rim_after, group_map, out):
    tp, here = (place[0], place[2])
    rows = out.shape[0]
    padded = rows + 2 * rim_width
    values = jnp.concatenate([rim_before[...], pool_input[...], rim_after[...]], axis=0).astype(f32)
    sums = values + pltpu.roll(values, 1, 0)
    chosen = sums
    for level in (1, 2, 3):
        step = 2 ** (level - 1)
        sums = pltpu.roll(sums, step, 0) + pltpu.roll(sums, padded - step, 0)
        chosen = jnp.where(tp >= level, sums, chosen)
    half = jnp.left_shift(1, tp)
    position = here * rows + lax.broadcasted_iota(jnp.int32, (rows, LANES), 0)
    last = place[3] * rows - 1
    low_end = jnp.maximum(position - half, 0)
    high_end = jnp.minimum(position + half - 1, last)
    counted = (high_end - low_end + 1).astype(f32)[:, 0:1]
    inside = slice(rim_width, rim_width + rows)
    pooled = (chosen[inside] / counted - values[inside]).astype(bf16)
    out[...] = matmul(pooled, group_map[tp]).astype(bf16)


def finish_kernel(part, query, entering, pooled, out):
    channel_one = lax.broadcasted_iota(jnp.int32, (LANES, DV), 0) < KEY_CHANNELS
    zero = jnp.zeros((), bf16)
    sides = []
    for d in range(2):
        state = entering[:, 0, d * LANES : (d + 1) * LANES].astype(bf16)
        sides.append(
            jnp.concatenate(
                [jnp.where(channel_one, state, zero), jnp.where(channel_one, zero, state)], axis=1
            )
        )
    joined = part[...] + matmul(query[...], jnp.concatenate(sides, axis=0))
    rows = joined.shape[0]
    ready = [pooled[...]]
    for h in range(2):
        mine = joined[:, h * DV : (h + 1) * DV]
        scale = lax.rsqrt(jnp.mean(mine * mine, axis=1, keepdims=True) + eps_value)
        ready.append((mine * scale).astype(bf16))
    owners = out.shape[0]
    for j in range(owners):
        at = slice(j * rows // owners, (j + 1) * rows // owners)
        start = 0
        for piece in ready:
            out[j, :, start : start + piece.shape[1]] = piece[at]
            start += piece.shape[1]


def output_kernel(place, activations, weight, out):
    tp = place[0]
    groups, _, width = activations.shape
    total = None
    for s in range(groups):
        source = lax.rem(tp + groups - s, groups)
        partial = matmul(
            activations[source], weight[:, s * width : (s + 1) * width], ((1,), (1,))
        )
        partial = partial.astype(bf16).astype(f32)
        total = partial if total is None else total + partial
    out[...] = total.astype(bf16)


def output_projection(place, activations, weights):
    groups, rows, width = activations.shape
    model = weights.shape[0]
    tile = 256
    return pl.pallas_call(
        output_kernel,
        grid=(model // tile,),
        in_specs=[
            pl.BlockSpec(memory_space=pltpu.SMEM),
            pl.BlockSpec((groups, rows, width), lambda n: (0, 0, 0)),
            pl.BlockSpec((tile, groups * width), lambda n: (n, 0)),
        ],
        out_specs=pl.BlockSpec((rows, tile), lambda n: (0, n)),
        out_shape=jax.ShapeDtypeStruct((rows, model), bf16),
        interpret=interpreted,
        name="output_kernel",
    )(place, activations, weights)


def shape_of(*lengths, kind=bf16):
    return jax.ShapeDtypeStruct(lengths, kind)


def shards(
    tokens,
    pooling_input_weight,
    query_matrix,
    key_matrix,
    value_matrix,
    decay_inner_weight,
    decay_outer_weight,
    channel_decay_bias,
    spike_log_decay,
    starting_state,
    pooling_group_map,
    pooling_output_weight,
    attention_output_weight,
):
    sp_index = lax.axis_index(SP)
    tp_index = lax.axis_index("tp")
    core = lax.axis_index("sp_2")
    positions = lax.axis_size(SP)
    place = jnp.stack([tp_index, core, sp_index, jnp.int32(positions)]).astype(jnp.int32)
    groups = lax.axis_size("tp")
    rows = tokens.shape[0] * groups
    model = tokens.shape[1]

    local_in = jnp.concatenate(
        [query_matrix, key_matrix, value_matrix, pooling_input_weight], axis=1
    )
    chips = lax.axis_size(CHIPS)
    copies = jnp.broadcast_to(local_in, (chips, *local_in.shape))
    weight_own = lax.all_to_all(copies, CHIPS, 0, 0, tiled=True)
    local_out = jnp.concatenate([pooling_output_weight, attention_output_weight], axis=0).T
    outs = [local_out] + [shifted(local_out, "tp", k) for k in range(1, groups)]
    normed = normalize(tokens)
    half = normed.shape[0] // 2
    before = shifted(normed, "tp", 1)
    after = shifted(normed, "tp", -1)
    top, end = (before[:half], after[half:])
    far_top = shifted(top, "tp", 1)
    far_end = shifted(end, "tp", -1)
    weight_other = shifted(weight_own, "sp_2", 1)
    whole_out = lax.all_gather(jnp.concatenate(outs, axis=1), SP, axis=0, tiled=True)

    qkv, pool_input, logs, packed = call(
        project_kernel,
        (
            shape_of(rows, 4 * LANES),
            shape_of(rows, 2 * LANES),
            shape_of(2, rows, LANES, kind=f32),
            shape_of(LANES, 1, 3 * LANES, kind=f32),
        ),
        (
            place,
            normed,
            before,
            after,
            far_top,
            far_end,
            weight_own,
            weight_other,
            decay_inner_weight,
            decay_outer_weight,
            channel_decay_bias,
            spike_log_decay.T,
        ),
        scratch=(
            pltpu.VMEM((rows, model), bf16),
            pltpu.VMEM((chips, 2, model // (2 * chips), 6 * LANES), bf16),
        ),
        flops=2 * rows * model * 7 * LANES,
        moved=10_000_000,
    )
    received = lax.all_to_all(packed, SP, 0, 0, tiled=True)
    rim_before = neighbours(pool_input[rows - rim_width :], SP, 1)
    rim_after = neighbours(pool_input[:rim_width], SP, -1)
    part, query = call(
        inner_kernel,
        (shape_of(rows, 2 * DV, kind=f32), shape_of(rows, 2 * LANES)),
        (qkv, logs),
        scalars=0,
        flops=2 * rows * model * 2 * LANES,
        moved=3_000_000,
    )
    states = call(
        scan_kernel,
        shape_of(positions, 1, 2 * LANES, kind=f32),
        (place[2:3], received, starting_state.reshape(2, -1, DV)),
        flops=40_000_000,
    )
    entering = lax.all_to_all(states, SP, 0, 0, tiled=True)
    pooled = call(
        pool_kernel,
        shape_of(rows, 2 * LANES),
        (place, pool_input, rim_before, rim_after, pooling_group_map),
        flops=2 * rows * 4 * LANES * LANES,
        moved=1_000_000,
    )
    activations = call(
        finish_kernel,
        shape_of(groups, rows // groups, 4 * LANES),
        (part, query, entering, pooled),
        scalars=0,
        flops=100_000_000,
        moved=2_000_000,
    )
    gathered = lax.all_to_all(activations, "tp", 0, 0, tiled=True)
    return output_projection(place, gathered, whole_out)


def solution(mesh):
    split = Mesh(mesh.devices.reshape(8, 8, 2, mesh.shape["tp"]), ("sp_0", "sp_1", "sp_2", "tp"))
    in_specs = (
        P(SP_TP, None),
        P(SP, "tp"),
        P(SP, "tp"),
        P(SP, "tp"),
        P(SP, "tp"),
        P(),
        P(),
        P(),
        P("tp", SP),
        P(None, "tp", None, None),
        P(),
        P("tp", SP),
        P("tp", SP),
    )
    out_specs = P(SP_TP, None)
    return jax.shard_map(
        shards, mesh=split, in_specs=in_specs, out_specs=out_specs, check_vma=False
    )
```

time: 328 us -> 197 us (0.60)
  the two profiles are of different devices: /device:TPU:2 before, /device:TPU:25 now
where the time goes in v2:
time: 197 us; the launch traced here: 196 us
  blocking collectives  89.9 us (46%)
  starting transfers between devices  45.3 us (23%)
  Pallas kernels  26.2 us (13%)
  waiting for transfers between devices  14.4 us (7%)
  between operations  13.6 us (7%)
  local copies, waits for them, and re-layouts  3.98 us (2%)
  other arithmetic  3.04 us (2%)
    all_to_all x1, blocking collectives, shards(): weight_own = lax.all_to_all(copies, CHIPS, 0, 0, tiled=True)  54.4 us
    ppermute x8, starting transfers between devices, shifted(): lax.ppermute(value, axis, [(i, (i + step) % devices) for i in range(devic...  30 us
    all_to_all x1, blocking collectives, shards(): received = lax.all_to_all(packed, SP, 0, 0, tiled=True)  21.2 us
    pallas_call x5, Pallas kernels, call(): pl.pallas_call(kernel, in_specs=[smem if i < scalars else vmem for i in r...  17.6 us
    all_to_all x1, blocking collectives, shards(): gathered = lax.all_to_all(activations, 'tp', 0, 0, tiled=True)  14.4 us
    ppermute x8, waiting for transfers between devices, shifted(): lax.ppermute(value, axis, [(i, (i + step) % devices) for i in range(devic...  13.4 us
    all_to_all x1, starting transfers between devices, shards(): entering = lax.all_to_all(states, SP, 0, 0, tiled=True)  8.57 us
    pallas_call x1, Pallas kernels, output_projection(): pl.pallas_call(output_kernel, grid=(model // tile,), in_specs=[pl.BlockSp...  8.55 us
  transfers between devices with their start and end apart: 12, of which 5 were waited for; matrix products, arithmetic and copies ran while one was open for 2% of the time, Pallas kernels for 9%

profile of v2, /device:TPU:25, one launch (start us, length us, event | category | flops | bytes accessed | tf_op | source)
XLA Modules:
  0.0 196.5 jit_solution(1436542405330331632)
XLA Ops:
  7.3 3.1 %collective-permute-start.7 = (bf16[16,512]{1,0:T(8,128)(2,1)S(1)}, bf16[16,512]{1,0:T(8,128)(2,1)S(1)}, u32[]{:S(2)}, u32[]{:S(2)}) collective-permute-start(bf16[16,512]{1,0:T(8,128)(2,1)S(1)} %maximum_bitcast_fusion), channel_id=1, source_target_pairs={{0,1},{1,2},{2,3},{3,0},{4,5},{5,6},{6,7},{7,4},{8,9},{9,10},{10,1... | collective-permute-start | bytes 49160 | tf_op jit(solution)/shard_map/ppermute | solution.py:49
  10.4 4.4 %collective-permute-start.8 = (bf16[16,512]{1,0:T(8,128)(2,1)S(1)}, bf16[16,512]{1,0:T(8,128)(2,1)S(1)}, u32[]{:S(2)}, u32[]{:S(2)}) collective-permute-start(bf16[16,512]{1,0:T(8,128)(2,1)S(1)} %maximum_bitcast_fusion), channel_id=1, source_target_pairs={{0,2},{1,3},{2,0},{3,1},{4,6},{5,7},{6,4},{7,5},{8,10},{9,11},{10,... | collective-permute-start | bytes 49160 | tf_op jit(solution)/shard_map/ppermute | solution.py:49
  14.7 3.1 %collective-permute-start.9 = (bf16[16,512]{1,0:T(8,128)(2,1)S(1)}, bf16[16,512]{1,0:T(8,128)(2,1)S(1)}, u32[]{:S(2)}, u32[]{:S(2)}) collective-permute-start(bf16[16,512]{1,0:T(8,128)(2,1)S(1)} %maximum_bitcast_fusion), channel_id=1, source_target_pairs={{0,3},{1,0},{2,1},{3,2},{4,7},{5,4},{6,5},{7,6},{8,11},{9,8},{10,9... | collective-permute-start | bytes 49160 | tf_op jit(solution)/shard_map/ppermute | solution.py:49
  17.8 1.4 collective-permute-done.9
  20.7 54.4 %all_to_all.20.weight_own = bf16[64,16,768]{2,1,0:T(8,128)(2,1)S(1)} all-to-all(bf16[64,16,768]{2,1,0:T(8,128)(2,1)S(1)} %broadcast_in_dim.4), channel_id=1, replica_groups=mesh['sp_0'=8,'sp_1'=8,'sp_2'=2,'tp'=4] {'sp_0','sp_1'}, dimensions={0} | all-to-all | bytes 3145728 | tf_op jit(solution)/shard_map/all_to_all | solution.py:400
  75.1 6.5 %collective-permute-start.4 = (bf16[64,16,768]{2,1,0:T(8,128)(2,1)S(1)}, bf16[64,16,768]{2,1,0:T(8,128)(2,1)}, u32[]{:S(2)}, u32[]{:S(2)}) collective-permute-start(bf16[64,16,768]{2,1,0:T(8,128)(2,1)S(1)} %all_to_all.20.weight_own), channel_id=1, source_target_pairs={{0,4},{4,0},{1,5},{5,1},{2,6},{6,2},{3,7},{7,3},{8,12},{12,8},{9,1... | collective-permute-start | bytes 4718600 | tf_op jit(solution)/shard_map/ppermute | solution.py:49
  82.0 1.9 collective-permute-start
  83.9 4.6 %collective-permute-start.1 = (bf16[128,2048]{1,0:T(8,128)(2,1)S(1)}, bf16[128,2048]{1,0:T(8,128)(2,1)S(1)}, u32[]{:S(2)}, u32[]{:S(2)}) collective-permute-start(bf16[128,2048]{1,0:T(8,128)(2,1)S(1)} %fusion.1.own), channel_id=1, source_target_pairs={{0,3},{1,0},{2,1},{3,2},{4,7},{5,4},{6,5},{7,6},{8,11},{9,8},{10,9... | collective-permute-start | bytes 1572872 | tf_op jit(solution)/shard_map/ppermute | solution.py:49
  88.5 10.1 %collective-permute-done.before = bf16[128,2048]{1,0:T(8,128)(2,1)S(1)} collective-permute-done((bf16[128,2048]{1,0:T(8,128)(2,1)S(1)}, bf16[128,2048]{1,0:T(8,128)(2,1)S(1)}, u32[]{:S(2)}, u32[]{:S(2)}) %collective-permute-start) | collective-permute-done | bytes 524320 | tf_op jit(solution)/shard_map/ppermute | solution.py:49
  98.6 1.9 collective-permute-start.2
  100.6 4.6 %collective-permute-start.3 = (bf16[64,2048]{1,0:T(8,128)(2,1)S(1)}, bf16[64,2048]{1,0:T(8,128)(2,1)}, u32[]{:S(2)}, u32[]{:S(2)}) collective-permute-start(bf16[64,2048]{1,0:T(8,128)(2,1)S(1)} %slice.17), channel_id=1, source_target_pairs={{0,3},{1,0},{2,1},{3,2},{4,7},{5,4},{6,5},{7,6},{8,11},{9,8},{10,9... | collective-permute-start | bytes 786440 | tf_op jit(solution)/shard_map/ppermute | solution.py:49
  105.2 1.0 copy.15.inner
  107.7 1.1 collective-permute-done.2.far_top
  109.7 7.2 %shard_map.127 = (bf16[512,512]{1,0:T(8,128)(2,1)}, bf16[512,256]{1,0:T(8,128)(2,1)}, f32[2,512,128]{2,1,0:T(8,128)}, f32[128,1,384]{2,1,0:T(1,128)}) custom-call(s32[4]{0:T(128)} %pad_add_fusion.place, bf16[128,2048]{1,0:T(8,128)(2,1)} %copy-done.2, bf16[128,2048]{1,0:T(8,128)(2,1)} %copy-done.5, bf16[128,2048]{1,0:T(8,128)(2,1)} %copy-done.6, ...), custom_call_target="tpu_custom_call" | custom-call | flops 1879048192 | bytes 10000000 | tf_op jit(solution)/shard_map/pallas_call | solution.py:36
  116.9 21.2 %all_to_all.21.received = f32[128,1,384]{2,1,0:T(1,128)} all-to-all(f32[128,1,384]{2,1,0:T(1,128)} %get-tuple-element.15), channel_id=1, replica_groups=mesh['sp_0'=8,'sp_1'=8,'sp_2'=2,'tp'=4] {'sp_0','sp_1','sp_2'}, dimensions={0} | all-to-all | bytes 393216 | tf_op jit(solution)/shard_map/all_to_all | solution.py:442
  138.1 2.3 %shard_map.129 = f32[128,1,256]{2,1,0:T(1,128)} custom-call(s32[1]{0:T(128)} %bitcast.2.place, f32[128,1,384]{2,1,0:T(1,128)} %all_to_all.21.received, f32[2,128,128]{2,1,0:T(8,128)} %bitcast.8), custom_call_target="tpu_custom_call" | custom-call | flops 40000000 | tf_op jit(solution)/shard_map/pallas_call | solution.py:36
  140.4 8.6 %all-to-all-start.2 = ((f32[128,1,256]{2,1,0:T(1,128)}), f32[128,1,256]{2,1,0:T(1,128)S(1)}, u32[]{:S(2)}, u32[]{:S(2)}) async-start(f32[128,1,256]{2,1,0:T(1,128)} %shard_map.129), calls=%async_computation.2 | async-start | bytes 262144 | tf_op jit(solution)/shard_map/all_to_all | solution.py:459
  149.6 4.6 %collective-permute-start.5 = (bf16[8,256]{1,0:T(8,128)(2,1)S(1)}, bf16[8,256]{1,0:T(8,128)(2,1)S(1)}, u32[]{:S(2)}, u32[]{:S(2)}) collective-permute-start(bf16[8,256]{1,0:T(8,128)(2,1)S(1)} %get-tuple-element.18), channel_id=1, source_target_pairs={{0,4},{4,8},{8,12},{12,16},{16,20},{20,24},{24,28},{28,32},{32,36}... | collective-permute-start | bytes 12296 | tf_op jit(solution)/shard_map/ppermute | solution.py:55
  154.2 2.1 %collective-permute-start.6 = (bf16[8,256]{1,0:T(8,128)(2,1)S(1)}, bf16[8,256]{1,0:T(8,128)(2,1)S(1)}, u32[]{:S(2)}, u32[]{:S(2)}) collective-permute-start(bf16[8,256]{1,0:T(8,128)(2,1)S(1)} %get-tuple-element.17), channel_id=1, source_target_pairs={{4,0},{8,4},{12,8},{16,12},{20,16},{24,20},{28,24},{32,28},{36,32}... | collective-permute-start | bytes 12296 | tf_op jit(solution)/shard_map/ppermute | solution.py:55
  156.3 3.0 %shard_map.128 = (f32[512,256]{1,0:T(8,128)}, bf16[512,256]{1,0:T(8,128)(2,1)}) custom-call(bf16[512,512]{1,0:T(8,128)(2,1)} %get-tuple-element.11.qkv, f32[2,512,128]{2,1,0:T(8,128)} %get-tuple-element.12.logs), custom_call_target="tpu_custom_call" | custom-call | flops 536870912 | bytes 3000000 | tf_op jit(solution)/shard_map/pallas_call | solution.py:36
  160.9 2.5 %shard_map.130.pooled = bf16[512,256]{1,0:T(8,128)(2,1)} custom-call(s32[4]{0:T(128)} %pad_add_fusion.place, bf16[512,256]{1,0:T(8,128)(2,1)} %get-tuple-element.16.pool_input, bf16[8,256]{1,0:T(8,128)(2,1)} %copy-done.8, bf16[8,256]{1,0:T(8,128)(2,1)} %copy-done.9, bf16[4,256,256]{2,1,0:T(8,128)(2,1)} %group_map.1), custom_call_target="tpu_custom_call" | custom-call | flops 67108864 | bytes 1000000 | tf_op jit(solution)/shard_map/pallas_call | solution.py:36
  164.1 2.6 %shard_map.131 = bf16[4,128,512]{2,1,0:T(8,128)(2,1)} custom-call(f32[512,256]{1,0:T(8,128)} %get-tuple-element.13.part, bf16[512,256]{1,0:T(8,128)(2,1)} %get-tuple-element.14.query, f32[128,1,256]{2,1,0:T(1,128)} %copy-done.3, bf16[512,256]{1,0:T(8,128)(2,1)} %shard_map.130.pooled), custom_call_target="tpu_custom_call" | custom-call | flops 100000000 | bytes 2000000 | tf_op jit(solution)/shard_map/pallas_call | solution.py:36
  166.7 14.4 %all_to_all.22.activations = bf16[4,128,512]{2,1,0:T(8,128)(2,1)} all-to-all(bf16[4,128,512]{2,1,0:T(8,128)(2,1)} %shard_map.131), channel_id=1, replica_groups=mesh['sp_0'=8,'sp_1'=8,'sp_2'=2,'tp'=4] {'tp'}, dimensions={0} | all-to-all | bytes 1048576 | tf_op jit(solution)/shard_map/all_to_all | solution.py:475
  181.1 8.5 %output_kernel.1 = bf16[128,2048]{1,0:T(8,128)(2,1)} custom-call(s32[4]{0:T(128)} %pad_add_fusion.place, bf16[4,128,512]{2,1,0:T(8,128)(2,1)} %all_to_all.22.activations, bf16[2048,2048]{1,0:T(8,128)(2,1)} %all-gather.2.cloned.1.call-done.weight), custom_call_target="tpu_custom_call" | custom-call | tf_op jit(solution)/shard_map/output_kernel/pallas_call | solution.py:352
  (43 shorter events, 7.9 us)
Async XLA Ops:
  6.5 174.5 %all-gather.2.cloned.1.call-start = ((), (), s32[]{:S(2)}) async-start(), calls=%async_computation.4 | async-start | bytes 8454144 | tf_op jit(solution)/shard_map/all_gather | solution.py:411
  7.3 10.6 %collective-permute-start.7 = (bf16[16,512]{1,0:T(8,128)(2,1)S(1)}, bf16[16,512]{1,0:T(8,128)(2,1)S(1)}, u32[]{:S(2)}, u32[]{:S(2)}) collective-permute-start(bf16[16,512]{1,0:T(8,128)(2,1)S(1)} %maximum_bitcast_fusion), channel_id=1, source_target_pairs={{0,1},{1,2},{2,3},{3,0},{4,5},{5,6},{6,7},{7,4},{8,9},{9,10},{10,1... | collective-permute-start | bytes 49160 | tf_op jit(solution)/shard_map/ppermute | solution.py:49
  10.4 7.4 %collective-permute-start.8 = (bf16[16,512]{1,0:T(8,128)(2,1)S(1)}, bf16[16,512]{1,0:T(8,128)(2,1)S(1)}, u32[]{:S(2)}, u32[]{:S(2)}) collective-permute-start(bf16[16,512]{1,0:T(8,128)(2,1)S(1)} %maximum_bitcast_fusion), channel_id=1, source_target_pairs={{0,2},{1,3},{2,0},{3,1},{4,6},{5,7},{6,4},{7,5},{8,10},{9,11},{10,... | collective-permute-start | bytes 49160 | tf_op jit(solution)/shard_map/ppermute | solution.py:49
  14.7 4.5 %collective-permute-start.9 = (bf16[16,512]{1,0:T(8,128)(2,1)S(1)}, bf16[16,512]{1,0:T(8,128)(2,1)S(1)}, u32[]{:S(2)}, u32[]{:S(2)}) collective-permute-start(bf16[16,512]{1,0:T(8,128)(2,1)S(1)} %maximum_bitcast_fusion), channel_id=1, source_target_pairs={{0,3},{1,0},{2,1},{3,2},{4,7},{5,4},{6,5},{7,6},{8,11},{9,8},{10,9... | collective-permute-start | bytes 49160 | tf_op jit(solution)/shard_map/ppermute | solution.py:49
  20.7 60.9 %copy-start = (bf16[128,2048]{1,0:T(8,128)(2,1)S(1)}, bf16[128,2048]{1,0:T(8,128)(2,1)}, u32[]{:S(2)}) copy-start(bf16[128,2048]{1,0:T(8,128)(2,1)} %param.13) | copy-start | bytes 1572868
  75.1 31.1 %copy-start.1 = (bf16[64,16,768]{2,1,0:T(8,128)(2,1)}, bf16[64,16,768]{2,1,0:T(8,128)(2,1)S(1)}, u32[]{:S(2)}) copy-start(bf16[64,16,768]{2,1,0:T(8,128)(2,1)S(1)} %all_to_all.20.weight_own) | copy-start | bytes 4718596
  75.1 30.1 %copy-start.4 = (bf16[2048,64]{0,1:T(8,128)(2,1)S(1)}, bf16[2048,64]{0,1:T(8,128)(2,1)}, u32[]{:S(2)}) copy-start(bf16[2048,64]{0,1:T(8,128)(2,1)} %param.18) | copy-start | bytes 786436
  75.1 34.6 %collective-permute-start.4 = (bf16[64,16,768]{2,1,0:T(8,128)(2,1)S(1)}, bf16[64,16,768]{2,1,0:T(8,128)(2,1)}, u32[]{:S(2)}, u32[]{:S(2)}) collective-permute-start(bf16[64,16,768]{2,1,0:T(8,128)(2,1)S(1)} %all_to_all.20.weight_own), channel_id=1, source_target_pairs={{0,4},{4,0},{1,5},{5,1},{2,6},{6,2},{3,7},{7,3},{8,12},{12,8},{9,1... | collective-permute-start | bytes 4718600 | tf_op jit(solution)/shard_map/ppermute | solution.py:49
  81.8 24.4 %copy-start.7 = (f32[2,512]{1,0:T(2,128)S(1)}, f32[2,512]{1,0:T(2,128)}, u32[]{:S(2)}) copy-start(f32[2,512]{1,0:T(2,128)} %param.21) | copy-start | bytes 12292
  82.0 27.7 %copy-start.2 = (bf16[128,2048]{1,0:T(8,128)(2,1)}, bf16[128,2048]{1,0:T(8,128)(2,1)S(1)}, u32[]{:S(2)}) copy-start(bf16[128,2048]{1,0:T(8,128)(2,1)S(1)} %fusion.1.own) | copy-start | bytes 1572868
  82.0 16.6 %collective-permute-start = (bf16[128,2048]{1,0:T(8,128)(2,1)S(1)}, bf16[128,2048]{1,0:T(8,128)(2,1)S(1)}, u32[]{:S(2)}, u32[]{:S(2)}) collective-permute-start(bf16[128,2048]{1,0:T(8,128)(2,1)S(1)} %fusion.1.own), channel_id=1, source_target_pairs={{0,1},{1,2},{2,3},{3,0},{4,5},{5,6},{6,7},{7,4},{8,9},{9,10},{10,1... | collective-permute-start | bytes 1572872 | tf_op jit(solution)/shard_map/ppermute | solution.py:49
  83.9 16.6 %collective-permute-start.1 = (bf16[128,2048]{1,0:T(8,128)(2,1)S(1)}, bf16[128,2048]{1,0:T(8,128)(2,1)S(1)}, u32[]{:S(2)}, u32[]{:S(2)}) collective-permute-start(bf16[128,2048]{1,0:T(8,128)(2,1)S(1)} %fusion.1.own), channel_id=1, source_target_pairs={{0,3},{1,0},{2,1},{3,2},{4,7},{5,4},{6,5},{7,6},{8,11},{9,8},{10,9... | collective-permute-start | bytes 1572872 | tf_op jit(solution)/shard_map/ppermute | solution.py:49
  98.6 11.1 %copy-start.5 = (bf16[128,2048]{1,0:T(8,128)(2,1)}, bf16[128,2048]{1,0:T(8,128)(2,1)S(1)}, u32[]{:S(2)}) copy-start(bf16[128,2048]{1,0:T(8,128)(2,1)S(1)} %collective-permute-done.before) | copy-start | bytes 1572868
  98.6 10.2 %collective-permute-start.2 = (bf16[64,2048]{1,0:T(8,128)(2,1)S(1)}, bf16[64,2048]{1,0:T(8,128)(2,1)}, u32[]{:S(2)}, u32[]{:S(2)}) collective-permute-start(bf16[64,2048]{1,0:T(8,128)(2,1)S(1)} %slice.16), channel_id=1, source_target_pairs={{0,1},{1,2},{2,3},{3,0},{4,5},{5,6},{6,7},{7,4},{8,9},{9,10},{10,1... | collective-permute-start | bytes 786440 | tf_op jit(solution)/shard_map/ppermute | solution.py:49
  100.6 4.6 %copy-start.6 = (bf16[128,2048]{1,0:T(8,128)(2,1)}, bf16[128,2048]{1,0:T(8,128)(2,1)S(1)}, u32[]{:S(2)}) copy-start(bf16[128,2048]{1,0:T(8,128)(2,1)S(1)} %collective-permute-done.1.after) | copy-start | bytes 1572868
  100.6 9.1 %collective-permute-start.3 = (bf16[64,2048]{1,0:T(8,128)(2,1)S(1)}, bf16[64,2048]{1,0:T(8,128)(2,1)}, u32[]{:S(2)}, u32[]{:S(2)}) collective-permute-start(bf16[64,2048]{1,0:T(8,128)(2,1)S(1)} %slice.17), channel_id=1, source_target_pairs={{0,3},{1,0},{2,1},{3,2},{4,7},{5,4},{6,5},{7,6},{8,11},{9,8},{10,9... | collective-permute-start | bytes 786440 | tf_op jit(solution)/shard_map/ppermute | solution.py:49
  140.4 23.1 %all-to-all-start.2 = ((f32[128,1,256]{2,1,0:T(1,128)}), f32[128,1,256]{2,1,0:T(1,128)S(1)}, u32[]{:S(2)}, u32[]{:S(2)}) async-start(f32[128,1,256]{2,1,0:T(1,128)} %shard_map.129), calls=%async_computation.2 | async-start | bytes 262144 | tf_op jit(solution)/shard_map/all_to_all | solution.py:459
  149.6 9.7 %collective-permute-start.5 = (bf16[8,256]{1,0:T(8,128)(2,1)S(1)}, bf16[8,256]{1,0:T(8,128)(2,1)S(1)}, u32[]{:S(2)}, u32[]{:S(2)}) collective-permute-start(bf16[8,256]{1,0:T(8,128)(2,1)S(1)} %get-tuple-element.18), channel_id=1, source_target_pairs={{0,4},{4,8},{8,12},{12,16},{16,20},{20,24},{24,28},{28,32},{32,36}... | collective-permute-start | bytes 12296 | tf_op jit(solution)/shard_map/ppermute | solution.py:55
  154.2 6.1 %collective-permute-start.6 = (bf16[8,256]{1,0:T(8,128)(2,1)S(1)}, bf16[8,256]{1,0:T(8,128)(2,1)S(1)}, u32[]{:S(2)}, u32[]{:S(2)}) collective-permute-start(bf16[8,256]{1,0:T(8,128)(2,1)S(1)} %get-tuple-element.17), channel_id=1, source_target_pairs={{4,0},{8,4},{12,8},{16,12},{20,16},{24,20},{28,24},{32,28},{36,32}... | collective-permute-start | bytes 12296 | tf_op jit(solution)/shard_map/ppermute | solution.py:55
  159.4 1.0 copy-start.8
  160.4 0.6 copy-start.9
  163.5 0.6 copy-start.3
Sparse Core Ops, SparseCore 0:
  20.0 116.6 all-gather.1

commit v3 on v2

--- a/solution.py
+++ b/solution.py
@@ -30,12 +30,14 @@
     return lax.dot_general(a, b, (dims, ((), ())), precision=precision, preferred_element_type=f32)
 
 
-def call(kernel, out_shapes, operands, scalars=1, scratch=(), flops=0, moved=0):
+def call(kernel, out_shapes, operands, scalars=1, far=0, scratch=(), flops=0, moved=0):
     smem = pl.BlockSpec(memory_space=pltpu.SMEM)
     vmem = pl.BlockSpec(memory_space=pltpu.VMEM)
+    anywhere = pl.BlockSpec(memory_space=pl.ANY)
+    near = len(operands) - scalars - far
     return pl.pallas_call(
         kernel,
-        in_specs=[smem if i < scalars else vmem for i in range(len(operands))],
+        in_specs=[smem] * scalars + [anywhere] * far + [vmem] * near,
         out_specs=jax.tree.map(lambda _: vmem, out_shapes),
         out_shape=out_shapes,
         scratch_shapes=list(scratch),
@@ -61,22 +63,6 @@
     return scaled.astype(bf16)
 
 
-def place_tokens(tp, pieces, whole_ref, first):
-    own, before, after, far_top, far_end = pieces
-    rows = own.shape[0]
-    half = rows // 2
-
-    def at(step):
-        return pl.multiple_of(first + lax.rem(tp + step, 4) * rows, 8)
-
-    whole_ref[pl.ds(at(0), rows), :] = own[...]
-    whole_ref[pl.ds(at(3), rows), :] = before[...]
-    whole_ref[pl.ds(at(1), rows), :] = after[...]
-    far = at(2)
-    whole_ref[pl.ds(far, half), :] = far_top[...]
-    whole_ref[pl.ds(pl.multiple_of(far + half, 8), half), :] = far_end[...]
-
-
 def split_dot(ones, values):
     high = values.astype(bf16)
     low = (values - high.astype(f32)).astype(bf16)
@@ -85,11 +71,7 @@
 
 def project_kernel(
     place,
-    own,
-    before,
-    after,
-    far_top,
-    far_end,
+    tokens_in,
     weight_own,
     weight_other,
     inner,
@@ -102,18 +84,19 @@
     packed_out,
     tokens_ref,
     weight_ref,
+    sems,
 ):
     tp, core = (place[0], place[1])
-    place_tokens(tp, (own, before, after, far_top, far_end), tokens_ref, 0)
-    weight_ref[:, pl.ds(core, 1)] = weight_own[...][:, None]
-    weight_ref[:, pl.ds(1 - core, 1)] = weight_other[...][:, None]
     rows, width = tokens_ref.shape
+    load_tokens = pltpu.make_async_copy(tokens_in, tokens_ref, sems.at[0])
+    load_own = pltpu.make_async_copy(weight_own, weight_ref.at[:, core], sems.at[1])
+    load_other = pltpu.make_async_copy(weight_other, weight_ref.at[:, 1 - core], sems.at[2])
+    load_tokens.start()
+    load_own.start()
+    load_other.start()
+    load_tokens.wait()
     tokens = tokens_ref[...]
     low_rank = matmul(tokens, inner[...]).astype(bf16)
-    projected = matmul(tokens, weight_ref[...].reshape(width, -1)).astype(bf16)
-    qkv = projected[:, : 4 * LANES]
-    qkv_out[...] = qkv
-    pool_out[...] = projected[:, 4 * LANES :]
     here = pl.ds(pl.multiple_of(tp * LANES, LANES), LANES)
     blank = jnp.zeros((RANK, LANES), bf16)
     outer_both = jnp.concatenate(
@@ -147,6 +130,12 @@
         logs_out[1, n * size : (n + 1) * size, :] = found
         carry = found[0:1, :]
     total_bwd = carry
+    load_own.wait()
+    load_other.wait()
+    projected = matmul(tokens_ref[...], weight_ref[...].reshape(width, -1)).astype(bf16)
+    qkv = projected[:, : 4 * LANES]
+    qkv_out[...] = qkv
+    pool_out[...] = projected[:, 4 * LANES :]
     keys = qkv[:, LANES : 2 * LANES].astype(f32)
     weighted = jnp.concatenate(
         [
@@ -331,18 +320,22 @@
             start += piece.shape[1]
 
 
-def output_kernel(place, activations, weight, out):
+def output_kernel(place, activations, weight, out, turned):
     tp = place[0]
     groups, _, width = activations.shape
+
+    @pl.when(pl.program_id(0) == 0)
+    def _():
+        for s in range(groups):
+            source = lax.rem(tp + groups - s, groups)
+            turned[s] = activations[source].astype(f32).T.astype(bf16)
+
     total = None
     for s in range(groups):
-        source = lax.rem(tp + groups - s, groups)
-        partial = matmul(
-            activations[source], weight[:, s * width : (s + 1) * width], ((1,), (1,))
-        )
+        partial = matmul(weight[:, s * width : (s + 1) * width], turned[s])
         partial = partial.astype(bf16).astype(f32)
         total = partial if total is None else total + partial
-    out[...] = total.astype(bf16)
+    out[...] = total.T.astype(bf16)
 
 
 def output_projection(place, activations, weights):
@@ -359,6 +352,7 @@
         ],
         out_specs=pl.BlockSpec((rows, tile), lambda n: (0, n)),
         out_shape=jax.ShapeDtypeStruct((rows, model), bf16),
+        scratch_shapes=[pltpu.VMEM((groups, width, rows), bf16)],
         interpret=interpreted,
         name="output_kernel",
     )(place, activations, weights)
@@ -400,14 +394,8 @@
     weight_own = lax.all_to_all(copies, CHIPS, 0, 0, tiled=True)
     local_out = jnp.concatenate([pooling_output_weight, attention_output_weight], axis=0).T
     outs = [local_out] + [shifted(local_out, "tp", k) for k in range(1, groups)]
-    normed = normalize(tokens)
-    half = normed.shape[0] // 2
-    before = shifted(normed, "tp", 1)
-    after = shifted(normed, "tp", -1)
-    top, end = (before[:half], after[half:])
-    far_top = shifted(top, "tp", 1)
-    far_end = shifted(end, "tp", -1)
     weight_other = shifted(weight_own, "sp_2", 1)
+    all_tokens = lax.all_gather(normalize(tokens), "tp", axis=0, tiled=True)
     whole_out = lax.all_gather(jnp.concatenate(outs, axis=1), SP, axis=0, tiled=True)
 
     qkv, pool_input, logs, packed = call(
@@ -420,11 +408,7 @@
         ),
         (
             place,
-            normed,
-            before,
-            after,
-            far_top,
-            far_end,
+            all_tokens,
             weight_own,
             weight_other,
             decay_inner_weight,
@@ -432,9 +416,11 @@
             channel_decay_bias,
             spike_log_decay.T,
         ),
+        far=3,
         scratch=(
             pltpu.VMEM((rows, model), bf16),
             pltpu.VMEM((chips, 2, model // (2 * chips), 6 * LANES), bf16),
+            pltpu.SemaphoreType.DMA((3,)),
         ),
         flops=2 * rows * model * 7 * LANES,
         moved=10_000_000,

time: 197 us -> 173 us (0.88)
  the two profiles are of different devices: /device:TPU:25 before, /device:TPU:1 now
where the time goes in v3:
time: 173 us; the launch traced here: 172 us
  blocking collectives  87.1 us (50%)
  starting transfers between devices  30.5 us (18%)
  Pallas kernels  27.1 us (16%)
  between operations  13.6 us (8%)
  local copies, waits for them, and re-layouts  5.45 us (3%)
  other arithmetic  4.48 us (3%)
  waiting for transfers between devices  3.6 us (2%)
    all_to_all x1, blocking collectives, shards(): weight_own = lax.all_to_all(copies, CHIPS, 0, 0, tiled=True)  51.9 us
    all_to_all x1, blocking collectives, shards(): received = lax.all_to_all(packed, SP, 0, 0, tiled=True)  21.8 us
    ppermute x4, starting transfers between devices, shifted(): lax.ppermute(value, axis, [(i, (i + step) % devices) for i in range(devic...  19.3 us
    pallas_call x5, Pallas kernels, call(): pl.pallas_call(kernel, in_specs=[smem] * scalars + [anywhere] * far + [vm...  18.3 us
    all_to_all x1, blocking collectives, shards(): gathered = lax.all_to_all(activations, 'tp', 0, 0, tiled=True)  13.4 us
    pallas_call x1, Pallas kernels, output_projection(): pl.pallas_call(output_kernel, grid=(model // tile,), in_specs=[pl.BlockSp...  8.85 us
    all_to_all x1, starting transfers between devices, shards(): entering = lax.all_to_all(states, SP, 0, 0, tiled=True)  5.63 us
    ppermute x2, starting transfers between devices, neighbours(): return lax.ppermute(value, axes, pairs)  5.45 us
  transfers between devices with their start and end apart: 9, of which 4 were waited for; matrix products, arithmetic and copies ran while one was open for 2% of the time, Pallas kernels for 11%

profile of v3, /device:TPU:1, one launch (start us, length us, event | category | flops | bytes accessed | tf_op | source)
XLA Modules:
  0.0 171.8 jit_solution(12029379060118624783)
XLA Ops:
  6.6 1.3 fusion
  7.9 2.0 %fusion.1 = bf16[128,2048]{1,0:T(8,128)(2,1)} fusion(bf16[128,2048]{1,0:T(8,128)(2,1)} %param.13, f32[128]{0:T(128)S(1)} %add_rsqrt_fusion), kind=kLoop, calls=%fused_computation.3 | loop fusion | flops 786432 | bytes 1049088 | tf_op jit(solution)/shard_map/convert_element_type | solution.py:63
  10.0 3.9 %collective-permute-start.3 = (bf16[16,512]{1,0:T(8,128)(2,1)S(1)}, bf16[16,512]{1,0:T(8,128)(2,1)S(1)}, u32[]{:S(2)}, u32[]{:S(2)}) collective-permute-start(bf16[16,512]{1,0:T(8,128)(2,1)S(1)} %maximum_bitcast_fusion), channel_id=1, source_target_pairs={{0,1},{1,2},{2,3},{3,0},{4,5},{5,6},{6,7},{7,4},{8,9},{9,10},{10,1... | collective-permute-start | bytes 49160 | tf_op jit(solution)/shard_map/ppermute | solution.py:51
  13.9 4.4 %collective-permute-start.4 = (bf16[16,512]{1,0:T(8,128)(2,1)S(1)}, bf16[16,512]{1,0:T(8,128)(2,1)S(1)}, u32[]{:S(2)}, u32[]{:S(2)}) collective-permute-start(bf16[16,512]{1,0:T(8,128)(2,1)S(1)} %maximum_bitcast_fusion), channel_id=1, source_target_pairs={{0,2},{1,3},{2,0},{3,1},{4,6},{5,7},{6,4},{7,5},{8,10},{9,11},{10,... | collective-permute-start | bytes 49160 | tf_op jit(solution)/shard_map/ppermute | solution.py:51
  18.3 3.1 %collective-permute-start.5 = (bf16[16,512]{1,0:T(8,128)(2,1)S(1)}, bf16[16,512]{1,0:T(8,128)(2,1)S(1)}, u32[]{:S(2)}, u32[]{:S(2)}) collective-permute-start(bf16[16,512]{1,0:T(8,128)(2,1)S(1)} %maximum_bitcast_fusion), channel_id=1, source_target_pairs={{0,3},{1,0},{2,1},{3,2},{4,7},{5,4},{6,5},{7,6},{8,11},{9,8},{10,9... | collective-permute-start | bytes 49160 | tf_op jit(solution)/shard_map/ppermute | solution.py:51
  21.4 1.7 collective-permute-done.5
  23.9 51.9 %all_to_all.20.weight_own = bf16[64,16,768]{2,1,0:T(8,128)(2,1)S(1)} all-to-all(bf16[64,16,768]{2,1,0:T(8,128)(2,1)S(1)} %broadcast_in_dim.4), channel_id=1, replica_groups=mesh['sp_0'=8,'sp_1'=8,'sp_2'=2,'tp'=4] {'sp_0','sp_1'}, dimensions={0} | all-to-all | bytes 3145728 | tf_op jit(solution)/shard_map/all_to_all | solution.py:394
  75.8 7.9 %collective-permute-start = (bf16[64,16,768]{2,1,0:T(8,128)(2,1)S(1)}, bf16[64,16,768]{2,1,0:T(8,128)(2,1)S(1)}, u32[]{:S(2)}, u32[]{:S(2)}) collective-permute-start(bf16[64,16,768]{2,1,0:T(8,128)(2,1)S(1)} %all_to_all.20.weight_own), channel_id=1, source_target_pairs={{0,4},{4,0},{1,5},{5,1},{2,6},{6,2},{3,7},{7,3},{8,12},{12,8},{9,1... | collective-permute-start | bytes 4718600 | tf_op jit(solution)/shard_map/ppermute | solution.py:51
  83.8 1.0 copy.15.inner
  84.8 0.9 copy.14
  86.8 1.2 copy-done.12
  88.0 7.8 %shard_map.127 = (bf16[512,512]{1,0:T(8,128)(2,1)}, bf16[512,256]{1,0:T(8,128)(2,1)}, f32[2,512,128]{2,1,0:T(8,128)}, f32[128,1,384]{2,1,0:T(1,128)}) custom-call(s32[4]{0:T(128)} %pad_add_fusion.place, bf16[512,2048]{1,0:T(8,128)(2,1)} %all-gather.3.cloned.1.call-done.tokens_in, bf16[64,16,768]{2,1,0:T(8,128)(2,1)} %copy-done, ...), custom_call_target="tpu_custom_call" | custom-call | flops 1879048192 | bytes 10000000 | tf_op jit(solution)/shard_map/pallas_call | solution.py:38
  95.8 21.8 %all_to_all.21.received = f32[128,1,384]{2,1,0:T(1,128)} all-to-all(f32[128,1,384]{2,1,0:T(1,128)} %get-tuple-element.15), channel_id=1, replica_groups=mesh['sp_0'=8,'sp_1'=8,'sp_2'=2,'tp'=4] {'sp_0','sp_1','sp_2'}, dimensions={0} | all-to-all | bytes 393216 | tf_op jit(solution)/shard_map/all_to_all | solution.py:428
  117.6 2.3 %shard_map.129 = f32[128,1,256]{2,1,0:T(1,128)} custom-call(s32[1]{0:T(128)} %bitcast.2.place, f32[128,1,384]{2,1,0:T(1,128)} %all_to_all.21.received, f32[2,128,128]{2,1,0:T(8,128)} %bitcast.8), custom_call_target="tpu_custom_call" | custom-call | flops 40000000 | tf_op jit(solution)/shard_map/pallas_call | solution.py:38
  119.8 5.6 %all-to-all-start.2 = ((f32[128,1,256]{2,1,0:T(1,128)}), f32[128,1,256]{2,1,0:T(1,128)S(1)}, u32[]{:S(2)}, u32[]{:S(2)}) async-start(f32[128,1,256]{2,1,0:T(1,128)} %shard_map.129), calls=%async_computation.2 | async-start | bytes 262144 | tf_op jit(solution)/shard_map/all_to_all | solution.py:445
  125.5 0.7 fusion.2
  126.2 3.5 %collective-permute-start.1 = (bf16[8,256]{1,0:T(8,128)(2,1)S(1)}, bf16[8,256]{1,0:T(8,128)(2,1)S(1)}, u32[]{:S(2)}, u32[]{:S(2)}) collective-permute-start(bf16[8,256]{1,0:T(8,128)(2,1)S(1)} %get-tuple-element.18), channel_id=1, source_target_pairs={{0,4},{4,8},{8,12},{12,16},{16,20},{20,24},{24,28},{28,32},{32,36}... | collective-permute-start | bytes 12296 | tf_op jit(solution)/shard_map/ppermute | solution.py:57
  129.7 1.9 %collective-permute-start.2 = (bf16[8,256]{1,0:T(8,128)(2,1)S(1)}, bf16[8,256]{1,0:T(8,128)(2,1)S(1)}, u32[]{:S(2)}, u32[]{:S(2)}) collective-permute-start(bf16[8,256]{1,0:T(8,128)(2,1)S(1)} %get-tuple-element.17), channel_id=1, source_target_pairs={{4,0},{8,4},{12,8},{16,12},{20,16},{24,20},{28,24},{32,28},{36,32}... | collective-permute-start | bytes 12296 | tf_op jit(solution)/shard_map/ppermute | solution.py:57
  131.6 3.1 %shard_map.128 = (f32[512,256]{1,0:T(8,128)}, bf16[512,256]{1,0:T(8,128)(2,1)}) custom-call(bf16[512,512]{1,0:T(8,128)(2,1)} %get-tuple-element.11.qkv, f32[2,512,128]{2,1,0:T(8,128)} %get-tuple-element.12.logs), custom_call_target="tpu_custom_call" | custom-call | flops 536870912 | bytes 3000000 | tf_op jit(solution)/shard_map/pallas_call | solution.py:38
  135.9 2.5 %shard_map.130.pooled = bf16[512,256]{1,0:T(8,128)(2,1)} custom-call(s32[4]{0:T(128)} %pad_add_fusion.place, bf16[512,256]{1,0:T(8,128)(2,1)} %get-tuple-element.16.pool_input, bf16[8,256]{1,0:T(8,128)(2,1)} %copy-done.8, bf16[8,256]{1,0:T(8,128)(2,1)} %copy-done.9, bf16[4,256,256]{2,1,0:T(8,128)(2,1)} %group_map.1), custom_call_target="tpu_custom_call" | custom-call | flops 67108864 | bytes 1000000 | tf_op jit(solution)/shard_map/pallas_call | solution.py:38
  138.5 1.1 all-to-all-done.2.entering
  140.2 2.5 %shard_map.131 = bf16[4,128,512]{2,1,0:T(8,128)(2,1)} custom-call(f32[512,256]{1,0:T(8,128)} %get-tuple-element.13.part, bf16[512,256]{1,0:T(8,128)(2,1)} %get-tuple-element.14.query, f32[128,1,256]{2,1,0:T(1,128)} %copy-done.1, bf16[512,256]{1,0:T(8,128)(2,1)} %shard_map.130.pooled), custom_call_target="tpu_custom_call" | custom-call | flops 100000000 | bytes 2000000 | tf_op jit(solution)/shard_map/pallas_call | solution.py:38
  142.7 13.4 %all_to_all.22.activations = bf16[4,128,512]{2,1,0:T(8,128)(2,1)} all-to-all(bf16[4,128,512]{2,1,0:T(8,128)(2,1)} %shard_map.131), channel_id=1, replica_groups=mesh['sp_0'=8,'sp_1'=8,'sp_2'=2,'tp'=4] {'tp'}, dimensions={0} | all-to-all | bytes 1048576 | tf_op jit(solution)/shard_map/all_to_all | solution.py:461
  156.1 8.9 %output_kernel.1 = bf16[128,2048]{1,0:T(8,128)(2,1)} custom-call(s32[4]{0:T(128)} %pad_add_fusion.place, bf16[4,128,512]{2,1,0:T(8,128)(2,1)} %all_to_all.22.activations, bf16[2048,2048]{1,0:T(8,128)(2,1)} %all-gather.5.cloned.1.call-done.weight), custom_call_target="tpu_custom_call" | custom-call | tf_op jit(solution)/shard_map/output_kernel/pallas_call | solution.py:345
  (42 shorter events, 3.8 us)
Async XLA Ops:
  6.5 3.4 %copy-start.4 = (bf16[256,16]{0,1:T(8,128)(2,1)S(1)}, bf16[256,16]{0,1:T(8,128)(2,1)}, u32[]{:S(2)}) copy-start(bf16[256,16]{0,1:T(8,128)(2,1)} %param.24) | copy-start | bytes 24580
  6.5 3.4 %copy-start.3 = (bf16[256,16]{0,1:T(8,128)(2,1)S(1)}, bf16[256,16]{0,1:T(8,128)(2,1)}, u32[]{:S(2)}) copy-start(bf16[256,16]{0,1:T(8,128)(2,1)} %param.25) | copy-start | bytes 24580
  6.5 17.2 %copy-start.5 = (bf16[16,256]{1,0:T(8,128)(2,1)S(1)}, bf16[16,256]{1,0:T(8,128)(2,1)}, u32[]{:S(2)}) copy-start(bf16[16,256]{1,0:T(8,128)(2,1)} %param.14) | copy-start | bytes 24580
  6.5 17.2 %copy-start.11 = (bf16[16,128]{1,0:T(8,128)(2,1)S(1)}, bf16[16,128]{1,0:T(8,128)(2,1)}, u32[]{:S(2)}) copy-start(bf16[16,128]{1,0:T(8,128)(2,1)} %param.15) | copy-start | bytes 12292
  6.5 17.2 %copy-start.10 = (bf16[16,128]{1,0:T(8,128)(2,1)S(1)}, bf16[16,128]{1,0:T(8,128)(2,1)}, u32[]{:S(2)}) copy-start(bf16[16,128]{1,0:T(8,128)(2,1)} %param.16) | copy-start | bytes 12292
  6.5 17.2 %copy-start.6 = (bf16[16,256]{1,0:T(8,128)(2,1)S(1)}, bf16[16,256]{1,0:T(8,128)(2,1)}, u32[]{:S(2)}) copy-start(bf16[16,256]{1,0:T(8,128)(2,1)} %param.17) | copy-start | bytes 24580
  6.6 79.7 %all-gather.3.cloned.1.call-start = ((), (), s32[]{:S(2)}) async-start(), calls=%async_computation.4 | async-start | bytes 2621440 | tf_op jit(solution)/shard_map/all_gather | solution.py:398
  9.9 146.2 %all-gather.5.cloned.1.call-start = ((), (), s32[]{:S(2)}) async-start(), calls=%async_computation.5 | async-start | bytes 8454144 | tf_op jit(solution)/shard_map/all_gather | solution.py:399
  10.0 11.4 %collective-permute-start.3 = (bf16[16,512]{1,0:T(8,128)(2,1)S(1)}, bf16[16,512]{1,0:T(8,128)(2,1)S(1)}, u32[]{:S(2)}, u32[]{:S(2)}) collective-permute-start(bf16[16,512]{1,0:T(8,128)(2,1)S(1)} %maximum_bitcast_fusion), channel_id=1, source_target_pairs={{0,1},{1,2},{2,3},{3,0},{4,5},{5,6},{6,7},{7,4},{8,9},{9,10},{10,1... | collective-permute-start | bytes 49160 | tf_op jit(solution)/shard_map/ppermute | solution.py:51
  13.9 7.4 %collective-permute-start.4 = (bf16[16,512]{1,0:T(8,128)(2,1)S(1)}, bf16[16,512]{1,0:T(8,128)(2,1)S(1)}, u32[]{:S(2)}, u32[]{:S(2)}) collective-permute-start(bf16[16,512]{1,0:T(8,128)(2,1)S(1)} %maximum_bitcast_fusion), channel_id=1, source_target_pairs={{0,2},{1,3},{2,0},{3,1},{4,6},{5,7},{6,4},{7,5},{8,10},{9,11},{10,... | collective-permute-start | bytes 49160 | tf_op jit(solution)/shard_map/ppermute | solution.py:51
  18.3 4.8 %collective-permute-start.5 = (bf16[16,512]{1,0:T(8,128)(2,1)S(1)}, bf16[16,512]{1,0:T(8,128)(2,1)S(1)}, u32[]{:S(2)}, u32[]{:S(2)}) collective-permute-start(bf16[16,512]{1,0:T(8,128)(2,1)S(1)} %maximum_bitcast_fusion), channel_id=1, source_target_pairs={{0,3},{1,0},{2,1},{3,2},{4,7},{5,4},{6,5},{7,6},{8,11},{9,8},{10,9... | collective-permute-start | bytes 49160 | tf_op jit(solution)/shard_map/ppermute | solution.py:51
  23.9 59.9 %copy-start.2 = (bf16[2048,64]{0,1:T(8,128)(2,1)S(1)}, bf16[2048,64]{0,1:T(8,128)(2,1)}, u32[]{:S(2)}) copy-start(bf16[2048,64]{0,1:T(8,128)(2,1)} %param.18) | copy-start | bytes 786436
  23.9 60.9 %copy-start.7 = (f32[2,512]{1,0:T(2,128)S(1)}, f32[2,512]{1,0:T(2,128)}, u32[]{:S(2)}) copy-start(f32[2,512]{1,0:T(2,128)} %param.21) | copy-start | bytes 12292
  75.8 11.0 %copy-start = (bf16[64,16,768]{2,1,0:T(8,128)(2,1)}, bf16[64,16,768]{2,1,0:T(8,128)(2,1)S(1)}, u32[]{:S(2)}) copy-start(bf16[64,16,768]{2,1,0:T(8,128)(2,1)S(1)} %all_to_all.20.weight_own) | copy-start | bytes 4718596
  75.8 11.0 %collective-permute-start = (bf16[64,16,768]{2,1,0:T(8,128)(2,1)S(1)}, bf16[64,16,768]{2,1,0:T(8,128)(2,1)S(1)}, u32[]{:S(2)}, u32[]{:S(2)}) collective-permute-start(bf16[64,16,768]{2,1,0:T(8,128)(2,1)S(1)} %all_to_all.20.weight_own), channel_id=1, source_target_pairs={{0,4},{4,0},{1,5},{5,1},{2,6},{6,2},{3,7},{7,3},{8,12},{12,8},{9,1... | collective-permute-start | bytes 4718600 | tf_op jit(solution)/shard_map/ppermute | solution.py:51
  86.8 1.2 copy-start.12
  119.8 19.7 %all-to-all-start.2 = ((f32[128,1,256]{2,1,0:T(1,128)}), f32[128,1,256]{2,1,0:T(1,128)S(1)}, u32[]{:S(2)}, u32[]{:S(2)}) async-start(f32[128,1,256]{2,1,0:T(1,128)} %shard_map.129), calls=%async_computation.2 | async-start | bytes 262144 | tf_op jit(solution)/shard_map/all_to_all | solution.py:445
  126.2 8.6 %collective-permute-start.1 = (bf16[8,256]{1,0:T(8,128)(2,1)S(1)}, bf16[8,256]{1,0:T(8,128)(2,1)S(1)}, u32[]{:S(2)}, u32[]{:S(2)}) collective-permute-start(bf16[8,256]{1,0:T(8,128)(2,1)S(1)} %get-tuple-element.18), channel_id=1, source_target_pairs={{0,4},{4,8},{8,12},{12,16},{16,20},{20,24},{24,28},{28,32},{32,36}... | collective-permute-start | bytes 12296 | tf_op jit(solution)/shard_map/ppermute | solution.py:57
  129.7 5.4 %collective-permute-start.2 = (bf16[8,256]{1,0:T(8,128)(2,1)S(1)}, bf16[8,256]{1,0:T(8,128)(2,1)S(1)}, u32[]{:S(2)}, u32[]{:S(2)}) collective-permute-start(bf16[8,256]{1,0:T(8,128)(2,1)S(1)} %get-tuple-element.17), channel_id=1, source_target_pairs={{4,0},{8,4},{12,8},{16,12},{20,16},{24,20},{28,24},{32,28},{36,32}... | collective-permute-start | bytes 12296 | tf_op jit(solution)/shard_map/ppermute | solution.py:57
  134.8 0.6 copy-start.8
  135.4 0.6 copy-start.9
  139.6 0.6 copy-start.1
Sparse Core Ops, SparseCore 0:
  10.0 41.3 all-gather.2
  54.6 92.4 all-gather.4

commit v4 on v2

--- a/solution.py
+++ b/solution.py
@@ -30,12 +30,14 @@
     return lax.dot_general(a, b, (dims, ((), ())), precision=precision, preferred_element_type=f32)
 
 
-def call(kernel, out_shapes, operands, scalars=1, scratch=(), flops=0, moved=0):
+def call(kernel, out_shapes, operands, scalars=1, far=0, scratch=(), flops=0, moved=0):
     smem = pl.BlockSpec(memory_space=pltpu.SMEM)
     vmem = pl.BlockSpec(memory_space=pltpu.VMEM)
+    anywhere = pl.BlockSpec(memory_space=pl.ANY)
+    near = len(operands) - scalars - far
     return pl.pallas_call(
         kernel,
-        in_specs=[smem if i < scalars else vmem for i in range(len(operands))],
+        in_specs=[smem] * scalars + [anywhere] * far + [vmem] * near,
         out_specs=jax.tree.map(lambda _: vmem, out_shapes),
         out_shape=out_shapes,
         scratch_shapes=list(scratch),
@@ -83,37 +85,24 @@
     return matmul(ones, high) + matmul(ones, low)
 
 
-def project_kernel(
+def decay_kernel(
     place,
     own,
     before,
     after,
     far_top,
     far_end,
-    weight_own,
-    weight_other,
     inner,
     outer,
     bias,
     spike,
-    qkv_out,
-    pool_out,
+    tokens_out,
     logs_out,
-    packed_out,
-    tokens_ref,
-    weight_ref,
 ):
-    tp, core = (place[0], place[1])
-    place_tokens(tp, (own, before, after, far_top, far_end), tokens_ref, 0)
-    weight_ref[:, pl.ds(core, 1)] = weight_own[...][:, None]
-    weight_ref[:, pl.ds(1 - core, 1)] = weight_other[...][:, None]
-    rows, width = tokens_ref.shape
-    tokens = tokens_ref[...]
-    low_rank = matmul(tokens, inner[...]).astype(bf16)
-    projected = matmul(tokens, weight_ref[...].reshape(width, -1)).astype(bf16)
-    qkv = projected[:, : 4 * LANES]
-    qkv_out[...] = qkv
-    pool_out[...] = projected[:, 4 * LANES :]
+    tp = place[0]
+    place_tokens(tp, (own, before, after, far_top, far_end), tokens_out, 0)
+    rows = tokens_out.shape[0]
+    low_rank = matmul(tokens_out[...], inner[...]).astype(bf16)
     here = pl.ds(pl.multiple_of(tp * LANES, LANES), LANES)
     blank = jnp.zeros((RANK, LANES), bf16)
     outer_both = jnp.concatenate(
@@ -140,18 +129,44 @@
         found = split_dot(upto, decay[n * size : (n + 1) * size, :LANES]) + carry
         logs_out[0, n * size : (n + 1) * size, :] = found
         carry = found[size - 1 : size, :]
-    total_fwd = carry
     carry = jnp.zeros((1, LANES), f32)
     for n in reversed(range(tiles)):
         found = split_dot(onward, decay[n * size : (n + 1) * size, LANES:]) + carry
         logs_out[1, n * size : (n + 1) * size, :] = found
         carry = found[0:1, :]
-    total_bwd = carry
+
+
+def project_kernel(
+    place,
+    weight_own,
+    weight_other,
+    tokens,
+    logs,
+    qkv_out,
+    pool_out,
+    packed_out,
+    weight_ref,
+    sems,
+):
+    core = place[1]
+    load_own = pltpu.make_async_copy(weight_own, weight_ref.at[:, core], sems.at[0])
+    load_other = pltpu.make_async_copy(weight_other, weight_ref.at[:, 1 - core], sems.at[1])
+    load_own.start()
+    load_other.start()
+    rows, width = tokens.shape
+    total_fwd = logs[0, rows - 1 : rows, :]
+    total_bwd = logs[1, 0:1, :]
+    load_own.wait()
+    load_other.wait()
+    projected = matmul(tokens[...], weight_ref[...].reshape(width, -1)).astype(bf16)
+    qkv = projected[:, : 4 * LANES]
+    qkv_out[...] = qkv
+    pool_out[...] = projected[:, 4 * LANES :]
     keys = qkv[:, LANES : 2 * LANES].astype(f32)
     weighted = jnp.concatenate(
         [
-            (keys * jnp.exp(total_fwd - logs_out[0])).astype(bf16),
-            (keys * jnp.exp(total_bwd - logs_out[1])).astype(bf16),
+            (keys * jnp.exp(total_fwd - logs[0])).astype(bf16),
+            (keys * jnp.exp(total_bwd - logs[1])).astype(bf16),
         ],
         axis=1,
     )
@@ -331,34 +346,42 @@
             start += piece.shape[1]
 
 
-def output_kernel(place, activations, weight, out):
-    tp = place[0]
-    groups, _, width = activations.shape
-    total = None
-    for s in range(groups):
-        source = lax.rem(tp + groups - s, groups)
-        partial = matmul(
-            activations[source], weight[:, s * width : (s + 1) * width], ((1,), (1,))
-        )
-        partial = partial.astype(bf16).astype(f32)
-        total = partial if total is None else total + partial
-    out[...] = total.astype(bf16)
+def output_kernel(place, activations, weight, out, total):
+    groups = activations.shape[0]
+    step, part = (pl.program_id(0), pl.program_id(1))
+    tile = weight.shape[0]
+    here = pl.ds(pl.multiple_of(part * tile, tile), tile)
+    source = lax.rem(place[0] + groups - step, groups)
+    partial = matmul(weight[...], activations[source], ((1,), (1,))).astype(bf16).astype(f32)
+
+    @pl.when(step == 0)
+    def _():
+        total[here, :] = partial
+
+    @pl.when(step > 0)
+    def _():
+        total[here, :] += partial
+
+    @pl.when(step == groups - 1)
+    def _():
+        out[:, here] = total[here, :].T.astype(bf16)
 
 
 def output_projection(place, activations, weights):
     groups, rows, width = activations.shape
     model = weights.shape[0]
-    tile = 256
+    parts = 2
     return pl.pallas_call(
         output_kernel,
-        grid=(model // tile,),
+        grid=(groups, parts),
         in_specs=[
             pl.BlockSpec(memory_space=pltpu.SMEM),
-            pl.BlockSpec((groups, rows, width), lambda n: (0, 0, 0)),
-            pl.BlockSpec((tile, groups * width), lambda n: (n, 0)),
+            pl.BlockSpec((groups, rows, width), lambda s, n: (0, 0, 0)),
+            pl.BlockSpec((model // parts, width), lambda s, n: (n, s)),
         ],
-        out_specs=pl.BlockSpec((rows, tile), lambda n: (0, n)),
+        out_specs=pl.BlockSpec((rows, model), lambda s, n: (0, 0)),
         out_shape=jax.ShapeDtypeStruct((rows, model), bf16),
+        scratch_shapes=[pltpu.VMEM((model, rows), f32)],
         interpret=interpreted,
         name="output_kernel",
     )(place, activations, weights)
@@ -410,14 +433,9 @@
     weight_other = shifted(weight_own, "sp_2", 1)
     whole_out = lax.all_gather(jnp.concatenate(outs, axis=1), SP, axis=0, tiled=True)
 
-    qkv, pool_input, logs, packed = call(
-        project_kernel,
-        (
-            shape_of(rows, 4 * LANES),
-            shape_of(rows, 2 * LANES),
-            shape_of(2, rows, LANES, kind=f32),
-            shape_of(LANES, 1, 3 * LANES, kind=f32),
-        ),
+    all_tokens, logs = call(
+        decay_kernel,
+        (shape_of(rows, model), shape_of(2, rows, LANES, kind=f32)),
         (
             place,
             normed,
@@ -425,19 +443,29 @@
             after,
             far_top,
             far_end,
-            weight_own,
-            weight_other,
             decay_inner_weight,
             decay_outer_weight,
             channel_decay_bias,
             spike_log_decay.T,
         ),
+        flops=2 * rows * model * 4 * LANES,
+        moved=5_000_000,
+    )
+    qkv, pool_input, packed = call(
+        project_kernel,
+        (
+            shape_of(rows, 4 * LANES),
+            shape_of(rows, 2 * LANES),
+            shape_of(LANES, 1, 3 * LANES, kind=f32),
+        ),
+        (place, weight_own, weight_other, all_tokens, logs),
+        far=2,
         scratch=(
-            pltpu.VMEM((rows, model), bf16),
             pltpu.VMEM((chips, 2, model // (2 * chips), 6 * LANES), bf16),
+            pltpu.SemaphoreType.DMA((2,)),
         ),
         flops=2 * rows * model * 7 * LANES,
-        moved=10_000_000,
+        moved=8_000_000,
     )
     received = lax.all_to_all(packed, SP, 0, 0, tiled=True)
     rim_before = neighbours(pool_input[rows - rim_width :], SP, 1)

time: 197 us -> 202 us (1.025)
  blocking collectives: 89.9 us -> 35.5 us
  waiting for transfers between devices: 14.4 us -> 52.6 us
  starting transfers between devices: 45.3 us -> 61.1 us
  Pallas kernels: 26.2 us -> 30.1 us
    all_to_all x1 -> x0, blocking collectives: 54.4 us -> none  [shards(): weight_own = lax.all_to_all(copies, CHIPS, 0, 0, tiled=True)]
    all_to_all x0 -> x1, waiting for transfers between devices: none -> 38.3 us  [shards(): weight_own = lax.all_to_all(copies, CHIPS, 0, 0, tiled=True)]
    all_to_all x0 -> x1, starting transfers between devices: none -> 15.9 us  [shards(): weight_own = lax.all_to_all(copies, CHIPS, 0, 0, tiled=True)]
    pallas_call x6 -> x7, Pallas kernels: 26.2 us -> 30.1 us  [the longest x6 21.3 us: call(): pl.pallas_call(kernel, in_specs=[smem] * scalars + [anywhere] * far + [vm...]
  transfers between devices with their start and end apart: 12 -> 13, of which waited for: 5 -> 6; matrix products, arithmetic and copies ran while one was open for 2% -> 3% of each run, Pallas kernels for 9% -> 11%
where the time goes in v4:
time: 202 us; the launch traced here: 201 us
  starting transfers between devices  61.1 us (30%)
  waiting for transfers between devices  52.6 us (26%)
  blocking collectives  35.5 us (18%)
  Pallas kernels  30.1 us (15%)
  between operations  13.6 us (7%)
  local copies, waits for them, and re-layouts  5.18 us (3%)
  other arithmetic  3.09 us (2%)
    all_to_all x1, waiting for transfers between devices, shards(): weight_own = lax.all_to_all(copies, CHIPS, 0, 0, tiled=True)  38.3 us
    ppermute x8, starting transfers between devices, shifted(): lax.ppermute(value, axis, [(i, (i + step) % devices) for i in range(devic...  30.3 us
    pallas_call x6, Pallas kernels, call(): pl.pallas_call(kernel, in_specs=[smem] * scalars + [anywhere] * far + [vm...  21.3 us
    all_to_all x1, blocking collectives, shards(): received = lax.all_to_all(packed, SP, 0, 0, tiled=True)  20.8 us
    all_to_all x1, starting transfers between devices, shards(): weight_own = lax.all_to_all(copies, CHIPS, 0, 0, tiled=True)  15.9 us
    all_to_all x1, blocking collectives, shards(): gathered = lax.all_to_all(activations, 'tp', 0, 0, tiled=True)  14.7 us
    ppermute x8, waiting for transfers between devices, shifted(): lax.ppermute(value, axis, [(i, (i + step) % devices) for i in range(devic...  13.4 us
    pallas_call x1, Pallas kernels, output_projection(): pl.pallas_call(output_kernel, grid=(groups, parts), in_specs=[pl.BlockSpe...  8.77 us
  transfers between devices with their start and end apart: 13, of which 6 were waited for; matrix products, arithmetic and copies ran while one was open for 3% of the time, Pallas kernels for 11%

profile of v4, /device:TPU:25, one launch (start us, length us, event | category | flops | bytes accessed | tf_op | source)
XLA Modules:
  0.0 201.1 jit_solution(5225364970836729247)
XLA Ops:
  7.3 3.1 %collective-permute-start.7 = (bf16[16,512]{1,0:T(8,128)(2,1)S(1)}, bf16[16,512]{1,0:T(8,128)(2,1)S(1)}, u32[]{:S(2)}, u32[]{:S(2)}) collective-permute-start(bf16[16,512]{1,0:T(8,128)(2,1)S(1)} %maximum_bitcast_fusion), channel_id=1, source_target_pairs={{0,1},{1,2},{2,3},{3,0},{4,5},{5,6},{6,7},{7,4},{8,9},{9,10},{10,1... | collective-permute-start | bytes 49160 | tf_op jit(solution)/shard_map/ppermute | solution.py:51
  10.4 4.4 %collective-permute-start.8 = (bf16[16,512]{1,0:T(8,128)(2,1)S(1)}, bf16[16,512]{1,0:T(8,128)(2,1)S(1)}, u32[]{:S(2)}, u32[]{:S(2)}) collective-permute-start(bf16[16,512]{1,0:T(8,128)(2,1)S(1)} %maximum_bitcast_fusion), channel_id=1, source_target_pairs={{0,2},{1,3},{2,0},{3,1},{4,6},{5,7},{6,4},{7,5},{8,10},{9,11},{10,... | collective-permute-start | bytes 49160 | tf_op jit(solution)/shard_map/ppermute | solution.py:51
  14.7 3.1 %collective-permute-start.9 = (bf16[16,512]{1,0:T(8,128)(2,1)S(1)}, bf16[16,512]{1,0:T(8,128)(2,1)S(1)}, u32[]{:S(2)}, u32[]{:S(2)}) collective-permute-start(bf16[16,512]{1,0:T(8,128)(2,1)S(1)} %maximum_bitcast_fusion), channel_id=1, source_target_pairs={{0,3},{1,0},{2,1},{3,2},{4,7},{5,4},{6,5},{7,6},{8,11},{9,8},{10,9... | collective-permute-start | bytes 49160 | tf_op jit(solution)/shard_map/ppermute | solution.py:51
  17.8 1.4 collective-permute-done.9
  21.9 15.9 %all-to-all-start = ((bf16[64,16,768]{2,1,0:T(8,128)(2,1)}), bf16[64,16,768]{2,1,0:T(8,128)(2,1)S(1)}, u32[]{:S(2)}, u32[]{:S(2)}) async-start(bf16[64,16,768]{2,1,0:T(8,128)(2,1)} %broadcast_in_dim.4), calls=%async_computation | async-start | bytes 3145728 | tf_op jit(solution)/shard_map/all_to_all | solution.py:423
  38.1 38.3 %all-to-all-done.weight_own = bf16[64,16,768]{2,1,0:T(8,128)(2,1)S(1)} async-done(((bf16[64,16,768]{2,1,0:T(8,128)(2,1)}), bf16[64,16,768]{2,1,0:T(8,128)(2,1)S(1)}, u32[]{:S(2)}, u32[]{:S(2)}) %all-to-all-start) | async-done | bytes 1572896 | tf_op jit(solution)/shard_map/all_to_all | solution.py:423
  76.3 6.8 %collective-permute-start = (bf16[64,16,768]{2,1,0:T(8,128)(2,1)S(1)}, bf16[64,16,768]{2,1,0:T(8,128)(2,1)}, u32[]{:S(2)}, u32[]{:S(2)}) collective-permute-start(bf16[64,16,768]{2,1,0:T(8,128)(2,1)S(1)} %all-to-all-done.weight_own), channel_id=1, source_target_pairs={{0,4},{4,0},{1,5},{5,1},{2,6},{6,2},{3,7},{7,3},{8,12},{12,8},{9,1... | collective-permute-start | bytes 4718600 | tf_op jit(solution)/shard_map/ppermute | solution.py:51
  83.3 1.9 collective-permute-start.1
  85.2 4.6 %collective-permute-start.2 = (bf16[128,2048]{1,0:T(8,128)(2,1)S(1)}, bf16[128,2048]{1,0:T(8,128)(2,1)S(1)}, u32[]{:S(2)}, u32[]{:S(2)}) collective-permute-start(bf16[128,2048]{1,0:T(8,128)(2,1)S(1)} %fusion.1.own), channel_id=1, source_target_pairs={{0,3},{1,0},{2,1},{3,2},{4,7},{5,4},{6,5},{7,6},{8,11},{9,8},{10,9... | collective-permute-start | bytes 1572872 | tf_op jit(solution)/shard_map/ppermute | solution.py:51
  89.8 10.1 %collective-permute-done.1.before = bf16[128,2048]{1,0:T(8,128)(2,1)S(1)} collective-permute-done((bf16[128,2048]{1,0:T(8,128)(2,1)S(1)}, bf16[128,2048]{1,0:T(8,128)(2,1)S(1)}, u32[]{:S(2)}, u32[]{:S(2)}) %collective-permute-start.1) | collective-permute-done | bytes 524320 | tf_op jit(solution)/shard_map/ppermute | solution.py:51
  99.9 1.9 collective-permute-start.3
  101.9 4.6 %collective-permute-start.4 = (bf16[64,2048]{1,0:T(8,128)(2,1)S(1)}, bf16[64,2048]{1,0:T(8,128)(2,1)}, u32[]{:S(2)}, u32[]{:S(2)}) collective-permute-start(bf16[64,2048]{1,0:T(8,128)(2,1)S(1)} %slice.17), channel_id=1, source_target_pairs={{0,3},{1,0},{2,1},{3,2},{4,7},{5,4},{6,5},{7,6},{8,11},{9,8},{10,9... | collective-permute-start | bytes 786440 | tf_op jit(solution)/shard_map/ppermute | solution.py:51
  111.0 4.4 %shard_map.127 = (bf16[512,2048]{1,0:T(8,128)(2,1)}, f32[2,512,128]{2,1,0:T(8,128)}) custom-call(s32[4]{0:T(128)} %pad_add_fusion.place, bf16[128,2048]{1,0:T(8,128)(2,1)} %copy-done.2, bf16[128,2048]{1,0:T(8,128)(2,1)} %copy-done.5, bf16[128,2048]{1,0:T(8,128)(2,1)} %copy-done.6, bf16[64,2048]{1,0:T(8,128)(2,1)} %collective-permute-done.3.far_top, ...), custom_call_target="tpu_custom_call" | custom-call | flops 1073741824 | bytes 5000000 | tf_op jit(solution)/shard_map/pallas_call | solution.py:38
  115.4 6.4 %shard_map.128 = (bf16[512,512]{1,0:T(8,128)(2,1)}, bf16[512,256]{1,0:T(8,128)(2,1)}, f32[128,1,384]{2,1,0:T(1,128)}) custom-call(s32[4]{0:T(128)} %pad_add_fusion.place, bf16[64,16,768]{2,1,0:T(8,128)(2,1)} %copy-done.1, bf16[64,16,768]{2,1,0:T(8,128)(2,1)} %collective-permute-done.weight_other, bf16[512,2048]{1,0:T(8,128)(2,1)} %get-tuple-element.12.tokens, ...), custom_call_target="tpu_custom_call" | custom-call | flops 1879048192 | bytes 8000000 | tf_op jit(solution)/shard_map/pallas_call | solution.py:38
  121.8 20.8 %all_to_all.20.received = f32[128,1,384]{2,1,0:T(1,128)} all-to-all(f32[128,1,384]{2,1,0:T(1,128)} %get-tuple-element.17), channel_id=1, replica_groups=mesh['sp_0'=8,'sp_1'=8,'sp_2'=2,'tp'=4] {'sp_0','sp_1','sp_2'}, dimensions={0} | all-to-all | bytes 393216 | tf_op jit(solution)/shard_map/all_to_all | solution.py:470
  142.6 2.3 %shard_map.130 = f32[128,1,256]{2,1,0:T(1,128)} custom-call(s32[1]{0:T(128)} %bitcast.2.place, f32[128,1,384]{2,1,0:T(1,128)} %all_to_all.20.received, f32[2,128,128]{2,1,0:T(8,128)} %bitcast.8), custom_call_target="tpu_custom_call" | custom-call | flops 40000000 | tf_op jit(solution)/shard_map/pallas_call | solution.py:38
  144.9 8.2 %all-to-all-start.2 = ((f32[128,1,256]{2,1,0:T(1,128)}), f32[128,1,256]{2,1,0:T(1,128)S(1)}, u32[]{:S(2)}, u32[]{:S(2)}) async-start(f32[128,1,256]{2,1,0:T(1,128)} %shard_map.130), calls=%async_computation.2 | async-start | bytes 262144 | tf_op jit(solution)/shard_map/all_to_all | solution.py:487
  153.8 4.6 %collective-permute-start.5 = (bf16[8,256]{1,0:T(8,128)(2,1)S(1)}, bf16[8,256]{1,0:T(8,128)(2,1)S(1)}, u32[]{:S(2)}, u32[]{:S(2)}) collective-permute-start(bf16[8,256]{1,0:T(8,128)(2,1)S(1)} %get-tuple-element.20), channel_id=1, source_target_pairs={{0,4},{4,8},{8,12},{12,16},{16,20},{20,24},{24,28},{28,32},{32,36}... | collective-permute-start | bytes 12296 | tf_op jit(solution)/shard_map/ppermute | solution.py:57
  158.4 2.1 %collective-permute-start.6 = (bf16[8,256]{1,0:T(8,128)(2,1)S(1)}, bf16[8,256]{1,0:T(8,128)(2,1)S(1)}, u32[]{:S(2)}, u32[]{:S(2)}) collective-permute-start(bf16[8,256]{1,0:T(8,128)(2,1)S(1)} %get-tuple-element.19), channel_id=1, source_target_pairs={{4,0},{8,4},{12,8},{16,12},{20,16},{24,20},{28,24},{32,28},{36,32}... | collective-permute-start | bytes 12296 | tf_op jit(solution)/shard_map/ppermute | solution.py:57
  160.5 3.1 %shard_map.129 = (f32[512,256]{1,0:T(8,128)}, bf16[512,256]{1,0:T(8,128)(2,1)}) custom-call(bf16[512,512]{1,0:T(8,128)(2,1)} %get-tuple-element.14.qkv, f32[2,512,128]{2,1,0:T(8,128)} %get-tuple-element.13.logs), custom_call_target="tpu_custom_call" | custom-call | flops 536870912 | bytes 3000000 | tf_op jit(solution)/shard_map/pallas_call | solution.py:38
  165.1 2.5 %shard_map.131.pooled = bf16[512,256]{1,0:T(8,128)(2,1)} custom-call(s32[4]{0:T(128)} %pad_add_fusion.place, bf16[512,256]{1,0:T(8,128)(2,1)} %get-tuple-element.18.pool_input, bf16[8,256]{1,0:T(8,128)(2,1)} %copy-done.8, bf16[8,256]{1,0:T(8,128)(2,1)} %copy-done.9, bf16[4,256,256]{2,1,0:T(8,128)(2,1)} %group_map.1), custom_call_target="tpu_custom_call" | custom-call | flops 67108864 | bytes 1000000 | tf_op jit(solution)/shard_map/pallas_call | solution.py:38
  168.3 2.5 %shard_map.132 = bf16[4,128,512]{2,1,0:T(8,128)(2,1)} custom-call(f32[512,256]{1,0:T(8,128)} %get-tuple-element.15.part, bf16[512,256]{1,0:T(8,128)(2,1)} %get-tuple-element.16.query, f32[128,1,256]{2,1,0:T(1,128)} %copy-done.3, bf16[512,256]{1,0:T(8,128)(2,1)} %shard_map.131.pooled), custom_call_target="tpu_custom_call" | custom-call | flops 100000000 | bytes 2000000 | tf_op jit(solution)/shard_map/pallas_call | solution.py:38
  170.8 14.7 %all_to_all.21.activations = bf16[4,128,512]{2,1,0:T(8,128)(2,1)} all-to-all(bf16[4,128,512]{2,1,0:T(8,128)(2,1)} %shard_map.132), channel_id=1, replica_groups=mesh['sp_0'=8,'sp_1'=8,'sp_2'=2,'tp'=4] {'tp'}, dimensions={0} | all-to-all | bytes 1048576 | tf_op jit(solution)/shard_map/all_to_all | solution.py:503
  185.5 8.8 %output_kernel.1 = bf16[128,2048]{1,0:T(8,128)(2,1)} custom-call(s32[4]{0:T(128)} %pad_add_fusion.place, bf16[4,128,512]{2,1,0:T(8,128)(2,1)} %all_to_all.21.activations, bf16[2048,2048]{1,0:T(8,128)(2,1)} %all-gather.2.cloned.1.call-done.weight), custom_call_target="tpu_custom_call" | custom-call | tf_op jit(solution)/shard_map/output_kernel/pallas_call | solution.py:374
  (45 shorter events, 11.1 us)
Async XLA Ops:
  6.5 179.0 %all-gather.2.cloned.1.call-start = ((), (), s32[]{:S(2)}) async-start(), calls=%async_computation.4 | async-start | bytes 8454144 | tf_op jit(solution)/shard_map/all_gather | solution.py:434
  7.3 10.6 %collective-permute-start.7 = (bf16[16,512]{1,0:T(8,128)(2,1)S(1)}, bf16[16,512]{1,0:T(8,128)(2,1)S(1)}, u32[]{:S(2)}, u32[]{:S(2)}) collective-permute-start(bf16[16,512]{1,0:T(8,128)(2,1)S(1)} %maximum_bitcast_fusion), channel_id=1, source_target_pairs={{0,1},{1,2},{2,3},{3,0},{4,5},{5,6},{6,7},{7,4},{8,9},{9,10},{10,1... | collective-permute-start | bytes 49160 | tf_op jit(solution)/shard_map/ppermute | solution.py:51
  10.4 7.4 %collective-permute-start.8 = (bf16[16,512]{1,0:T(8,128)(2,1)S(1)}, bf16[16,512]{1,0:T(8,128)(2,1)S(1)}, u32[]{:S(2)}, u32[]{:S(2)}) collective-permute-start(bf16[16,512]{1,0:T(8,128)(2,1)S(1)} %maximum_bitcast_fusion), channel_id=1, source_target_pairs={{0,2},{1,3},{2,0},{3,1},{4,6},{5,7},{6,4},{7,5},{8,10},{9,11},{10,... | collective-permute-start | bytes 49160 | tf_op jit(solution)/shard_map/ppermute | solution.py:51
  14.7 4.5 %collective-permute-start.9 = (bf16[16,512]{1,0:T(8,128)(2,1)S(1)}, bf16[16,512]{1,0:T(8,128)(2,1)S(1)}, u32[]{:S(2)}, u32[]{:S(2)}) collective-permute-start(bf16[16,512]{1,0:T(8,128)(2,1)S(1)} %maximum_bitcast_fusion), channel_id=1, source_target_pairs={{0,3},{1,0},{2,1},{3,2},{4,7},{5,4},{6,5},{7,6},{8,11},{9,8},{10,9... | collective-permute-start | bytes 49160 | tf_op jit(solution)/shard_map/ppermute | solution.py:51
  21.9 15.9 %copy-start = (bf16[128,2048]{1,0:T(8,128)(2,1)S(1)}, bf16[128,2048]{1,0:T(8,128)(2,1)}, u32[]{:S(2)}) copy-start(bf16[128,2048]{1,0:T(8,128)(2,1)} %param.13) | copy-start | bytes 1572868
  21.9 54.4 %all-to-all-start = ((bf16[64,16,768]{2,1,0:T(8,128)(2,1)}), bf16[64,16,768]{2,1,0:T(8,128)(2,1)S(1)}, u32[]{:S(2)}, u32[]{:S(2)}) async-start(bf16[64,16,768]{2,1,0:T(8,128)(2,1)} %broadcast_in_dim.4), calls=%async_computation | async-start | bytes 3145728 | tf_op jit(solution)/shard_map/all_to_all | solution.py:423
  37.9 68.6 %copy-start.4 = (bf16[2048,64]{0,1:T(8,128)(2,1)S(1)}, bf16[2048,64]{0,1:T(8,128)(2,1)}, u32[]{:S(2)}) copy-start(bf16[2048,64]{0,1:T(8,128)(2,1)} %param.18) | copy-start | bytes 786436
  38.1 69.4 %copy-start.7 = (f32[2,512]{1,0:T(2,128)S(1)}, f32[2,512]{1,0:T(2,128)}, u32[]{:S(2)}) copy-start(f32[2,512]{1,0:T(2,128)} %param.21) | copy-start | bytes 12292
  76.3 32.0 %copy-start.1 = (bf16[64,16,768]{2,1,0:T(8,128)(2,1)}, bf16[64,16,768]{2,1,0:T(8,128)(2,1)S(1)}, u32[]{:S(2)}) copy-start(bf16[64,16,768]{2,1,0:T(8,128)(2,1)S(1)} %all-to-all-done.weight_own) | copy-start | bytes 4718596
  76.3 39.0 %collective-permute-start = (bf16[64,16,768]{2,1,0:T(8,128)(2,1)S(1)}, bf16[64,16,768]{2,1,0:T(8,128)(2,1)}, u32[]{:S(2)}, u32[]{:S(2)}) collective-permute-start(bf16[64,16,768]{2,1,0:T(8,128)(2,1)S(1)} %all-to-all-done.weight_own), channel_id=1, source_target_pairs={{0,4},{4,0},{1,5},{5,1},{2,6},{6,2},{3,7},{7,3},{8,12},{12,8},{9,1... | collective-permute-start | bytes 4718600 | tf_op jit(solution)/shard_map/ppermute | solution.py:51
  83.3 27.7 %copy-start.2 = (bf16[128,2048]{1,0:T(8,128)(2,1)}, bf16[128,2048]{1,0:T(8,128)(2,1)S(1)}, u32[]{:S(2)}) copy-start(bf16[128,2048]{1,0:T(8,128)(2,1)S(1)} %fusion.1.own) | copy-start | bytes 1572868
  83.3 16.6 %collective-permute-start.1 = (bf16[128,2048]{1,0:T(8,128)(2,1)S(1)}, bf16[128,2048]{1,0:T(8,128)(2,1)S(1)}, u32[]{:S(2)}, u32[]{:S(2)}) collective-permute-start(bf16[128,2048]{1,0:T(8,128)(2,1)S(1)} %fusion.1.own), channel_id=1, source_target_pairs={{0,1},{1,2},{2,3},{3,0},{4,5},{5,6},{6,7},{7,4},{8,9},{9,10},{10,1... | collective-permute-start | bytes 1572872 | tf_op jit(solution)/shard_map/ppermute | solution.py:51
  85.2 16.6 %collective-permute-start.2 = (bf16[128,2048]{1,0:T(8,128)(2,1)S(1)}, bf16[128,2048]{1,0:T(8,128)(2,1)S(1)}, u32[]{:S(2)}, u32[]{:S(2)}) collective-permute-start(bf16[128,2048]{1,0:T(8,128)(2,1)S(1)} %fusion.1.own), channel_id=1, source_target_pairs={{0,3},{1,0},{2,1},{3,2},{4,7},{5,4},{6,5},{7,6},{8,11},{9,8},{10,9... | collective-permute-start | bytes 1572872 | tf_op jit(solution)/shard_map/ppermute | solution.py:51
  99.9 11.1 %copy-start.5 = (bf16[128,2048]{1,0:T(8,128)(2,1)}, bf16[128,2048]{1,0:T(8,128)(2,1)S(1)}, u32[]{:S(2)}) copy-start(bf16[128,2048]{1,0:T(8,128)(2,1)S(1)} %collective-permute-done.1.before) | copy-start | bytes 1572868
  99.9 10.2 %collective-permute-start.3 = (bf16[64,2048]{1,0:T(8,128)(2,1)S(1)}, bf16[64,2048]{1,0:T(8,128)(2,1)}, u32[]{:S(2)}, u32[]{:S(2)}) collective-permute-start(bf16[64,2048]{1,0:T(8,128)(2,1)S(1)} %slice.16), channel_id=1, source_target_pairs={{0,1},{1,2},{2,3},{3,0},{4,5},{5,6},{6,7},{7,4},{8,9},{9,10},{10,1... | collective-permute-start | bytes 786440 | tf_op jit(solution)/shard_map/ppermute | solution.py:51
  101.9 4.6 %copy-start.6 = (bf16[128,2048]{1,0:T(8,128)(2,1)}, bf16[128,2048]{1,0:T(8,128)(2,1)S(1)}, u32[]{:S(2)}) copy-start(bf16[128,2048]{1,0:T(8,128)(2,1)S(1)} %collective-permute-done.2.after) | copy-start | bytes 1572868
  101.9 9.1 %collective-permute-start.4 = (bf16[64,2048]{1,0:T(8,128)(2,1)S(1)}, bf16[64,2048]{1,0:T(8,128)(2,1)}, u32[]{:S(2)}, u32[]{:S(2)}) collective-permute-start(bf16[64,2048]{1,0:T(8,128)(2,1)S(1)} %slice.17), channel_id=1, source_target_pairs={{0,3},{1,0},{2,1},{3,2},{4,7},{5,4},{6,5},{7,6},{8,11},{9,8},{10,9... | collective-permute-start | bytes 786440 | tf_op jit(solution)/shard_map/ppermute | solution.py:51
  144.9 22.8 %all-to-all-start.2 = ((f32[128,1,256]{2,1,0:T(1,128)}), f32[128,1,256]{2,1,0:T(1,128)S(1)}, u32[]{:S(2)}, u32[]{:S(2)}) async-start(f32[128,1,256]{2,1,0:T(1,128)} %shard_map.130), calls=%async_computation.2 | async-start | bytes 262144 | tf_op jit(solution)/shard_map/all_to_all | solution.py:487
  153.8 9.8 %collective-permute-start.5 = (bf16[8,256]{1,0:T(8,128)(2,1)S(1)}, bf16[8,256]{1,0:T(8,128)(2,1)S(1)}, u32[]{:S(2)}, u32[]{:S(2)}) collective-permute-start(bf16[8,256]{1,0:T(8,128)(2,1)S(1)} %get-tuple-element.20), channel_id=1, source_target_pairs={{0,4},{4,8},{8,12},{12,16},{16,20},{20,24},{24,28},{28,32},{32,36}... | collective-permute-start | bytes 12296 | tf_op jit(solution)/shard_map/ppermute | solution.py:57
  158.4 6.1 %collective-permute-start.6 = (bf16[8,256]{1,0:T(8,128)(2,1)S(1)}, bf16[8,256]{1,0:T(8,128)(2,1)S(1)}, u32[]{:S(2)}, u32[]{:S(2)}) collective-permute-start(bf16[8,256]{1,0:T(8,128)(2,1)S(1)} %get-tuple-element.19), channel_id=1, source_target_pairs={{4,0},{8,4},{12,8},{16,12},{20,16},{24,20},{28,24},{32,28},{36,32}... | collective-permute-start | bytes 12296 | tf_op jit(solution)/shard_map/ppermute | solution.py:57
  163.6 0.9 copy-start.8
  164.5 0.6 copy-start.9
  167.7 0.7 copy-start.3
Sparse Core Ops, SparseCore 0:
  20.0 114.7 all-gather.1

commit v5 on v4

--- a/solution.py
+++ b/solution.py
@@ -23,7 +23,6 @@
 
 bf16 = jnp.bfloat16
 f32 = jnp.float32
-exact = lax.Precision.HIGHEST
 
 
 def matmul(a, b, dims=((1,), (0,)), precision=None):
@@ -102,7 +101,7 @@
     tp = place[0]
     place_tokens(tp, (own, before, after, far_top, far_end), tokens_out, 0)
     rows = tokens_out.shape[0]
-    low_rank = matmul(tokens_out[...], inner[...]).astype(bf16)
+    low_rank = matmul(tokens_out[...], inner[...], ((1,), (1,))).astype(bf16)
     here = pl.ds(pl.multiple_of(tp * LANES, LANES), LANES)
     blank = jnp.zeros((RANK, LANES), bf16)
     outer_both = jnp.concatenate(
@@ -116,7 +115,8 @@
     pre = matmul(low_rank, outer_both) + bias_both
     gate = jnp.minimum(pre, 0.0) - jnp.log1p(jnp.exp(-jnp.abs(pre)))
     lane = lax.broadcasted_iota(jnp.int32, (rows, LANES), 1)
-    spikes = jnp.where(lane < KEY_CHANNELS, spike[:, 0:1], spike[:, 1:2])
+    spike_rows = jnp.concatenate([spike[...], jnp.zeros((6, rows), f32)], axis=0).T
+    spikes = jnp.where(lane < KEY_CHANNELS, spike_rows[:, 0:1], spike_rows[:, 1:2])
     decay = gate * (1.0 / gate_norm_factor) + jnp.concatenate([spikes, spikes], axis=1)
     size = LANES
     row_ids = lax.broadcasted_iota(jnp.int32, (size, size), 0)
@@ -136,41 +136,35 @@
         carry = found[0:1, :]
 
 
+def load_weights(core, start, weight_own, weight_other, weight_ref, sems):
+    columns = slice(start, start + weight_ref.shape[-1])
+    for n, (side, source) in enumerate(((core, weight_own), (1 - core, weight_other))):
+        yield pltpu.make_async_copy(
+            source.at[:, :, columns], weight_ref.at[:, side], sems.at[n]
+        )
+
+
 def project_kernel(
-    place,
-    weight_own,
-    weight_other,
-    tokens,
-    logs,
-    qkv_out,
-    pool_out,
-    packed_out,
-    weight_ref,
-    sems,
+    place, weight_own, weight_other, tokens, logs, keys_values, packed_out, tokens_ref, weight_ref, sems
 ):
-    core = place[1]
-    load_own = pltpu.make_async_copy(weight_own, weight_ref.at[:, core], sems.at[0])
-    load_other = pltpu.make_async_copy(weight_other, weight_ref.at[:, 1 - core], sems.at[1])
-    load_own.start()
-    load_other.start()
-    rows, width = tokens.shape
+    loads = list(load_weights(place[1], 0, weight_own, weight_other, weight_ref, sems))
+    loads.append(pltpu.make_async_copy(tokens, tokens_ref, sems.at[2]))
+    for load in loads:
+        load.start()
+    rows, width = tokens_ref.shape
     total_fwd = logs[0, rows - 1 : rows, :]
     total_bwd = logs[1, 0:1, :]
-    load_own.wait()
-    load_other.wait()
-    projected = matmul(tokens[...], weight_ref[...].reshape(width, -1)).astype(bf16)
-    qkv = projected[:, : 4 * LANES]
-    qkv_out[...] = qkv
-    pool_out[...] = projected[:, 4 * LANES :]
-    keys = qkv[:, LANES : 2 * LANES].astype(f32)
+    far_fwd = jnp.exp(total_fwd - logs[0])
+    far_bwd = jnp.exp(total_bwd - logs[1])
+    for load in loads:
+        load.wait()
+    found = matmul(tokens_ref[...], weight_ref[...].reshape(width, -1)).astype(bf16)
+    keys_values[...] = found
+    keys = found[:, :LANES].astype(f32)
     weighted = jnp.concatenate(
-        [
-            (keys * jnp.exp(total_fwd - logs[0])).astype(bf16),
-            (keys * jnp.exp(total_bwd - logs[1])).astype(bf16),
-        ],
-        axis=1,
-    )
-    updates = matmul(weighted, qkv[:, 2 * LANES :], ((0,), (0,)))
+        [(keys * far_fwd).astype(bf16), (keys * far_bwd).astype(bf16)], axis=1
+    )
+    updates = matmul(weighted, found[:, LANES:], ((0,), (0,)))
     first = lax.broadcasted_iota(jnp.int32, (LANES, LANES), 0) < KEY_CHANNELS
     for d in range(2):
         mine = updates[d * LANES : (d + 1) * LANES]
@@ -182,18 +176,37 @@
     packed_out[:, 0, 2 * LANES :] = stacked.T
 
 
+def late_kernel(
+    place, weight_own, weight_other, tokens, query_out, pool_out, tokens_ref, weight_ref, sems
+):
+    loads = list(load_weights(place[1], 3 * LANES, weight_own, weight_other, weight_ref, sems))
+    loads.append(pltpu.make_async_copy(tokens, tokens_ref, sems.at[2]))
+    for load in loads:
+        load.start()
+    for load in loads:
+        load.wait()
+    width = tokens_ref.shape[1]
+    found = matmul(tokens_ref[...], weight_ref[...].reshape(width, -1)).astype(bf16)
+    query_out[...] = found[:, :LANES]
+    pool_out[...] = found[:, LANES:]
+
+
 def scan_kernel(place, received, start, out):
     devices = received.shape[0]
     here = place[0]
     logs = received[:, 0, 2 * LANES :]
     row = lax.broadcasted_iota(jnp.int32, (devices, devices), 0)
     col = lax.broadcasted_iota(jnp.int32, (devices, devices), 1)
-    earlier = (col < row).astype(f32)
-    upto = (row <= col).astype(f32)
-    strictly = (row < col).astype(f32)
-    before_col = matmul(earlier, logs, precision=exact)
-    before_row = matmul(logs, strictly, ((0,), (0,)), precision=exact)
-    past_row = matmul(logs, upto, ((0,), (0,)), precision=exact)
+    high = logs.astype(bf16)
+    low = (logs - high.astype(f32)).astype(bf16)
+    turn = ((0,), (0,))
+    earlier = (col < row).astype(bf16)
+    strictly = (row < col).astype(bf16)
+    upto = (row <= col).astype(bf16)
+    before_col = matmul(earlier, high) + matmul(earlier, low)
+    before_row = matmul(high, strictly, turn) + matmul(low, strictly, turn)
+    past_row = matmul(high, upto, turn) + matmul(low, upto, turn)
+    logs = high.astype(f32) + low.astype(f32)
     past_col = before_col + logs
     total = jnp.sum(logs, axis=0, keepdims=True)
     for r in range(2):
@@ -215,8 +228,8 @@
         out[:, 0, r * LANES : (r + 1) * LANES] = entering
 
 
-def inner_kernel(qkv, logs, part_out, query_out):
-    rows = qkv.shape[0]
+def inner_kernel(query, keys_values, logs, part_out, query_out):
+    rows = query.shape[0]
     blocks = rows // BLOCK
     lane = lax.broadcasted_iota(jnp.int32, (BLOCK, LANES), 1)
     row = lax.broadcasted_iota(jnp.int32, (BLOCK, LANES), 0)
@@ -240,9 +253,9 @@
         cum_bwd = logs[1, at, :] - base_bwd
         edge_fwd = cum_fwd[BLOCK - 1 : BLOCK, :]
         edge_bwd = cum_bwd[0:1, :]
-        queries = qkv[at, :LANES].astype(f32) * scale
-        keys = qkv[at, LANES : 2 * LANES].astype(f32)
-        values = qkv[at, 2 * LANES :]
+        queries = query[at, :].astype(f32) * scale
+        keys = keys_values[at, :LANES].astype(f32)
+        values = keys_values[at, LANES:]
         query_out[at, :LANES] = (queries * jnp.exp(logs[0, at, :])).astype(bf16)
         query_out[at, LANES:] = (queries * jnp.exp(logs[1, at, :])).astype(bf16)
         query_fwd = (queries * jnp.exp(cum_fwd)).astype(bf16)
@@ -346,45 +359,49 @@
             start += piece.shape[1]
 
 
-def output_kernel(place, activations, weight, out, total):
-    groups = activations.shape[0]
-    step, part = (pl.program_id(0), pl.program_id(1))
-    tile = weight.shape[0]
-    here = pl.ds(pl.multiple_of(part * tile, tile), tile)
-    source = lax.rem(place[0] + groups - step, groups)
-    partial = matmul(weight[...], activations[source], ((1,), (1,))).astype(bf16).astype(f32)
-
-    @pl.when(step == 0)
-    def _():
-        total[here, :] = partial
-
-    @pl.when(step > 0)
-    def _():
-        total[here, :] += partial
-
-    @pl.when(step == groups - 1)
-    def _():
-        out[:, here] = total[here, :].T.astype(bf16)
+def output_kernel(place, weights, activations, out, weight_ref, total, sems):
+    groups, _, width = activations.shape
+    parts, tile = weight_ref.shape[1:3]
+    loads = {}
+    for s in range(groups):
+        for n in range(parts):
+            loads[s, n] = pltpu.make_async_copy(
+                weights.at[n * tile : (n + 1) * tile, s * width : (s + 1) * width],
+                weight_ref.at[s, n],
+                sems.at[s * parts + n],
+            )
+            loads[s, n].start()
+    for s in range(groups):
+        mine = activations[lax.rem(place[0] + groups - s, groups)]
+        for n in range(parts):
+            here = slice(n * tile, (n + 1) * tile)
+            loads[s, n].wait()
+            partial = matmul(weight_ref[s, n], mine, ((1,), (1,))).astype(bf16).astype(f32)
+            if s == 0:
+                total[here, :] = partial
+            elif s + 1 < groups:
+                total[here, :] += partial
+            else:
+                out[:, here] = (total[here, :] + partial).T.astype(bf16)
 
 
 def output_projection(place, activations, weights):
     groups, rows, width = activations.shape
     model = weights.shape[0]
     parts = 2
-    return pl.pallas_call(
+    return call(
         output_kernel,
-        grid=(groups, parts),
-        in_specs=[
-            pl.BlockSpec(memory_space=pltpu.SMEM),
-            pl.BlockSpec((groups, rows, width), lambda s, n: (0, 0, 0)),
-            pl.BlockSpec((model // parts, width), lambda s, n: (n, s)),
-        ],
-        out_specs=pl.BlockSpec((rows, model), lambda s, n: (0, 0)),
-        out_shape=jax.ShapeDtypeStruct((rows, model), bf16),
-        scratch_shapes=[pltpu.VMEM((model, rows), f32)],
-        interpret=interpreted,
-        name="output_kernel",
-    )(place, activations, weights)
+        shape_of(rows, model),
+        (place, weights, activations),
+        far=1,
+        scratch=(
+            pltpu.VMEM((groups, parts, model // parts, width), bf16),
+            pltpu.VMEM((model, rows), f32),
+            pltpu.SemaphoreType.DMA((groups * parts,)),
+        ),
+        flops=2 * rows * model * groups * width,
+        moved=2 * model * groups * width,
+    )
 
 
 def shape_of(*lengths, kind=bf16):
@@ -416,7 +433,7 @@
     model = tokens.shape[1]
 
     local_in = jnp.concatenate(
-        [query_matrix, key_matrix, value_matrix, pooling_input_weight], axis=1
+        [key_matrix, value_matrix, query_matrix, pooling_input_weight], axis=1
     )
     chips = lax.axis_size(CHIPS)
     copies = jnp.broadcast_to(local_in, (chips, *local_in.shape))
@@ -443,41 +460,48 @@
             after,
             far_top,
             far_end,
-            decay_inner_weight,
+            decay_inner_weight.T,
             decay_outer_weight,
             channel_decay_bias,
-            spike_log_decay.T,
+            spike_log_decay,
         ),
         flops=2 * rows * model * 4 * LANES,
         moved=5_000_000,
     )
-    qkv, pool_input, packed = call(
+    project_scratch = (
+        pltpu.VMEM((rows, model), bf16),
+        pltpu.VMEM((chips, 2, model // (2 * chips), 3 * LANES), bf16),
+        pltpu.SemaphoreType.DMA((3,)),
+    )
+    keys_values, packed = call(
         project_kernel,
-        (
-            shape_of(rows, 4 * LANES),
-            shape_of(rows, 2 * LANES),
-            shape_of(LANES, 1, 3 * LANES, kind=f32),
-        ),
+        (shape_of(rows, 3 * LANES), shape_of(LANES, 1, 3 * LANES, kind=f32)),
         (place, weight_own, weight_other, all_tokens, logs),
-        far=2,
-        scratch=(
-            pltpu.VMEM((chips, 2, model // (2 * chips), 6 * LANES), bf16),
-            pltpu.SemaphoreType.DMA((2,)),
-        ),
-        flops=2 * rows * model * 7 * LANES,
-        moved=8_000_000,
+        far=3,
+        scratch=project_scratch,
+        flops=2 * rows * model * 4 * LANES,
+        moved=4_000_000,
     )
     received = lax.all_to_all(packed, SP, 0, 0, tiled=True)
-    rim_before = neighbours(pool_input[rows - rim_width :], SP, 1)
-    rim_after = neighbours(pool_input[:rim_width], SP, -1)
+    query, pool_input = call(
+        late_kernel,
+        (shape_of(rows, LANES), shape_of(rows, 2 * LANES)),
+        (place, weight_own, weight_other, all_tokens),
+        far=3,
+        scratch=project_scratch,
+        flops=2 * rows * model * 3 * LANES,
+        moved=4_000_000,
+    )
     part, query = call(
         inner_kernel,
         (shape_of(rows, 2 * DV, kind=f32), shape_of(rows, 2 * LANES)),
-        (qkv, logs),
+        (query, keys_values, logs),
         scalars=0,
         flops=2 * rows * model * 2 * LANES,
         moved=3_000_000,
     )
+    rim_before = neighbours(pool_input[rows - rim_width :], SP, 1)
+    rim_after = neighbours(pool_input[:rim_width], SP, -1)
     states = call(
         scan_kernel,
         shape_of(positions, 1, 2 * LANES, kind=f32),

time: 202 us -> 205 us (1.015)
  blocking collectives: 35.5 us -> 14.4 us
  starting transfers between devices: 61.1 us -> 70.6 us
  waiting for transfers between devices: 52.6 us -> 61.5 us
  Pallas kernels: 30.1 us -> 33.8 us
    all_to_all x1 -> x0, blocking collectives: 20.8 us -> none  [shards(): received = lax.all_to_all(packed, SP, 0, 0, tiled=True)]
    pallas_call x6 -> x8, Pallas kernels: 21.3 us -> 33.8 us  [call(): pl.pallas_call(kernel, in_specs=[smem] * scalars + [anywhere] * far + [vm...]
    all_to_all x0 -> x1, starting transfers between devices: none -> 9.73 us  [shards(): received = lax.all_to_all(packed, SP, 0, 0, tiled=True)]
    pallas_call x1 -> x0, Pallas kernels: 8.77 us -> none  [output_projection(): pl.pallas_call(output_kernel, grid=(groups, parts), in_specs=[pl.BlockSpe...]
    all_to_all x0 -> x1, waiting for transfers between devices: none -> 6.64 us  [shards(): received = lax.all_to_all(packed, SP, 0, 0, tiled=True)]
    ppermute x8, waiting for transfers between devices: 13.4 us -> 15.6 us  [shifted(): lax.ppermute(value, axis, [(i, (i + step) % devices) for i in range(devic...]
  transfers between devices with their start and end apart: 13 -> 14, of which waited for: 6 -> 7; matrix products, arithmetic and copies ran while one was open for 3% -> 3% of each run, Pallas kernels for 11% -> 12%
where the time goes in v5:
time: 205 us; the launch traced here: 204 us
  starting transfers between devices  70.6 us (34%)
  waiting for transfers between devices  61.5 us (30%)
  Pallas kernels  33.8 us (16%)
  blocking collectives  14.4 us (7%)
  between operations  13.6 us (7%)
  local copies, waits for them, and re-layouts  5.98 us (3%)
  other arithmetic  4.08 us (2%)
    all_to_all x1, waiting for transfers between devices, shards(): weight_own = lax.all_to_all(copies, CHIPS, 0, 0, tiled=True)  38.3 us
    pallas_call x8, Pallas kernels, call(): pl.pallas_call(kernel, in_specs=[smem] * scalars + [anywhere] * far + [vm...  33.8 us
    ppermute x8, starting transfers between devices, shifted(): lax.ppermute(value, axis, [(i, (i + step) % devices) for i in range(devic...  30.1 us
    all_to_all x1, starting transfers between devices, shards(): weight_own = lax.all_to_all(copies, CHIPS, 0, 0, tiled=True)  15.9 us
    ppermute x8, waiting for transfers between devices, shifted(): lax.ppermute(value, axis, [(i, (i + step) % devices) for i in range(devic...  15.6 us
    all_to_all x1, blocking collectives, shards(): gathered = lax.all_to_all(activations, 'tp', 0, 0, tiled=True)  14.4 us
    all_to_all x1, starting transfers between devices, shards(): received = lax.all_to_all(packed, SP, 0, 0, tiled=True)  9.73 us
    all_to_all x1, starting transfers between devices, shards(): entering = lax.all_to_all(states, SP, 0, 0, tiled=True)  8.13 us
  transfers between devices with their start and end apart: 14, of which 7 were waited for; matrix products, arithmetic and copies ran while one was open for 3% of the time, Pallas kernels for 12%

profile of v5, /device:TPU:25, one launch (start us, length us, event | category | flops | bytes accessed | tf_op | source)
XLA Modules:
  0.0 204.0 jit_solution(1077239933166273133)
XLA Ops:
  7.3 3.1 %collective-permute-start = (bf16[16,512]{1,0:T(8,128)(2,1)S(1)}, bf16[16,512]{1,0:T(8,128)(2,1)S(1)}, u32[]{:S(2)}, u32[]{:S(2)}) collective-permute-start(bf16[16,512]{1,0:T(8,128)(2,1)S(1)} %maximum_bitcast_fusion), channel_id=1, source_target_pairs={{0,1},{1,2},{2,3},{3,0},{4,5},{5,6},{6,7},{7,4},{8,9},{9,10},{10,1... | collective-permute-start | bytes 49160 | tf_op jit(solution)/shard_map/ppermute | solution.py:50
  10.4 4.4 %collective-permute-start.1 = (bf16[16,512]{1,0:T(8,128)(2,1)S(1)}, bf16[16,512]{1,0:T(8,128)(2,1)S(1)}, u32[]{:S(2)}, u32[]{:S(2)}) collective-permute-start(bf16[16,512]{1,0:T(8,128)(2,1)S(1)} %maximum_bitcast_fusion), channel_id=1, source_target_pairs={{0,2},{1,3},{2,0},{3,1},{4,6},{5,7},{6,4},{7,5},{8,10},{9,11},{10,... | collective-permute-start | bytes 49160 | tf_op jit(solution)/shard_map/ppermute | solution.py:50
  14.7 3.1 %collective-permute-start.2 = (bf16[16,512]{1,0:T(8,128)(2,1)S(1)}, bf16[16,512]{1,0:T(8,128)(2,1)S(1)}, u32[]{:S(2)}, u32[]{:S(2)}) collective-permute-start(bf16[16,512]{1,0:T(8,128)(2,1)S(1)} %maximum_bitcast_fusion), channel_id=1, source_target_pairs={{0,3},{1,0},{2,1},{3,2},{4,7},{5,4},{6,5},{7,6},{8,11},{9,8},{10,9... | collective-permute-start | bytes 49160 | tf_op jit(solution)/shard_map/ppermute | solution.py:50
  21.9 15.9 %all-to-all-start = ((bf16[64,16,768]{2,1,0:T(8,128)(2,1)}), bf16[64,16,768]{2,1,0:T(8,128)(2,1)S(1)}, u32[]{:S(2)}, u32[]{:S(2)}) async-start(bf16[64,16,768]{2,1,0:T(8,128)(2,1)} %broadcast_in_dim.4), calls=%async_computation | async-start | bytes 3145728 | tf_op jit(solution)/shard_map/all_to_all | solution.py:440
  38.0 38.3 %all-to-all-done.weight_own = bf16[64,16,768]{2,1,0:T(8,128)(2,1)S(1)} async-done(((bf16[64,16,768]{2,1,0:T(8,128)(2,1)}), bf16[64,16,768]{2,1,0:T(8,128)(2,1)S(1)}, u32[]{:S(2)}, u32[]{:S(2)}) %all-to-all-start) | async-done | bytes 1572896 | tf_op jit(solution)/shard_map/all_to_all | solution.py:440
  76.3 6.6 %collective-permute-start.3 = (bf16[64,16,768]{2,1,0:T(8,128)(2,1)S(1)}, bf16[64,16,768]{2,1,0:T(8,128)(2,1)S(1)}, u32[]{:S(2)}, u32[]{:S(2)}) collective-permute-start(bf16[64,16,768]{2,1,0:T(8,128)(2,1)S(1)} %all-to-all-done.weight_own), channel_id=1, source_target_pairs={{0,4},{4,0},{1,5},{5,1},{2,6},{6,2},{3,7},{7,3},{8,12},{12,8},{9,1... | collective-permute-start | bytes 4718600 | tf_op jit(solution)/shard_map/ppermute | solution.py:50
  86.1 4.6 %collective-permute-start.5 = (bf16[128,2048]{1,0:T(8,128)(2,1)S(1)}, bf16[128,2048]{1,0:T(8,128)(2,1)S(1)}, u32[]{:S(2)}, u32[]{:S(2)}) collective-permute-start(bf16[128,2048]{1,0:T(8,128)(2,1)S(1)} %fusion.1.own), channel_id=1, source_target_pairs={{0,3},{1,0},{2,1},{3,2},{4,7},{5,4},{6,5},{7,6},{8,11},{9,8},{10,9... | collective-permute-start | bytes 1572872 | tf_op jit(solution)/shard_map/ppermute | solution.py:50
  90.7 10.1 %collective-permute-done.4.before = bf16[128,2048]{1,0:T(8,128)(2,1)S(1)} collective-permute-done((bf16[128,2048]{1,0:T(8,128)(2,1)S(1)}, bf16[128,2048]{1,0:T(8,128)(2,1)S(1)}, u32[]{:S(2)}, u32[]{:S(2)}) %collective-permute-start.4) | collective-permute-done | bytes 524320 | tf_op jit(solution)/shard_map/ppermute | solution.py:50
  103.6 4.6 %collective-permute-start.7 = (bf16[64,2048]{1,0:T(8,128)(2,1)}, bf16[64,2048]{1,0:T(8,128)(2,1)}, u32[]{:S(2)}, u32[]{:S(2)}) collective-permute-start(bf16[64,2048]{1,0:T(8,128)(2,1)} %slice.17), channel_id=1, source_target_pairs={{0,3},{1,0},{2,1},{3,2},{4,7},{5,4},{6,5},{7,6},{8,11},{9,8},{10,9... | collective-permute-start | bytes 786440 | tf_op jit(solution)/shard_map/ppermute | solution.py:50
  108.8 2.2 %collective-permute-done.6.far_top = bf16[64,2048]{1,0:T(8,128)(2,1)} collective-permute-done((bf16[64,2048]{1,0:T(8,128)(2,1)S(1)}, bf16[64,2048]{1,0:T(8,128)(2,1)}, u32[]{:S(2)}, u32[]{:S(2)}) %collective-permute-start.6) | collective-permute-done | bytes 262176 | tf_op jit(solution)/shard_map/ppermute | solution.py:50
  113.0 4.2 %shard_map.127 = (bf16[512,2048]{1,0:T(8,128)(2,1)}, f32[2,512,128]{2,1,0:T(8,128)}) custom-call(s32[4]{0:T(128)} %pad_add_fusion.place, bf16[128,2048]{1,0:T(8,128)(2,1)} %copy-done.4, bf16[128,2048]{1,0:T(8,128)(2,1)} %copy-done.6, bf16[128,2048]{1,0:T(8,128)(2,1)} %copy-done.7, bf16[64,2048]{1,0:T(8,128)(2,1)} %collective-permute-done.6.far_top, ...), custom_call_target="tpu_custom_call" | custom-call | flops 1073741824 | bytes 5000000 | tf_op jit(solution)/shard_map/pallas_call | solution.py:37
  118.4 5.5 %shard_map.129 = (bf16[512,384]{1,0:T(8,128)(2,1)}, f32[128,1,384]{2,1,0:T(1,128)}) custom-call(s32[4]{0:T(128)} %pad_add_fusion.place, bf16[64,16,768]{2,1,0:T(8,128)(2,1)} %copy-done, bf16[64,16,768]{2,1,0:T(8,128)(2,1)} %copy-done.1, bf16[512,2048]{1,0:T(8,128)(2,1)} %get-tuple-element.13.tokens, f32[2,512,128]{2,1,0:T(8,128)} %get-tuple-element.15.logs), custom_call_target="tpu_custom_call" | custom-call | flops 1073741824 | bytes 4000000 | tf_op jit(solution)/shard_map/pallas_call | solution.py:37
  123.9 9.7 %all-to-all-start.1 = ((f32[128,1,384]{2,1,0:T(1,128)}), f32[128,1,384]{2,1,0:T(1,128)S(1)}, u32[]{:S(2)}, u32[]{:S(2)}) async-start(f32[128,1,384]{2,1,0:T(1,128)} %get-tuple-element.19), calls=%async_computation.1 | async-start | bytes 393216 | tf_op jit(solution)/shard_map/all_to_all | solution.py:485
  133.6 4.8 %shard_map.128 = (bf16[512,128]{1,0:T(8,128)(2,1)}, bf16[512,256]{1,0:T(8,128)(2,1)}) custom-call(s32[4]{0:T(128)} %pad_add_fusion.place, bf16[64,16,768]{2,1,0:T(8,128)(2,1)} %copy-done, bf16[64,16,768]{2,1,0:T(8,128)(2,1)} %copy-done.1, bf16[512,2048]{1,0:T(8,128)(2,1)} %get-tuple-element.13.tokens), custom_call_target="tpu_custom_call" | custom-call | flops 805306368 | bytes 4000000 | tf_op jit(solution)/shard_map/pallas_call | solution.py:37
  138.4 6.6 %all-to-all-done.1.received = f32[128,1,384]{2,1,0:T(1,128)S(1)} async-done(((f32[128,1,384]{2,1,0:T(1,128)}), f32[128,1,384]{2,1,0:T(1,128)S(1)}, u32[]{:S(2)}, u32[]{:S(2)}) %all-to-all-start.1) | async-done | bytes 196640 | tf_op jit(solution)/shard_map/all_to_all | solution.py:485
  145.7 2.4 %shard_map.131 = f32[128,1,256]{2,1,0:T(1,128)} custom-call(s32[1]{0:T(128)} %bitcast.2.place, f32[128,1,384]{2,1,0:T(1,128)} %copy-done.3, f32[2,128,128]{2,1,0:T(8,128)} %bitcast.7), custom_call_target="tpu_custom_call" | custom-call | flops 40000000 | tf_op jit(solution)/shard_map/pallas_call | solution.py:37
  148.1 8.1 %all-to-all-start.2 = ((f32[128,1,256]{2,1,0:T(1,128)}), f32[128,1,256]{2,1,0:T(1,128)S(1)}, u32[]{:S(2)}, u32[]{:S(2)}) async-start(f32[128,1,256]{2,1,0:T(1,128)} %shard_map.131), calls=%async_computation.2 | async-start | bytes 262144 | tf_op jit(solution)/shard_map/all_to_all | solution.py:511
  156.9 4.6 %collective-permute-start.8 = (bf16[8,256]{1,0:T(8,128)(2,1)S(1)}, bf16[8,256]{1,0:T(8,128)(2,1)S(1)}, u32[]{:S(2)}, u32[]{:S(2)}) collective-permute-start(bf16[8,256]{1,0:T(8,128)(2,1)S(1)} %get-tuple-element.22), channel_id=1, source_target_pairs={{0,4},{4,8},{8,12},{12,16},{16,20},{20,24},{24,28},{28,32},{32,36}... | collective-permute-start | bytes 12296 | tf_op jit(solution)/shard_map/ppermute | solution.py:56
  161.5 2.1 %collective-permute-start.9 = (bf16[8,256]{1,0:T(8,128)(2,1)S(1)}, bf16[8,256]{1,0:T(8,128)(2,1)S(1)}, u32[]{:S(2)}, u32[]{:S(2)}) collective-permute-start(bf16[8,256]{1,0:T(8,128)(2,1)S(1)} %get-tuple-element.21), channel_id=1, source_target_pairs={{4,0},{8,4},{12,8},{16,12},{20,16},{24,20},{28,24},{32,28},{36,32}... | collective-permute-start | bytes 12296 | tf_op jit(solution)/shard_map/ppermute | solution.py:56
  163.6 3.1 %shard_map.130 = (f32[512,256]{1,0:T(8,128)}, bf16[512,256]{1,0:T(8,128)(2,1)}) custom-call(bf16[512,128]{1,0:T(8,128)(2,1)} %get-tuple-element.14.query, bf16[512,384]{1,0:T(8,128)(2,1)} %get-tuple-element.16.keys_values, f32[2,512,128]{2,1,0:T(8,128)} %get-tuple-element.15.logs), custom_call_target="tpu_custom_call" | custom-call | flops 536870912 | bytes 3000000 | tf_op jit(solution)/shard_map/pallas_call | solution.py:37
  168.2 2.5 %shard_map.132.pooled = bf16[512,256]{1,0:T(8,128)(2,1)} custom-call(s32[4]{0:T(128)} %pad_add_fusion.place, bf16[512,256]{1,0:T(8,128)(2,1)} %get-tuple-element.20.pool_input, bf16[8,256]{1,0:T(8,128)(2,1)} %copy-done.8, bf16[8,256]{1,0:T(8,128)(2,1)} %copy-done.9, bf16[4,256,256]{2,1,0:T(8,128)(2,1)} %group_map.1), custom_call_target="tpu_custom_call" | custom-call | flops 67108864 | bytes 1000000 | tf_op jit(solution)/shard_map/pallas_call | solution.py:37
  171.4 2.6 %shard_map.133 = bf16[4,128,512]{2,1,0:T(8,128)(2,1)} custom-call(f32[512,256]{1,0:T(8,128)} %get-tuple-element.17.part, bf16[512,256]{1,0:T(8,128)(2,1)} %get-tuple-element.18.query, f32[128,1,256]{2,1,0:T(1,128)} %copy-done.5, bf16[512,256]{1,0:T(8,128)(2,1)} %shard_map.132.pooled), custom_call_target="tpu_custom_call" | custom-call | flops 100000000 | bytes 2000000 | tf_op jit(solution)/shard_map/pallas_call | solution.py:37
  174.0 14.4 %all_to_all.20.activations = bf16[4,128,512]{2,1,0:T(8,128)(2,1)} all-to-all(bf16[4,128,512]{2,1,0:T(8,128)(2,1)} %shard_map.133), channel_id=1, replica_groups=mesh['sp_0'=8,'sp_1'=8,'sp_2'=2,'tp'=4] {'tp'}, dimensions={0} | all-to-all | bytes 1048576 | tf_op jit(solution)/shard_map/all_to_all | solution.py:527
  188.4 8.8 %shard_map.134 = bf16[128,2048]{1,0:T(8,128)(2,1)} custom-call(s32[4]{0:T(128)} %pad_add_fusion.place, bf16[2048,2048]{1,0:T(8,128)(2,1)} %all-gather.2.cloned.1.call-done.weights, bf16[4,128,512]{2,1,0:T(8,128)(2,1)} %all_to_all.20.activations), custom_call_target="tpu_custom_call" | custom-call | flops 1073741824 | bytes 8388608 | tf_op jit(solution)/shard_map/pallas_call | solution.py:37
  (45 shorter events, 18.3 us)
Async XLA Ops:
  6.5 181.8 %all-gather.2.cloned.1.call-start = ((), (), s32[]{:S(2)}) async-start(), calls=%async_computation.4 | async-start | bytes 8454144 | tf_op jit(solution)/shard_map/all_gather | solution.py:451
  7.3 10.6 %collective-permute-start = (bf16[16,512]{1,0:T(8,128)(2,1)S(1)}, bf16[16,512]{1,0:T(8,128)(2,1)S(1)}, u32[]{:S(2)}, u32[]{:S(2)}) collective-permute-start(bf16[16,512]{1,0:T(8,128)(2,1)S(1)} %maximum_bitcast_fusion), channel_id=1, source_target_pairs={{0,1},{1,2},{2,3},{3,0},{4,5},{5,6},{6,7},{7,4},{8,9},{9,10},{10,1... | collective-permute-start | bytes 49160 | tf_op jit(solution)/shard_map/ppermute | solution.py:50
  10.4 7.4 %collective-permute-start.1 = (bf16[16,512]{1,0:T(8,128)(2,1)S(1)}, bf16[16,512]{1,0:T(8,128)(2,1)S(1)}, u32[]{:S(2)}, u32[]{:S(2)}) collective-permute-start(bf16[16,512]{1,0:T(8,128)(2,1)S(1)} %maximum_bitcast_fusion), channel_id=1, source_target_pairs={{0,2},{1,3},{2,0},{3,1},{4,6},{5,7},{6,4},{7,5},{8,10},{9,11},{10,... | collective-permute-start | bytes 49160 | tf_op jit(solution)/shard_map/ppermute | solution.py:50
  14.7 4.5 %collective-permute-start.2 = (bf16[16,512]{1,0:T(8,128)(2,1)S(1)}, bf16[16,512]{1,0:T(8,128)(2,1)S(1)}, u32[]{:S(2)}, u32[]{:S(2)}) collective-permute-start(bf16[16,512]{1,0:T(8,128)(2,1)S(1)} %maximum_bitcast_fusion), channel_id=1, source_target_pairs={{0,3},{1,0},{2,1},{3,2},{4,7},{5,4},{6,5},{7,6},{8,11},{9,8},{10,9... | collective-permute-start | bytes 49160 | tf_op jit(solution)/shard_map/ppermute | solution.py:50
  21.9 15.9 %copy-start.2 = (bf16[128,2048]{1,0:T(8,128)(2,1)S(1)}, bf16[128,2048]{1,0:T(8,128)(2,1)}, u32[]{:S(2)}) copy-start(bf16[128,2048]{1,0:T(8,128)(2,1)} %param.13) | copy-start | bytes 1572868
  21.9 54.4 %all-to-all-start = ((bf16[64,16,768]{2,1,0:T(8,128)(2,1)}), bf16[64,16,768]{2,1,0:T(8,128)(2,1)S(1)}, u32[]{:S(2)}, u32[]{:S(2)}) async-start(bf16[64,16,768]{2,1,0:T(8,128)(2,1)} %broadcast_in_dim.4), calls=%async_computation | async-start | bytes 3145728 | tf_op jit(solution)/shard_map/all_to_all | solution.py:440
  76.3 40.9 %copy-start = (bf16[64,16,768]{2,1,0:T(8,128)(2,1)}, bf16[64,16,768]{2,1,0:T(8,128)(2,1)S(1)}, u32[]{:S(2)}) copy-start(bf16[64,16,768]{2,1,0:T(8,128)(2,1)S(1)} %all-to-all-done.weight_own) | copy-start | bytes 4718596
  76.3 40.9 %collective-permute-start.3 = (bf16[64,16,768]{2,1,0:T(8,128)(2,1)S(1)}, bf16[64,16,768]{2,1,0:T(8,128)(2,1)S(1)}, u32[]{:S(2)}, u32[]{:S(2)}) collective-permute-start(bf16[64,16,768]{2,1,0:T(8,128)(2,1)S(1)} %all-to-all-done.weight_own), channel_id=1, source_target_pairs={{0,4},{4,0},{1,5},{5,1},{2,6},{6,2},{3,7},{7,3},{8,12},{12,8},{9,1... | collective-permute-start | bytes 4718600 | tf_op jit(solution)/shard_map/ppermute | solution.py:50
  84.2 1.9 copy-start.4
  84.2 16.6 %collective-permute-start.4 = (bf16[128,2048]{1,0:T(8,128)(2,1)S(1)}, bf16[128,2048]{1,0:T(8,128)(2,1)S(1)}, u32[]{:S(2)}, u32[]{:S(2)}) collective-permute-start(bf16[128,2048]{1,0:T(8,128)(2,1)S(1)} %fusion.1.own), channel_id=1, source_target_pairs={{0,1},{1,2},{2,3},{3,0},{4,5},{5,6},{6,7},{7,4},{8,9},{9,10},{10,1... | collective-permute-start | bytes 1572872 | tf_op jit(solution)/shard_map/ppermute | solution.py:50
  86.1 16.6 %collective-permute-start.5 = (bf16[128,2048]{1,0:T(8,128)(2,1)S(1)}, bf16[128,2048]{1,0:T(8,128)(2,1)S(1)}, u32[]{:S(2)}, u32[]{:S(2)}) collective-permute-start(bf16[128,2048]{1,0:T(8,128)(2,1)S(1)} %fusion.1.own), channel_id=1, source_target_pairs={{0,3},{1,0},{2,1},{3,2},{4,7},{5,4},{6,5},{7,6},{8,11},{9,8},{10,9... | collective-permute-start | bytes 1572872 | tf_op jit(solution)/shard_map/ppermute | solution.py:50
  100.7 2.0 copy-start.6
  100.8 10.2 %collective-permute-start.6 = (bf16[64,2048]{1,0:T(8,128)(2,1)S(1)}, bf16[64,2048]{1,0:T(8,128)(2,1)}, u32[]{:S(2)}, u32[]{:S(2)}) collective-permute-start(bf16[64,2048]{1,0:T(8,128)(2,1)S(1)} %slice.16), channel_id=1, source_target_pairs={{0,1},{1,2},{2,3},{3,0},{4,5},{5,6},{6,7},{7,4},{8,9},{9,10},{10,1... | collective-permute-start | bytes 786440 | tf_op jit(solution)/shard_map/ppermute | solution.py:50
  102.7 0.9 copy-start.7
  103.6 9.4 %collective-permute-start.7 = (bf16[64,2048]{1,0:T(8,128)(2,1)}, bf16[64,2048]{1,0:T(8,128)(2,1)}, u32[]{:S(2)}, u32[]{:S(2)}) collective-permute-start(bf16[64,2048]{1,0:T(8,128)(2,1)} %slice.17), channel_id=1, source_target_pairs={{0,3},{1,0},{2,1},{3,2},{4,7},{5,4},{6,5},{7,6},{8,11},{9,8},{10,9... | collective-permute-start | bytes 786440 | tf_op jit(solution)/shard_map/ppermute | solution.py:50
  117.2 1.2 copy-start.1
  123.9 21.2 %all-to-all-start.1 = ((f32[128,1,384]{2,1,0:T(1,128)}), f32[128,1,384]{2,1,0:T(1,128)S(1)}, u32[]{:S(2)}, u32[]{:S(2)}) async-start(f32[128,1,384]{2,1,0:T(1,128)} %get-tuple-element.19), calls=%async_computation.1 | async-start | bytes 393216 | tf_op jit(solution)/shard_map/all_to_all | solution.py:485
  145.0 0.7 copy-start.3
  148.1 22.7 %all-to-all-start.2 = ((f32[128,1,256]{2,1,0:T(1,128)}), f32[128,1,256]{2,1,0:T(1,128)S(1)}, u32[]{:S(2)}, u32[]{:S(2)}) async-start(f32[128,1,256]{2,1,0:T(1,128)} %shard_map.131), calls=%async_computation.2 | async-start | bytes 262144 | tf_op jit(solution)/shard_map/all_to_all | solution.py:511
  156.9 9.8 %collective-permute-start.8 = (bf16[8,256]{1,0:T(8,128)(2,1)S(1)}, bf16[8,256]{1,0:T(8,128)(2,1)S(1)}, u32[]{:S(2)}, u32[]{:S(2)}) collective-permute-start(bf16[8,256]{1,0:T(8,128)(2,1)S(1)} %get-tuple-element.22), channel_id=1, source_target_pairs={{0,4},{4,8},{8,12},{12,16},{16,20},{20,24},{24,28},{28,32},{32,36}... | collective-permute-start | bytes 12296 | tf_op jit(solution)/shard_map/ppermute | solution.py:56
  161.5 6.1 %collective-permute-start.9 = (bf16[8,256]{1,0:T(8,128)(2,1)S(1)}, bf16[8,256]{1,0:T(8,128)(2,1)S(1)}, u32[]{:S(2)}, u32[]{:S(2)}) collective-permute-start(bf16[8,256]{1,0:T(8,128)(2,1)S(1)} %get-tuple-element.21), channel_id=1, source_target_pairs={{4,0},{8,4},{12,8},{16,12},{20,16},{24,20},{28,24},{32,28},{36,32}... | collective-permute-start | bytes 12296 | tf_op jit(solution)/shard_map/ppermute | solution.py:56
  166.7 1.0 copy-start.8
  167.6 0.6 copy-start.9
  170.7 0.6 copy-start.5
Sparse Core Ops, SparseCore 0:
  20.0 114.7 all-gather.1

commit v6 on v4

--- a/solution.py
+++ b/solution.py
@@ -14,6 +14,7 @@
 LANES = 128
 SP = ("sp_0", "sp_1", "sp_2")
 CHIPS = ("sp_0", "sp_1")
+GROUP = ("sp_1", "sp_2")
 SP_TP = ("sp_0", "sp_1", "sp_2", "tp")
 
 eps_value = 1e-06
@@ -23,7 +24,6 @@
 
 bf16 = jnp.bfloat16
 f32 = jnp.float32
-exact = lax.Precision.HIGHEST
 
 
 def matmul(a, b, dims=((1,), (0,)), precision=None):
@@ -102,7 +102,7 @@
     tp = place[0]
     place_tokens(tp, (own, before, after, far_top, far_end), tokens_out, 0)
     rows = tokens_out.shape[0]
-    low_rank = matmul(tokens_out[...], inner[...]).astype(bf16)
+    low_rank = matmul(tokens_out[...], inner[...], ((1,), (1,))).astype(bf16)
     here = pl.ds(pl.multiple_of(tp * LANES, LANES), LANES)
     blank = jnp.zeros((RANK, LANES), bf16)
     outer_both = jnp.concatenate(
@@ -116,7 +116,8 @@
     pre = matmul(low_rank, outer_both) + bias_both
     gate = jnp.minimum(pre, 0.0) - jnp.log1p(jnp.exp(-jnp.abs(pre)))
     lane = lax.broadcasted_iota(jnp.int32, (rows, LANES), 1)
-    spikes = jnp.where(lane < KEY_CHANNELS, spike[:, 0:1], spike[:, 1:2])
+    spike_rows = jnp.concatenate([spike[...], jnp.zeros((6, rows), f32)], axis=0).T
+    spikes = jnp.where(lane < KEY_CHANNELS, spike_rows[:, 0:1], spike_rows[:, 1:2])
     decay = gate * (1.0 / gate_norm_factor) + jnp.concatenate([spikes, spikes], axis=1)
     size = LANES
     row_ids = lax.broadcasted_iota(jnp.int32, (size, size), 0)
@@ -145,74 +146,91 @@
     qkv_out,
     pool_out,
     packed_out,
+    tokens_ref,
     weight_ref,
     sems,
 ):
     core = place[1]
-    load_own = pltpu.make_async_copy(weight_own, weight_ref.at[:, core], sems.at[0])
-    load_other = pltpu.make_async_copy(weight_other, weight_ref.at[:, 1 - core], sems.at[1])
-    load_own.start()
-    load_other.start()
-    rows, width = tokens.shape
+    loads = (
+        pltpu.make_async_copy(tokens, tokens_ref, sems.at[0]),
+        pltpu.make_async_copy(weight_own, weight_ref.at[:, core], sems.at[1]),
+        pltpu.make_async_copy(weight_other, weight_ref.at[:, 1 - core], sems.at[2]),
+    )
+    for load in loads:
+        load.start()
+    rows, width = tokens_ref.shape
     total_fwd = logs[0, rows - 1 : rows, :]
     total_bwd = logs[1, 0:1, :]
-    load_own.wait()
-    load_other.wait()
-    projected = matmul(tokens[...], weight_ref[...].reshape(width, -1)).astype(bf16)
+    far_fwd = jnp.exp(total_fwd - logs[0])
+    far_bwd = jnp.exp(total_bwd - logs[1])
+    totals = jnp.concatenate([total_fwd, total_bwd], axis=0)
+    high = totals.astype(bf16).astype(f32)
+    stacked = jnp.concatenate([high, totals - high, jnp.zeros((LANES - 4, LANES), f32)], axis=0)
+    packed_out[:, 2 * LANES :] = stacked.T.astype(bf16)
+    for load in loads:
+        load.wait()
+    projected = matmul(tokens_ref[...], weight_ref[...].reshape(width, -1)).astype(bf16)
     qkv = projected[:, : 4 * LANES]
     qkv_out[...] = qkv
     pool_out[...] = projected[:, 4 * LANES :]
     keys = qkv[:, LANES : 2 * LANES].astype(f32)
     weighted = jnp.concatenate(
-        [
-            (keys * jnp.exp(total_fwd - logs[0])).astype(bf16),
-            (keys * jnp.exp(total_bwd - logs[1])).astype(bf16),
-        ],
-        axis=1,
+        [(keys * far_fwd).astype(bf16), (keys * far_bwd).astype(bf16)], axis=1
     )
     updates = matmul(weighted, qkv[:, 2 * LANES :], ((0,), (0,)))
     first = lax.broadcasted_iota(jnp.int32, (LANES, LANES), 0) < KEY_CHANNELS
     for d in range(2):
         mine = updates[d * LANES : (d + 1) * LANES]
-        packed_out[:, 0, d * LANES : (d + 1) * LANES] = jnp.where(
+        packed_out[:, d * LANES : (d + 1) * LANES] = jnp.where(
             first, mine[:, :LANES], mine[:, LANES:]
-        )
-    totals = jnp.concatenate([total_fwd, total_bwd], axis=0)
-    stacked = jnp.concatenate([totals, jnp.zeros((LANES - 2, LANES), f32)], axis=0)
-    packed_out[:, 0, 2 * LANES :] = stacked.T
-
-
-def scan_kernel(place, received, start, out):
-    devices = received.shape[0]
-    here = place[0]
-    logs = received[:, 0, 2 * LANES :]
-    row = lax.broadcasted_iota(jnp.int32, (devices, devices), 0)
-    col = lax.broadcasted_iota(jnp.int32, (devices, devices), 1)
-    earlier = (col < row).astype(f32)
-    upto = (row <= col).astype(f32)
-    strictly = (row < col).astype(f32)
-    before_col = matmul(earlier, logs, precision=exact)
-    before_row = matmul(logs, strictly, ((0,), (0,)), precision=exact)
-    past_row = matmul(logs, upto, ((0,), (0,)), precision=exact)
-    past_col = before_col + logs
-    total = jnp.sum(logs, axis=0, keepdims=True)
-    for r in range(2):
-        if r == 0:
-            between = before_col[:, 0:1] - past_row[0:1, :]
-            allowed = col < row
-            outside = before_col[:, 0:1]
-        else:
-            between = before_row[1:2, :] - past_col[:, 1:2]
-            allowed = col > row
-            outside = total[:, 1:2] - past_col[:, 1:2]
-        weights = jnp.where(allowed, jnp.exp(jnp.minimum(between, 0.0)), 0.0)
-        high = weights.astype(bf16)
-        low = (weights - high.astype(f32)).astype(bf16)
-        updates = received[:, 0, r * LANES : (r + 1) * LANES].astype(bf16)
-        first = start[r, pl.ds(here, 1), :]
-        entering = matmul(high, updates) + matmul(low, updates)
-        entering = entering + jnp.exp(jnp.minimum(outside, 0.0)) * first
-        out[:, 0, r * LANES : (r + 1) * LANES] = entering
+        ).astype(bf16)
+
+
+def decays_of(tile):
+    edge = tile[:, 2 * LANES :].astype(f32)
+    return [edge[:, d : d + 1] + edge[:, d + 2 : d + 3] for d in range(2)]
+
+
+def updates_of(tile):
+    return [tile[:, d * LANES : (d + 1) * LANES].astype(f32) for d in range(2)]
+
+
+def total_kernel(received, out):
+    members, rows = received.shape[:2]
+    orders = (range(members), reversed(range(members)))
+    lane = lax.broadcasted_iota(jnp.int32, (rows, LANES), 1)
+    edge = jnp.zeros((rows, LANES), f32)
+    for d, order in enumerate(orders):
+        state = jnp.zeros((rows, LANES), f32)
+        total = jnp.zeros((rows, 1), f32)
+        for n in order:
+            tile = received[n]
+            log = decays_of(tile)[d]
+            state = jnp.exp(log) * state + updates_of(tile)[d]
+            total = total + log
+        high = total.astype(bf16).astype(f32)
+        edge = jnp.where(lane == d, high, jnp.where(lane == d + 2, total - high, edge))
+        out[:, d * LANES : (d + 1) * LANES] = state.astype(bf16)
+    out[:, 2 * LANES :] = edge.astype(bf16)
+
+
+def scan_kernel(place, received, totals, start, out):
+    layer, member = (place[4], place[5])
+    members, rows = received.shape[:2]
+    layers = totals.shape[0]
+    here = pl.ds(pl.multiple_of(member * rows, rows), rows)
+    for d in range(2):
+        turn = list if d == 0 else (lambda r: list(reversed(r)))
+        state = start[d, here, :]
+        for n in turn(range(layers)):
+            tile = totals[n]
+            passed = (n < layer) if d == 0 else (n > layer)
+            moved = jnp.exp(decays_of(tile)[d]) * state + updates_of(tile)[d]
+            state = jnp.where(passed, moved, state)
+        for n in turn(range(members)):
+            out[n, :, d * LANES : (d + 1) * LANES] = state.astype(bf16)
+            tile = received[n]
+            state = jnp.exp(decays_of(tile)[d]) * state + updates_of(tile)[d]
 
 
 def inner_kernel(qkv, logs, part_out, query_out):
@@ -324,7 +342,7 @@
     zero = jnp.zeros((), bf16)
     sides = []
     for d in range(2):
-        state = entering[:, 0, d * LANES : (d + 1) * LANES].astype(bf16)
+        state = entering[:, d * LANES : (d + 1) * LANES]
         sides.append(
             jnp.concatenate(
                 [jnp.where(channel_one, state, zero), jnp.where(channel_one, zero, state)], axis=1
@@ -346,45 +364,40 @@
             start += piece.shape[1]
 
 
-def output_kernel(place, activations, weight, out, total):
-    groups = activations.shape[0]
-    step, part = (pl.program_id(0), pl.program_id(1))
-    tile = weight.shape[0]
-    here = pl.ds(pl.multiple_of(part * tile, tile), tile)
-    source = lax.rem(place[0] + groups - step, groups)
-    partial = matmul(weight[...], activations[source], ((1,), (1,))).astype(bf16).astype(f32)
-
-    @pl.when(step == 0)
-    def _():
-        total[here, :] = partial
-
-    @pl.when(step > 0)
-    def _():
-        total[here, :] += partial
-
-    @pl.when(step == groups - 1)
-    def _():
-        out[:, here] = total[here, :].T.astype(bf16)
+def output_kernel(place, weights, activations, out, weight_ref, sems):
+    groups, _, width = activations.shape
+    pieces = sems.shape[0]
+    tile = weights.shape[0] // pieces
+    loads = []
+    for n in range(pieces):
+        here = slice(n * tile, (n + 1) * tile)
+        loads.append(pltpu.make_async_copy(weights.at[here], weight_ref.at[here], sems.at[n]))
+        loads[n].start()
+    mine = [activations[lax.rem(place[0] + groups - s, groups)] for s in range(groups)]
+    for n in range(pieces):
+        here = slice(n * tile, (n + 1) * tile)
+        loads[n].wait()
+        total = None
+        for s in range(groups):
+            block = weight_ref[here, s * width : (s + 1) * width]
+            partial = matmul(mine[s], block, ((1,), (1,))).astype(bf16).astype(f32)
+            total = partial if total is None else total + partial
+        out[:, here] = total.astype(bf16)
 
 
 def output_projection(place, activations, weights):
     groups, rows, width = activations.shape
     model = weights.shape[0]
-    parts = 2
-    return pl.pallas_call(
+    pieces = 8
+    return call(
         output_kernel,
-        grid=(groups, parts),
-        in_specs=[
-            pl.BlockSpec(memory_space=pltpu.SMEM),
-            pl.BlockSpec((groups, rows, width), lambda s, n: (0, 0, 0)),
-            pl.BlockSpec((model // parts, width), lambda s, n: (n, s)),
-        ],
-        out_specs=pl.BlockSpec((rows, model), lambda s, n: (0, 0)),
-        out_shape=jax.ShapeDtypeStruct((rows, model), bf16),
-        scratch_shapes=[pltpu.VMEM((model, rows), f32)],
-        interpret=interpreted,
-        name="output_kernel",
-    )(place, activations, weights)
+        shape_of(rows, model),
+        (place, weights, activations),
+        far=1,
+        scratch=(pltpu.VMEM((model, groups * width), bf16), pltpu.SemaphoreType.DMA((pieces,))),
+        flops=2 * rows * model * groups * width,
+        moved=2 * model * groups * width,
+    )
 
 
 def shape_of(*lengths, kind=bf16):
@@ -410,7 +423,10 @@
     tp_index = lax.axis_index("tp")
     core = lax.axis_index("sp_2")
     positions = lax.axis_size(SP)
-    place = jnp.stack([tp_index, core, sp_index, jnp.int32(positions)]).astype(jnp.int32)
+    layer, member = (lax.axis_index("sp_0"), lax.axis_index(GROUP))
+    layers, members = (lax.axis_size("sp_0"), lax.axis_size(GROUP))
+    place = jnp.stack([tp_index, core, sp_index, jnp.int32(positions), layer, member])
+    place = place.astype(jnp.int32)
     groups = lax.axis_size("tp")
     rows = tokens.shape[0] * groups
     model = tokens.shape[1]
@@ -443,10 +459,10 @@
             after,
             far_top,
             far_end,
-            decay_inner_weight,
+            decay_inner_weight.T,
             decay_outer_weight,
             channel_decay_bias,
-            spike_log_decay.T,
+            spike_log_decay,
         ),
         flops=2 * rows * model * 4 * LANES,
         moved=5_000_000,
@@ -456,20 +472,35 @@
         (
             shape_of(rows, 4 * LANES),
             shape_of(rows, 2 * LANES),
-            shape_of(LANES, 1, 3 * LANES, kind=f32),
+            shape_of(LANES, 3 * LANES),
         ),
         (place, weight_own, weight_other, all_tokens, logs),
-        far=2,
+        far=3,
         scratch=(
+            pltpu.VMEM((rows, model), bf16),
             pltpu.VMEM((chips, 2, model // (2 * chips), 6 * LANES), bf16),
-            pltpu.SemaphoreType.DMA((2,)),
+            pltpu.SemaphoreType.DMA((3,)),
         ),
         flops=2 * rows * model * 7 * LANES,
         moved=8_000_000,
     )
-    received = lax.all_to_all(packed, SP, 0, 0, tiled=True)
-    rim_before = neighbours(pool_input[rows - rim_width :], SP, 1)
-    rim_after = neighbours(pool_input[:rim_width], SP, -1)
+    packed = packed.reshape(members, LANES // members, 3 * LANES)
+    received = lax.all_to_all(packed, GROUP, 0, 0, tiled=True)
+    totals = call(
+        total_kernel, shape_of(*packed.shape[1:]), (received,), scalars=0, flops=1_000_000
+    )
+    copies = jnp.broadcast_to(totals, (layers, *totals.shape))
+    totals = lax.all_to_all(copies, "sp_0", 0, 0, tiled=True)
+    states = call(
+        scan_kernel,
+        shape_of(members, LANES // members, 2 * LANES),
+        (place, received, totals, starting_state.reshape(2, -1, DV)),
+        flops=1_000_000,
+    )
+    entering = lax.all_to_all(states, GROUP, 0, 0, tiled=True).reshape(LANES, 2 * LANES)
+    last, leading = (pool_input[rows - rim_width :], pool_input[:rim_width])
+    rim_before = neighbours(last, SP, 1)
+    rim_after = neighbours(leading, SP, -1)
     part, query = call(
         inner_kernel,
         (shape_of(rows, 2 * DV, kind=f32), shape_of(rows, 2 * LANES)),
@@ -478,13 +509,6 @@
         flops=2 * rows * model * 2 * LANES,
         moved=3_000_000,
     )
-    states = call(
-        scan_kernel,
-        shape_of(positions, 1, 2 * LANES, kind=f32),
-        (place[2:3], received, starting_state.reshape(2, -1, DV)),
-        flops=40_000_000,
-    )
-    entering = lax.all_to_all(states, SP, 0, 0, tiled=True)
     pooled = call(
         pool_kernel,
         shape_of(rows, 2 * LANES),

time: 202 us -> 204 us (level)
  blocking collectives: 35.5 us -> 38.2 us
  waiting for transfers between devices: 52.6 us -> 54.7 us
    pallas_call x1 -> x0, Pallas kernels: 8.77 us -> none  [output_projection(): pl.pallas_call(output_kernel, grid=(groups, parts), in_specs=[pl.BlockSpe...]
    pallas_call x6 -> x8, Pallas kernels: 21.3 us -> 29.3 us  [call(): pl.pallas_call(kernel, in_specs=[smem] * scalars + [anywhere] * far + [vm...]
    all_to_all x1 -> x2, blocking collectives: 20.8 us -> 23.6 us  [the longest x1 13.5 us: shards(): received = lax.all_to_all(packed, GROUP, 0, 0, tiled=True)]
  transfers between devices with their start and end apart: 13 -> 13, of which waited for: 6 -> 6; matrix products, arithmetic and copies ran while one was open for 3% -> 2% of each run, Pallas kernels for 11% -> 11%
where the time goes in v6:
time: 204 us; the launch traced here: 203 us
  starting transfers between devices  59.8 us (29%)
  waiting for transfers between devices  54.7 us (27%)
  blocking collectives  38.2 us (19%)
  Pallas kernels  29.3 us (14%)
  between operations  13.6 us (7%)
  local copies, waits for them, and re-layouts  4.56 us (2%)
  other arithmetic  2.43 us (1%)
    all_to_all x1, waiting for transfers between devices, shards(): weight_own = lax.all_to_all(copies, CHIPS, 0, 0, tiled=True)  38.3 us
    ppermute x8, starting transfers between devices, shifted(): lax.ppermute(value, axis, [(i, (i + step) % devices) for i in range(devic...  30.2 us
    pallas_call x8, Pallas kernels, call(): pl.pallas_call(kernel, in_specs=[smem] * scalars + [anywhere] * far + [vm...  29.3 us
    all_to_all x1, starting transfers between devices, shards(): weight_own = lax.all_to_all(copies, CHIPS, 0, 0, tiled=True)  15.9 us
    ppermute x8, waiting for transfers between devices, shifted(): lax.ppermute(value, axis, [(i, (i + step) % devices) for i in range(devic...  15.3 us
    all_to_all x1, blocking collectives, shards(): gathered = lax.all_to_all(activations, 'tp', 0, 0, tiled=True)  14.6 us
    all_to_all x1, blocking collectives, shards(): received = lax.all_to_all(packed, GROUP, 0, 0, tiled=True)  13.5 us
    all_to_all x1, blocking collectives, shards(): totals = lax.all_to_all(copies, 'sp_0', 0, 0, tiled=True)  10.1 us
  transfers between devices with their start and end apart: 13, of which 6 were waited for; matrix products, arithmetic and copies ran while one was open for 2% of the time, Pallas kernels for 11%

profile of v6, /device:TPU:25, one launch (start us, length us, event | category | flops | bytes accessed | tf_op | source)
XLA Modules:
  0.0 202.6 jit_solution(15159461552353081724)
XLA Ops:
  7.3 3.1 %collective-permute-start = (bf16[16,512]{1,0:T(8,128)(2,1)S(1)}, bf16[16,512]{1,0:T(8,128)(2,1)S(1)}, u32[]{:S(2)}, u32[]{:S(2)}) collective-permute-start(bf16[16,512]{1,0:T(8,128)(2,1)S(1)} %maximum_bitcast_fusion), channel_id=1, source_target_pairs={{0,1},{1,2},{2,3},{3,0},{4,5},{5,6},{6,7},{7,4},{8,9},{9,10},{10,1... | collective-permute-start | bytes 49160 | tf_op jit(solution)/shard_map/ppermute | solution.py:51
  10.4 4.4 %collective-permute-start.1 = (bf16[16,512]{1,0:T(8,128)(2,1)S(1)}, bf16[16,512]{1,0:T(8,128)(2,1)S(1)}, u32[]{:S(2)}, u32[]{:S(2)}) collective-permute-start(bf16[16,512]{1,0:T(8,128)(2,1)S(1)} %maximum_bitcast_fusion), channel_id=1, source_target_pairs={{0,2},{1,3},{2,0},{3,1},{4,6},{5,7},{6,4},{7,5},{8,10},{9,11},{10,... | collective-permute-start | bytes 49160 | tf_op jit(solution)/shard_map/ppermute | solution.py:51
  14.7 3.1 %collective-permute-start.2 = (bf16[16,512]{1,0:T(8,128)(2,1)S(1)}, bf16[16,512]{1,0:T(8,128)(2,1)S(1)}, u32[]{:S(2)}, u32[]{:S(2)}) collective-permute-start(bf16[16,512]{1,0:T(8,128)(2,1)S(1)} %maximum_bitcast_fusion), channel_id=1, source_target_pairs={{0,3},{1,0},{2,1},{3,2},{4,7},{5,4},{6,5},{7,6},{8,11},{9,8},{10,9... | collective-permute-start | bytes 49160 | tf_op jit(solution)/shard_map/ppermute | solution.py:51
  21.9 15.9 %all-to-all-start = ((bf16[64,16,768]{2,1,0:T(8,128)(2,1)}), bf16[64,16,768]{2,1,0:T(8,128)(2,1)S(1)}, u32[]{:S(2)}, u32[]{:S(2)}) async-start(bf16[64,16,768]{2,1,0:T(8,128)(2,1)} %broadcast_in_dim.7), calls=%async_computation | async-start | bytes 3145728 | tf_op jit(solution)/shard_map/all_to_all | solution.py:439
  38.0 38.3 %all-to-all-done.weight_own = bf16[64,16,768]{2,1,0:T(8,128)(2,1)S(1)} async-done(((bf16[64,16,768]{2,1,0:T(8,128)(2,1)}), bf16[64,16,768]{2,1,0:T(8,128)(2,1)S(1)}, u32[]{:S(2)}, u32[]{:S(2)}) %all-to-all-start) | async-done | bytes 1572896 | tf_op jit(solution)/shard_map/all_to_all | solution.py:439
  76.3 6.6 %collective-permute-start.3 = (bf16[64,16,768]{2,1,0:T(8,128)(2,1)S(1)}, bf16[64,16,768]{2,1,0:T(8,128)(2,1)}, u32[]{:S(2)}, u32[]{:S(2)}) collective-permute-start(bf16[64,16,768]{2,1,0:T(8,128)(2,1)S(1)} %all-to-all-done.weight_own), channel_id=1, source_target_pairs={{0,4},{4,0},{1,5},{5,1},{2,6},{6,2},{3,7},{7,3},{8,12},{12,8},{9,1... | collective-permute-start | bytes 4718600 | tf_op jit(solution)/shard_map/ppermute | solution.py:51
  83.2 1.9 collective-permute-start.4
  85.1 4.6 %collective-permute-start.5 = (bf16[128,2048]{1,0:T(8,128)(2,1)S(1)}, bf16[128,2048]{1,0:T(8,128)(2,1)S(1)}, u32[]{:S(2)}, u32[]{:S(2)}) collective-permute-start(bf16[128,2048]{1,0:T(8,128)(2,1)S(1)} %fusion.1.own), channel_id=1, source_target_pairs={{0,3},{1,0},{2,1},{3,2},{4,7},{5,4},{6,5},{7,6},{8,11},{9,8},{10,9... | collective-permute-start | bytes 1572872 | tf_op jit(solution)/shard_map/ppermute | solution.py:51
  89.7 10.1 %collective-permute-done.4.before = bf16[128,2048]{1,0:T(8,128)(2,1)S(1)} collective-permute-done((bf16[128,2048]{1,0:T(8,128)(2,1)S(1)}, bf16[128,2048]{1,0:T(8,128)(2,1)S(1)}, u32[]{:S(2)}, u32[]{:S(2)}) %collective-permute-start.4) | collective-permute-done | bytes 524320 | tf_op jit(solution)/shard_map/ppermute | solution.py:51
  99.8 1.9 collective-permute-start.6
  101.7 4.6 %collective-permute-start.7 = (bf16[64,2048]{1,0:T(8,128)(2,1)S(1)}, bf16[64,2048]{1,0:T(8,128)(2,1)}, u32[]{:S(2)}, u32[]{:S(2)}) collective-permute-start(bf16[64,2048]{1,0:T(8,128)(2,1)S(1)} %slice.17), channel_id=1, source_target_pairs={{0,3},{1,0},{2,1},{3,2},{4,7},{5,4},{6,5},{7,6},{8,11},{9,8},{10,9... | collective-permute-start | bytes 786440 | tf_op jit(solution)/shard_map/ppermute | solution.py:51
  107.0 2.9 %collective-permute-done.6.far_top = bf16[64,2048]{1,0:T(8,128)(2,1)S(1)} collective-permute-done((bf16[64,2048]{1,0:T(8,128)(2,1)S(1)}, bf16[64,2048]{1,0:T(8,128)(2,1)S(1)}, u32[]{:S(2)}, u32[]{:S(2)}) %collective-permute-start.6) | collective-permute-done | bytes 262176 | tf_op jit(solution)/shard_map/ppermute | solution.py:51
  110.8 4.3 %shard_map.127 = (bf16[512,2048]{1,0:T(8,128)(2,1)}, f32[2,512,128]{2,1,0:T(8,128)}) custom-call(s32[6]{0:T(128)} %stack.23.place, bf16[128,2048]{1,0:T(8,128)(2,1)} %copy-done.2, bf16[128,2048]{1,0:T(8,128)(2,1)} %copy-done.4, bf16[128,2048]{1,0:T(8,128)(2,1)} %copy-done.5, bf16[64,2048]{1,0:T(8,128)(2,1)} %copy-done.8, ...), custom_call_target="tpu_custom_call" | custom-call | flops 1073741824 | bytes 5000000 | tf_op jit(solution)/shard_map/pallas_call | solution.py:38
  115.1 6.5 %shard_map.128 = (bf16[512,512]{1,0:T(8,128)(2,1)}, bf16[512,256]{1,0:T(8,128)(2,1)}, bf16[128,384]{1,0:T(8,128)(2,1)}) custom-call(s32[6]{0:T(128)} %stack.23.place, bf16[64,16,768]{2,1,0:T(8,128)(2,1)} %copy-done.1, bf16[64,16,768]{2,1,0:T(8,128)(2,1)} %collective-permute-done.3.weight_other, bf16[512,2048]{1,0:T(8,128)(2,1)} %get-tuple-element.12.tokens, ...), custom_call_target="tpu_custom_call" | custom-call | flops 1879048192 | bytes 8000000 | tf_op jit(solution)/shard_map/pallas_call | solution.py:38
  121.6 13.5 %all_to_all.25.received = bf16[16,8,384]{2,1,0:T(8,128)(2,1)} all-to-all(bf16[16,8,384]{2,1,0:T(8,128)(2,1)} %bitcast.13), channel_id=1, replica_groups=mesh['sp_0'=8,'sp_1'=8,'sp_2'=2,'tp'=4] {'sp_1','sp_2'}, dimensions={0} | all-to-all | bytes 196608 | tf_op jit(solution)/shard_map/all_to_all | solution.py:488
  137.5 10.1 %all_to_all.26.totals = bf16[8,8,384]{2,1,0:T(8,128)(2,1)} all-to-all(bf16[8,8,384]{2,1,0:T(8,128)(2,1)S(1)} %broadcast_in_dim.8), channel_id=1, replica_groups=mesh['sp_0'=8,'sp_1'=8,'sp_2'=2,'tp'=4] {'sp_0'}, dimensions={0} | all-to-all | bytes 98304 | tf_op jit(solution)/shard_map/all_to_all | solution.py:493
  149.4 7.3 %all-to-all-start.3 = ((bf16[16,8,256]{2,1,0:T(8,128)(2,1)}), bf16[16,8,256]{2,1,0:T(8,128)(2,1)S(1)}, u32[]{:S(2)}, u32[]{:S(2)}) async-start(bf16[16,8,256]{2,1,0:T(8,128)(2,1)} %shard_map.131), calls=%async_computation.3 | async-start | bytes 131072 | tf_op jit(solution)/shard_map/all_to_all | solution.py:500
  157.4 4.6 %collective-permute-start.8 = (bf16[8,256]{1,0:T(8,128)(2,1)S(1)}, bf16[8,256]{1,0:T(8,128)(2,1)S(1)}, u32[]{:S(2)}, u32[]{:S(2)}) collective-permute-start(bf16[8,256]{1,0:T(8,128)(2,1)S(1)} %get-tuple-element.20), channel_id=1, source_target_pairs={{0,4},{4,8},{8,12},{12,16},{16,20},{20,24},{24,28},{28,32},{32,36}... | collective-permute-start | bytes 12296 | tf_op jit(solution)/shard_map/ppermute | solution.py:57
  162.0 1.9 collective-permute-start.9
  163.9 3.1 %shard_map.129 = (f32[512,256]{1,0:T(8,128)}, bf16[512,256]{1,0:T(8,128)(2,1)}) custom-call(bf16[512,512]{1,0:T(8,128)(2,1)} %get-tuple-element.14.qkv, f32[2,512,128]{2,1,0:T(8,128)} %get-tuple-element.13.logs), custom_call_target="tpu_custom_call" | custom-call | flops 536870912 | bytes 3000000 | tf_op jit(solution)/shard_map/pallas_call | solution.py:38
  168.7 2.5 %shard_map.132.pooled = bf16[512,256]{1,0:T(8,128)(2,1)} custom-call(s32[6]{0:T(128)} %stack.23.place, bf16[512,256]{1,0:T(8,128)(2,1)} %get-tuple-element.18.pool_input, bf16[8,256]{1,0:T(8,128)(2,1)} %copy-done.6, bf16[8,256]{1,0:T(8,128)(2,1)} %copy-done.7, bf16[4,256,256]{2,1,0:T(8,128)(2,1)} %group_map.1), custom_call_target="tpu_custom_call" | custom-call | flops 67108864 | bytes 1000000 | tf_op jit(solution)/shard_map/pallas_call | solution.py:38
  171.8 2.4 %shard_map.133 = bf16[4,128,512]{2,1,0:T(8,128)(2,1)} custom-call(f32[512,256]{1,0:T(8,128)} %get-tuple-element.15.part, bf16[512,256]{1,0:T(8,128)(2,1)} %get-tuple-element.16.query, bf16[128,256]{1,0:T(8,128)(2,1)} %bitcast.11, bf16[512,256]{1,0:T(8,128)(2,1)} %shard_map.132.pooled), custom_call_target="tpu_custom_call" | custom-call | flops 100000000 | bytes 2000000 | tf_op jit(solution)/shard_map/pallas_call | solution.py:38
  174.2 14.6 %all_to_all.27.activations = bf16[4,128,512]{2,1,0:T(8,128)(2,1)} all-to-all(bf16[4,128,512]{2,1,0:T(8,128)(2,1)} %shard_map.133), channel_id=1, replica_groups=mesh['sp_0'=8,'sp_1'=8,'sp_2'=2,'tp'=4] {'tp'}, dimensions={0} | all-to-all | bytes 1048576 | tf_op jit(solution)/shard_map/all_to_all | solution.py:527
  188.8 6.9 %shard_map.134 = bf16[128,2048]{1,0:T(8,128)(2,1)} custom-call(s32[6]{0:T(128)} %stack.23.place, bf16[2048,2048]{1,0:T(8,128)(2,1)} %all-gather.2.cloned.1.call-done.weights, bf16[4,128,512]{2,1,0:T(8,128)(2,1)} %all_to_all.27.activations), custom_call_target="tpu_custom_call" | custom-call | flops 1073741824 | bytes 8388608 | tf_op jit(solution)/shard_map/pallas_call | solution.py:38
  (44 shorter events, 14.0 us)
Async XLA Ops:
  6.5 182.3 %all-gather.2.cloned.1.call-start = ((), (), s32[]{:S(2)}) async-start(), calls=%async_computation.5 | async-start | bytes 8454144 | tf_op jit(solution)/shard_map/all_gather | solution.py:450
  7.3 10.6 %collective-permute-start = (bf16[16,512]{1,0:T(8,128)(2,1)S(1)}, bf16[16,512]{1,0:T(8,128)(2,1)S(1)}, u32[]{:S(2)}, u32[]{:S(2)}) collective-permute-start(bf16[16,512]{1,0:T(8,128)(2,1)S(1)} %maximum_bitcast_fusion), channel_id=1, source_target_pairs={{0,1},{1,2},{2,3},{3,0},{4,5},{5,6},{6,7},{7,4},{8,9},{9,10},{10,1... | collective-permute-start | bytes 49160 | tf_op jit(solution)/shard_map/ppermute | solution.py:51
  10.4 7.4 %collective-permute-start.1 = (bf16[16,512]{1,0:T(8,128)(2,1)S(1)}, bf16[16,512]{1,0:T(8,128)(2,1)S(1)}, u32[]{:S(2)}, u32[]{:S(2)}) collective-permute-start(bf16[16,512]{1,0:T(8,128)(2,1)S(1)} %maximum_bitcast_fusion), channel_id=1, source_target_pairs={{0,2},{1,3},{2,0},{3,1},{4,6},{5,7},{6,4},{7,5},{8,10},{9,11},{10,... | collective-permute-start | bytes 49160 | tf_op jit(solution)/shard_map/ppermute | solution.py:51
  14.7 4.5 %collective-permute-start.2 = (bf16[16,512]{1,0:T(8,128)(2,1)S(1)}, bf16[16,512]{1,0:T(8,128)(2,1)S(1)}, u32[]{:S(2)}, u32[]{:S(2)}) collective-permute-start(bf16[16,512]{1,0:T(8,128)(2,1)S(1)} %maximum_bitcast_fusion), channel_id=1, source_target_pairs={{0,3},{1,0},{2,1},{3,2},{4,7},{5,4},{6,5},{7,6},{8,11},{9,8},{10,9... | collective-permute-start | bytes 49160 | tf_op jit(solution)/shard_map/ppermute | solution.py:51
  21.9 15.9 %copy-start = (bf16[128,2048]{1,0:T(8,128)(2,1)S(1)}, bf16[128,2048]{1,0:T(8,128)(2,1)}, u32[]{:S(2)}) copy-start(bf16[128,2048]{1,0:T(8,128)(2,1)} %param.13) | copy-start | bytes 1572868
  21.9 54.4 %all-to-all-start = ((bf16[64,16,768]{2,1,0:T(8,128)(2,1)}), bf16[64,16,768]{2,1,0:T(8,128)(2,1)S(1)}, u32[]{:S(2)}, u32[]{:S(2)}) async-start(bf16[64,16,768]{2,1,0:T(8,128)(2,1)} %broadcast_in_dim.7), calls=%async_computation | async-start | bytes 3145728 | tf_op jit(solution)/shard_map/all_to_all | solution.py:439
  76.3 38.8 %copy-start.1 = (bf16[64,16,768]{2,1,0:T(8,128)(2,1)}, bf16[64,16,768]{2,1,0:T(8,128)(2,1)S(1)}, u32[]{:S(2)}) copy-start(bf16[64,16,768]{2,1,0:T(8,128)(2,1)S(1)} %all-to-all-done.weight_own) | copy-start | bytes 4718596
  76.3 38.8 %collective-permute-start.3 = (bf16[64,16,768]{2,1,0:T(8,128)(2,1)S(1)}, bf16[64,16,768]{2,1,0:T(8,128)(2,1)}, u32[]{:S(2)}, u32[]{:S(2)}) collective-permute-start(bf16[64,16,768]{2,1,0:T(8,128)(2,1)S(1)} %all-to-all-done.weight_own), channel_id=1, source_target_pairs={{0,4},{4,0},{1,5},{5,1},{2,6},{6,2},{3,7},{7,3},{8,12},{12,8},{9,1... | collective-permute-start | bytes 4718600 | tf_op jit(solution)/shard_map/ppermute | solution.py:51
  83.2 27.7 %copy-start.2 = (bf16[128,2048]{1,0:T(8,128)(2,1)}, bf16[128,2048]{1,0:T(8,128)(2,1)S(1)}, u32[]{:S(2)}) copy-start(bf16[128,2048]{1,0:T(8,128)(2,1)S(1)} %fusion.1.own) | copy-start | bytes 1572868
  83.2 16.6 %collective-permute-start.4 = (bf16[128,2048]{1,0:T(8,128)(2,1)S(1)}, bf16[128,2048]{1,0:T(8,128)(2,1)S(1)}, u32[]{:S(2)}, u32[]{:S(2)}) collective-permute-start(bf16[128,2048]{1,0:T(8,128)(2,1)S(1)} %fusion.1.own), channel_id=1, source_target_pairs={{0,1},{1,2},{2,3},{3,0},{4,5},{5,6},{6,7},{7,4},{8,9},{9,10},{10,1... | collective-permute-start | bytes 1572872 | tf_op jit(solution)/shard_map/ppermute | solution.py:51
  85.1 16.6 %collective-permute-start.5 = (bf16[128,2048]{1,0:T(8,128)(2,1)S(1)}, bf16[128,2048]{1,0:T(8,128)(2,1)S(1)}, u32[]{:S(2)}, u32[]{:S(2)}) collective-permute-start(bf16[128,2048]{1,0:T(8,128)(2,1)S(1)} %fusion.1.own), channel_id=1, source_target_pairs={{0,3},{1,0},{2,1},{3,2},{4,7},{5,4},{6,5},{7,6},{8,11},{9,8},{10,9... | collective-permute-start | bytes 1572872 | tf_op jit(solution)/shard_map/ppermute | solution.py:51
  99.7 11.1 %copy-start.4 = (bf16[128,2048]{1,0:T(8,128)(2,1)}, bf16[128,2048]{1,0:T(8,128)(2,1)S(1)}, u32[]{:S(2)}) copy-start(bf16[128,2048]{1,0:T(8,128)(2,1)S(1)} %collective-permute-done.4.before) | copy-start | bytes 1572868
  99.8 10.1 %collective-permute-start.6 = (bf16[64,2048]{1,0:T(8,128)(2,1)S(1)}, bf16[64,2048]{1,0:T(8,128)(2,1)S(1)}, u32[]{:S(2)}, u32[]{:S(2)}) collective-permute-start(bf16[64,2048]{1,0:T(8,128)(2,1)S(1)} %slice.16), channel_id=1, source_target_pairs={{0,1},{1,2},{2,3},{3,0},{4,5},{5,6},{6,7},{7,4},{8,9},{9,10},{10,1... | collective-permute-start | bytes 786440 | tf_op jit(solution)/shard_map/ppermute | solution.py:51
  101.7 4.6 %copy-start.5 = (bf16[128,2048]{1,0:T(8,128)(2,1)}, bf16[128,2048]{1,0:T(8,128)(2,1)S(1)}, u32[]{:S(2)}) copy-start(bf16[128,2048]{1,0:T(8,128)(2,1)S(1)} %collective-permute-done.5.after) | copy-start | bytes 1572868
  101.7 9.1 %collective-permute-start.7 = (bf16[64,2048]{1,0:T(8,128)(2,1)S(1)}, bf16[64,2048]{1,0:T(8,128)(2,1)}, u32[]{:S(2)}, u32[]{:S(2)}) collective-permute-start(bf16[64,2048]{1,0:T(8,128)(2,1)S(1)} %slice.17), channel_id=1, source_target_pairs={{0,3},{1,0},{2,1},{3,2},{4,7},{5,4},{6,5},{7,6},{8,11},{9,8},{10,9... | collective-permute-start | bytes 786440 | tf_op jit(solution)/shard_map/ppermute | solution.py:51
  109.9 1.0 copy-start.8
  149.4 21.8 %all-to-all-start.3 = ((bf16[16,8,256]{2,1,0:T(8,128)(2,1)}), bf16[16,8,256]{2,1,0:T(8,128)(2,1)S(1)}, u32[]{:S(2)}, u32[]{:S(2)}) async-start(bf16[16,8,256]{2,1,0:T(8,128)(2,1)} %shard_map.131), calls=%async_computation.3 | async-start | bytes 131072 | tf_op jit(solution)/shard_map/all_to_all | solution.py:500
  157.4 9.6 %collective-permute-start.8 = (bf16[8,256]{1,0:T(8,128)(2,1)S(1)}, bf16[8,256]{1,0:T(8,128)(2,1)S(1)}, u32[]{:S(2)}, u32[]{:S(2)}) collective-permute-start(bf16[8,256]{1,0:T(8,128)(2,1)S(1)} %get-tuple-element.20), channel_id=1, source_target_pairs={{0,4},{4,8},{8,12},{12,16},{16,20},{20,24},{24,28},{28,32},{32,36}... | collective-permute-start | bytes 12296 | tf_op jit(solution)/shard_map/ppermute | solution.py:57
  162.0 6.1 %collective-permute-start.9 = (bf16[8,256]{1,0:T(8,128)(2,1)S(1)}, bf16[8,256]{1,0:T(8,128)(2,1)S(1)}, u32[]{:S(2)}, u32[]{:S(2)}) collective-permute-start(bf16[8,256]{1,0:T(8,128)(2,1)S(1)} %get-tuple-element.19), channel_id=1, source_target_pairs={{4,0},{8,4},{12,8},{16,12},{20,16},{24,20},{28,24},{32,28},{36,32}... | collective-permute-start | bytes 12296 | tf_op jit(solution)/shard_map/ppermute | solution.py:57
  167.0 1.1 copy-start.6
  168.1 0.6 copy-start.7
  171.2 0.6 copy-start.3
Sparse Core Ops, SparseCore 0:
  20.0 116.5 all-gather.1

commit v7 on v2

--- a/solution.py
+++ b/solution.py
@@ -30,12 +30,14 @@
     return lax.dot_general(a, b, (dims, ((), ())), precision=precision, preferred_element_type=f32)
 
 
-def call(kernel, out_shapes, operands, scalars=1, scratch=(), flops=0, moved=0):
+def call(kernel, out_shapes, operands, scalars=1, far=0, scratch=(), flops=0, moved=0):
     smem = pl.BlockSpec(memory_space=pltpu.SMEM)
     vmem = pl.BlockSpec(memory_space=pltpu.VMEM)
+    anywhere = pl.BlockSpec(memory_space=pl.ANY)
+    near = len(operands) - scalars - far
     return pl.pallas_call(
         kernel,
-        in_specs=[smem if i < scalars else vmem for i in range(len(operands))],
+        in_specs=[smem] * scalars + [anywhere] * far + [vmem] * near,
         out_specs=jax.tree.map(lambda _: vmem, out_shapes),
         out_shape=out_shapes,
         scratch_shapes=list(scratch),
@@ -304,7 +306,8 @@
     out[...] = matmul(pooled, group_map[tp]).astype(bf16)
 
 
-def finish_kernel(part, query, entering, pooled, out):
+def finish_kernel(place, part, query, entering, pooled, *outs_and_scratch):
+    *outs, ready = outs_and_scratch
     channel_one = lax.broadcasted_iota(jnp.int32, (LANES, DV), 0) < KEY_CHANNELS
     zero = jnp.zeros((), bf16)
     sides = []
@@ -317,51 +320,48 @@
         )
     joined = part[...] + matmul(query[...], jnp.concatenate(sides, axis=0))
     rows = joined.shape[0]
-    ready = [pooled[...]]
+    width = pooled.shape[1]
+    ready[:, :width] = pooled[...]
     for h in range(2):
         mine = joined[:, h * DV : (h + 1) * DV]
         scale = lax.rsqrt(jnp.mean(mine * mine, axis=1, keepdims=True) + eps_value)
-        ready.append((mine * scale).astype(bf16))
-    owners = out.shape[0]
-    for j in range(owners):
-        at = slice(j * rows // owners, (j + 1) * rows // owners)
-        start = 0
-        for piece in ready:
-            out[j, :, start : start + piece.shape[1]] = piece[at]
-            start += piece.shape[1]
-
-
-def output_kernel(place, activations, weight, out):
-    tp = place[0]
-    groups, _, width = activations.shape
-    total = None
-    for s in range(groups):
-        source = lax.rem(tp + groups - s, groups)
-        partial = matmul(
-            activations[source], weight[:, s * width : (s + 1) * width], ((1,), (1,))
-        )
-        partial = partial.astype(bf16).astype(f32)
-        total = partial if total is None else total + partial
-    out[...] = total.astype(bf16)
-
-
-def output_projection(place, activations, weights):
-    groups, rows, width = activations.shape
-    model = weights.shape[0]
-    tile = 256
-    return pl.pallas_call(
-        output_kernel,
-        grid=(model // tile,),
-        in_specs=[
-            pl.BlockSpec(memory_space=pltpu.SMEM),
-            pl.BlockSpec((groups, rows, width), lambda n: (0, 0, 0)),
-            pl.BlockSpec((tile, groups * width), lambda n: (n, 0)),
-        ],
-        out_specs=pl.BlockSpec((rows, tile), lambda n: (0, n)),
-        out_shape=jax.ShapeDtypeStruct((rows, model), bf16),
-        interpret=interpreted,
-        name="output_kernel",
-    )(place, activations, weights)
+        ready[:, width + h * DV : width + (h + 1) * DV] = (mine * scale).astype(bf16)
+    owners = len(outs)
+    share = rows // owners
+    for step, out in enumerate(outs):
+        first = pl.multiple_of(lax.rem(place[0] + step, owners) * share, share)
+        out[...] = ready[pl.ds(first, share), :]
+
+
+def start_loads(weights, start, weight_ref, sems):
+    pieces = sems.shape[0]
+    tile = weights.shape[0] // pieces
+    columns = slice(start, start + weight_ref.shape[1])
+    loads = []
+    for n in range(pieces):
+        here = slice(n * tile, (n + 1) * tile)
+        load = pltpu.make_async_copy(weights.at[here, columns], weight_ref.at[here], sems.at[n])
+        load.start()
+        loads.append((here, load))
+    return loads
+
+
+def own_kernel(weights, mine, out, weight_ref, sems):
+    for here, load in start_loads(weights, 0, weight_ref, sems):
+        load.wait()
+        out[:, here] = matmul(mine[...], weight_ref[here, :], ((1,), (1,))).astype(bf16)
+
+
+def output_kernel(weights, own_part, *rest):
+    *others, out, weight_ref, sems = rest
+    width = others[0].shape[1]
+    for here, load in start_loads(weights, width, weight_ref, sems):
+        load.wait()
+        total = own_part[:, here].astype(f32)
+        for s, other in enumerate(others):
+            block = weight_ref[here, s * width : (s + 1) * width]
+            total = total + matmul(other[...], block, ((1,), (1,))).astype(bf16).astype(f32)
+        out[:, here] = total.astype(bf16)
 
 
 def shape_of(*lengths, kind=bf16):
@@ -464,16 +464,42 @@
         flops=2 * rows * 4 * LANES * LANES,
         moved=1_000_000,
     )
-    activations = call(
+    share = rows // groups
+    width = 4 * LANES
+    mine, for_next, for_far, for_last = call(
         finish_kernel,
-        shape_of(groups, rows // groups, 4 * LANES),
-        (part, query, entering, pooled),
-        scalars=0,
+        (shape_of(share, width),) * groups,
+        (place, part, query, entering, pooled),
+        scratch=(pltpu.VMEM((rows, width), bf16),),
         flops=100_000_000,
         moved=2_000_000,
     )
-    gathered = lax.all_to_all(activations, "tp", 0, 0, tiled=True)
-    return output_projection(place, gathered, whole_out)
+    first = shifted(for_next, "tp", 1)
+    third = shifted(for_last, "tp", -1)
+    second = shifted(for_far, "tp", 2)
+    own_part = call(
+        own_kernel,
+        shape_of(share, model),
+        (whole_out, mine),
+        scalars=0,
+        far=1,
+        scratch=(pltpu.VMEM((model, width), bf16), pltpu.SemaphoreType.DMA((4,))),
+        flops=2 * share * model * width,
+        moved=2 * model * width,
+    )
+    return call(
+        output_kernel,
+        shape_of(share, model),
+        (whole_out, own_part, first, second, third),
+        scalars=0,
+        far=1,
+        scratch=(
+            pltpu.VMEM((model, (groups - 1) * width), bf16),
+            pltpu.SemaphoreType.DMA((8,)),
+        ),
+        flops=2 * share * model * (groups - 1) * width,
+        moved=2 * model * (groups - 1) * width,
+    )
 
 
 def solution(mesh):

time: 197 us -> 198 us (level)
  the two profiles are of different devices: /device:TPU:25 before, /device:TPU:66 now
where the time goes in v7:
time: 198 us; the launch traced here: 197 us
  blocking collectives  78.7 us (40%)
  starting transfers between devices  50.6 us (26%)
  Pallas kernels  28.6 us (14%)
  waiting for transfers between devices  16.7 us (8%)
  between operations  13.7 us (7%)
  local copies, waits for them, and re-layouts  5.88 us (3%)
  other arithmetic  2.99 us (2%)
    all_to_all x1, blocking collectives, shards(): weight_own = lax.all_to_all(copies, CHIPS, 0, 0, tiled=True)  56 us
    ppermute x11, starting transfers between devices, shifted(): lax.ppermute(value, axis, [(i, (i + step) % devices) for i in range(devic...  36.7 us
    pallas_call x7, Pallas kernels, call(): pl.pallas_call(kernel, in_specs=[smem] * scalars + [anywhere] * far + [vm...  28.6 us
    all_to_all x1, blocking collectives, shards(): received = lax.all_to_all(packed, SP, 0, 0, tiled=True)  22.7 us
    ppermute x11, waiting for transfers between devices, shifted(): lax.ppermute(value, axis, [(i, (i + step) % devices) for i in range(devic...  16.7 us
    ppermute x2, starting transfers between devices, neighbours(): return lax.ppermute(value, axes, pairs)  7.84 us
    all_to_all x1, starting transfers between devices, shards(): entering = lax.all_to_all(states, SP, 0, 0, tiled=True)  6.01 us
    unnamed x28, local copies, waits for them, and re-layouts  5.05 us
  transfers between devices with their start and end apart: 15, of which 5 were waited for; matrix products, arithmetic and copies ran while one was open for 2% of the time, Pallas kernels for 11%

profile of v7, /device:TPU:66, one launch (start us, length us, event | category | flops | bytes accessed | tf_op | source)
XLA Modules:
  0.0 197.1 jit_solution(14160140867856327627)
XLA Ops:
  7.3 3.4 %collective-permute-start = (bf16[16,512]{1,0:T(8,128)(2,1)S(1)}, bf16[16,512]{1,0:T(8,128)(2,1)S(1)}, u32[]{:S(2)}, u32[]{:S(2)}) collective-permute-start(bf16[16,512]{1,0:T(8,128)(2,1)S(1)} %maximum_bitcast_fusion), channel_id=1, source_target_pairs={{0,1},{1,2},{2,3},{3,0},{4,5},{5,6},{6,7},{7,4},{8,9},{9,10},{10,1... | collective-permute-start | bytes 49160 | tf_op jit(solution)/shard_map/ppermute | solution.py:51
  10.6 3.0 %collective-permute-start.1 = (bf16[16,512]{1,0:T(8,128)(2,1)S(1)}, bf16[16,512]{1,0:T(8,128)(2,1)S(1)}, u32[]{:S(2)}, u32[]{:S(2)}) collective-permute-start(bf16[16,512]{1,0:T(8,128)(2,1)S(1)} %maximum_bitcast_fusion), channel_id=1, source_target_pairs={{0,2},{1,3},{2,0},{3,1},{4,6},{5,7},{6,4},{7,5},{8,10},{9,11},{10,... | collective-permute-start | bytes 49160 | tf_op jit(solution)/shard_map/ppermute | solution.py:51
  13.7 4.1 %collective-permute-start.2 = (bf16[16,512]{1,0:T(8,128)(2,1)S(1)}, bf16[16,512]{1,0:T(8,128)(2,1)S(1)}, u32[]{:S(2)}, u32[]{:S(2)}) collective-permute-start(bf16[16,512]{1,0:T(8,128)(2,1)S(1)} %maximum_bitcast_fusion), channel_id=1, source_target_pairs={{0,3},{1,0},{2,1},{3,2},{4,7},{5,4},{6,5},{7,6},{8,11},{9,8},{10,9... | collective-permute-start | bytes 49160 | tf_op jit(solution)/shard_map/ppermute | solution.py:51
  20.8 56.0 %all_to_all.15.weight_own = bf16[64,16,768]{2,1,0:T(8,128)(2,1)S(1)} all-to-all(bf16[64,16,768]{2,1,0:T(8,128)(2,1)S(1)} %broadcast_in_dim.4), channel_id=1, replica_groups=mesh['sp_0'=8,'sp_1'=8,'sp_2'=2,'tp'=4] {'sp_0','sp_1'}, dimensions={0} | all-to-all | bytes 3145728 | tf_op jit(solution)/shard_map/all_to_all | solution.py:400
  76.8 2.0 %collective-permute-start.7 = (bf16[64,16,768]{2,1,0:T(8,128)(2,1)S(1)}, bf16[64,16,768]{2,1,0:T(8,128)(2,1)}, u32[]{:S(2)}, u32[]{:S(2)}) collective-permute-start(bf16[64,16,768]{2,1,0:T(8,128)(2,1)S(1)} %all_to_all.15.weight_own), channel_id=1, source_target_pairs={{0,4},{4,0},{1,5},{5,1},{2,6},{6,2},{3,7},{7,3},{8,12},{12,8},{9,1... | collective-permute-start | bytes 4718600 | tf_op jit(solution)/shard_map/ppermute | solution.py:51
  79.3 2.6 %collective-permute-start.3 = (bf16[128,2048]{1,0:T(8,128)(2,1)S(1)}, bf16[128,2048]{1,0:T(8,128)(2,1)S(1)}, u32[]{:S(2)}, u32[]{:S(2)}) collective-permute-start(bf16[128,2048]{1,0:T(8,128)(2,1)S(1)} %fusion.1.own), channel_id=1, source_target_pairs={{0,1},{1,2},{2,3},{3,0},{4,5},{5,6},{6,7},{7,4},{8,9},{9,10},{10,1... | collective-permute-start | bytes 1572872 | tf_op jit(solution)/shard_map/ppermute | solution.py:51
  81.8 3.3 %collective-permute-start.4 = (bf16[128,2048]{1,0:T(8,128)(2,1)S(1)}, bf16[128,2048]{1,0:T(8,128)(2,1)S(1)}, u32[]{:S(2)}, u32[]{:S(2)}) collective-permute-start(bf16[128,2048]{1,0:T(8,128)(2,1)S(1)} %fusion.1.own), channel_id=1, source_target_pairs={{0,3},{1,0},{2,1},{3,2},{4,7},{5,4},{6,5},{7,6},{8,11},{9,8},{10,9... | collective-permute-start | bytes 1572872 | tf_op jit(solution)/shard_map/ppermute | solution.py:51
  85.1 10.4 %collective-permute-done.3.before = bf16[128,2048]{1,0:T(8,128)(2,1)S(1)} collective-permute-done((bf16[128,2048]{1,0:T(8,128)(2,1)S(1)}, bf16[128,2048]{1,0:T(8,128)(2,1)S(1)}, u32[]{:S(2)}, u32[]{:S(2)}) %collective-permute-start.3) | collective-permute-done | bytes 524320 | tf_op jit(solution)/shard_map/ppermute | solution.py:51
  95.5 3.0 %collective-permute-start.5 = (bf16[64,2048]{1,0:T(8,128)(2,1)S(1)}, bf16[64,2048]{1,0:T(8,128)(2,1)}, u32[]{:S(2)}, u32[]{:S(2)}) collective-permute-start(bf16[64,2048]{1,0:T(8,128)(2,1)S(1)} %slice.16), channel_id=1, source_target_pairs={{0,1},{1,2},{2,3},{3,0},{4,5},{5,6},{6,7},{7,4},{8,9},{9,10},{10,1... | collective-permute-start | bytes 786440 | tf_op jit(solution)/shard_map/ppermute | solution.py:51
  98.9 3.1 %collective-permute-start.6 = (bf16[64,2048]{1,0:T(8,128)(2,1)S(1)}, bf16[64,2048]{1,0:T(8,128)(2,1)}, u32[]{:S(2)}, u32[]{:S(2)}) collective-permute-start(bf16[64,2048]{1,0:T(8,128)(2,1)S(1)} %slice.17), channel_id=1, source_target_pairs={{0,3},{1,0},{2,1},{3,2},{4,7},{5,4},{6,5},{7,6},{8,11},{9,8},{10,9... | collective-permute-start | bytes 786440 | tf_op jit(solution)/shard_map/ppermute | solution.py:51
  106.3 2.5 %collective-permute-done.6.far_end = bf16[64,2048]{1,0:T(8,128)(2,1)} collective-permute-done((bf16[64,2048]{1,0:T(8,128)(2,1)S(1)}, bf16[64,2048]{1,0:T(8,128)(2,1)}, u32[]{:S(2)}, u32[]{:S(2)}) %collective-permute-start.6) | collective-permute-done | bytes 262176 | tf_op jit(solution)/shard_map/ppermute | solution.py:51
  108.8 7.3 %shard_map.127 = (bf16[512,512]{1,0:T(8,128)(2,1)}, bf16[512,256]{1,0:T(8,128)(2,1)}, f32[2,512,128]{2,1,0:T(8,128)}, f32[128,1,384]{2,1,0:T(1,128)}) custom-call(s32[4]{0:T(128)} %pad_add_fusion.place, bf16[128,2048]{1,0:T(8,128)(2,1)} %copy-done.3, bf16[128,2048]{1,0:T(8,128)(2,1)} %copy-done.8, bf16[128,2048]{1,0:T(8,128)(2,1)} %copy-done.9, ...), custom_call_target="tpu_custom_call" | custom-call | flops 1879048192 | bytes 10000000 | tf_op jit(solution)/shard_map/pallas_call | solution.py:38
  116.1 22.7 %all_to_all.16.received = f32[128,1,384]{2,1,0:T(1,128)} all-to-all(f32[128,1,384]{2,1,0:T(1,128)} %get-tuple-element.19), channel_id=1, replica_groups=mesh['sp_0'=8,'sp_1'=8,'sp_2'=2,'tp'=4] {'sp_0','sp_1','sp_2'}, dimensions={0} | all-to-all | bytes 393216 | tf_op jit(solution)/shard_map/all_to_all | solution.py:442
  138.8 2.3 %shard_map.129 = f32[128,1,256]{2,1,0:T(1,128)} custom-call(s32[1]{0:T(128)} %bitcast.3.place, f32[128,1,384]{2,1,0:T(1,128)} %all_to_all.16.received, f32[2,128,128]{2,1,0:T(8,128)} %bitcast.8), custom_call_target="tpu_custom_call" | custom-call | flops 40000000 | tf_op jit(solution)/shard_map/pallas_call | solution.py:38
  141.1 6.0 %all-to-all-start.2 = ((f32[128,1,256]{2,1,0:T(1,128)}), f32[128,1,256]{2,1,0:T(1,128)S(1)}, u32[]{:S(2)}, u32[]{:S(2)}) async-start(f32[128,1,256]{2,1,0:T(1,128)} %shard_map.129), calls=%async_computation.2 | async-start | bytes 262144 | tf_op jit(solution)/shard_map/all_to_all | solution.py:459
  149.8 5.8 %collective-permute-start.9 = (bf16[8,256]{1,0:T(8,128)(2,1)S(1)}, bf16[8,256]{1,0:T(8,128)(2,1)S(1)}, u32[]{:S(2)}, u32[]{:S(2)}) collective-permute-start(bf16[8,256]{1,0:T(8,128)(2,1)S(1)} %get-tuple-element.25), channel_id=1, source_target_pairs={{4,0},{8,4},{12,8},{16,12},{20,16},{24,20},{28,24},{32,28},{36,32}... | collective-permute-start | bytes 12296 | tf_op jit(solution)/shard_map/ppermute | solution.py:57
  155.6 3.0 %shard_map.128 = (f32[512,256]{1,0:T(8,128)}, bf16[512,256]{1,0:T(8,128)(2,1)}) custom-call(bf16[512,512]{1,0:T(8,128)(2,1)} %get-tuple-element.15.qkv, f32[2,512,128]{2,1,0:T(8,128)} %get-tuple-element.16.logs), custom_call_target="tpu_custom_call" | custom-call | flops 536870912 | bytes 3000000 | tf_op jit(solution)/shard_map/pallas_call | solution.py:38
  159.9 2.5 %shard_map.130.pooled = bf16[512,256]{1,0:T(8,128)(2,1)} custom-call(s32[4]{0:T(128)} %pad_add_fusion.place, bf16[512,256]{1,0:T(8,128)(2,1)} %get-tuple-element.20.pool_input, bf16[8,256]{1,0:T(8,128)(2,1)} %copy-done.11, bf16[8,256]{1,0:T(8,128)(2,1)} %copy-done.12, bf16[4,256,256]{2,1,0:T(8,128)(2,1)} %group_map.1), custom_call_target="tpu_custom_call" | custom-call | flops 67108864 | bytes 1000000 | tf_op jit(solution)/shard_map/pallas_call | solution.py:38
  163.0 2.6 %shard_map.131 = (bf16[128,512]{1,0:T(8,128)(2,1)}, bf16[128,512]{1,0:T(8,128)(2,1)}, bf16[128,512]{1,0:T(8,128)(2,1)}, bf16[128,512]{1,0:T(8,128)(2,1)}) custom-call(s32[4]{0:T(128)} %pad_add_fusion.place, f32[512,256]{1,0:T(8,128)} %get-tuple-element.17.part, bf16[512,256]{1,0:T(8,128)(2,1)} %get-tuple-element.18.query, f32[128,1,256]{2,1,0:T(1,128)} %copy-done.2, ...), custom_call_target="tpu_custom_call" | custom-call | flops 100000000 | bytes 2000000 | tf_op jit(solution)/shard_map/pallas_call | solution.py:38
  165.6 3.7 %collective-permute-start.10 = (bf16[128,512]{1,0:T(8,128)(2,1)}, bf16[128,512]{1,0:T(8,128)(2,1)S(1)}, u32[]{:S(2)}, u32[]{:S(2)}) collective-permute-start(bf16[128,512]{1,0:T(8,128)(2,1)} %get-tuple-element.22), channel_id=1, source_target_pairs={{0,1},{1,2},{2,3},{3,0},{4,5},{5,6},{6,7},{7,4},{8,9},{9,10},{10,1... | collective-permute-start | bytes 393224 | tf_op jit(solution)/shard_map/ppermute | solution.py:51
  169.4 4.1 %collective-permute-start.11 = (bf16[128,512]{1,0:T(8,128)(2,1)}, bf16[128,512]{1,0:T(8,128)(2,1)S(1)}, u32[]{:S(2)}, u32[]{:S(2)}) collective-permute-start(bf16[128,512]{1,0:T(8,128)(2,1)} %get-tuple-element.23), channel_id=1, source_target_pairs={{0,2},{1,3},{2,0},{3,1},{4,6},{5,7},{6,4},{7,5},{8,10},{9,11},{10,... | collective-permute-start | bytes 393224 | tf_op jit(solution)/shard_map/ppermute | solution.py:51
  173.4 4.5 %collective-permute-start.12 = (bf16[128,512]{1,0:T(8,128)(2,1)}, bf16[128,512]{1,0:T(8,128)(2,1)S(1)}, u32[]{:S(2)}, u32[]{:S(2)}) collective-permute-start(bf16[128,512]{1,0:T(8,128)(2,1)} %get-tuple-element.24), channel_id=1, source_target_pairs={{0,3},{1,0},{2,1},{3,2},{4,7},{5,4},{6,5},{7,6},{8,11},{9,8},{10,9... | collective-permute-start | bytes 393224 | tf_op jit(solution)/shard_map/ppermute | solution.py:51
  178.0 4.1 %shard_map.132.own_part = bf16[128,2048]{1,0:T(8,128)(2,1)} custom-call(bf16[2048,2048]{1,0:T(8,128)(2,1)} %all-gather.2.cloned.1.call-done.weights, bf16[128,512]{1,0:T(8,128)(2,1)} %get-tuple-element.21.mine), custom_call_target="tpu_custom_call" | custom-call | flops 268435456 | bytes 2097152 | tf_op jit(solution)/shard_map/pallas_call | solution.py:38
  183.4 6.8 %shard_map.133 = bf16[128,2048]{1,0:T(8,128)(2,1)} custom-call(bf16[2048,2048]{1,0:T(8,128)(2,1)} %all-gather.2.cloned.1.call-done.weights, bf16[128,2048]{1,0:T(8,128)(2,1)} %shard_map.132.own_part, bf16[128,512]{1,0:T(8,128)(2,1)} %copy-done.5, bf16[128,512]{1,0:T(8,128)(2,1)} %copy-done.6, bf16[128,512]{1,0:T(8,128)(2,1)} %copy-done.7), custom_call_target="tpu_custom_call" | custom-call | flops 805306368 | bytes 6291456 | tf_op jit(solution)/shard_map/pallas_call | solution.py:38
  (55 shorter events, 14.7 us)
Async XLA Ops:
  6.5 171.4 %all-gather.2.cloned.1.call-start = ((), (), s32[]{:S(2)}) async-start(), calls=%async_computation.3 | async-start | bytes 8454144 | tf_op jit(solution)/shard_map/all_gather | solution.py:411
  7.3 10.5 %collective-permute-start = (bf16[16,512]{1,0:T(8,128)(2,1)S(1)}, bf16[16,512]{1,0:T(8,128)(2,1)S(1)}, u32[]{:S(2)}, u32[]{:S(2)}) collective-permute-start(bf16[16,512]{1,0:T(8,128)(2,1)S(1)} %maximum_bitcast_fusion), channel_id=1, source_target_pairs={{0,1},{1,2},{2,3},{3,0},{4,5},{5,6},{6,7},{7,4},{8,9},{9,10},{10,1... | collective-permute-start | bytes 49160 | tf_op jit(solution)/shard_map/ppermute | solution.py:51
  10.6 7.1 %collective-permute-start.1 = (bf16[16,512]{1,0:T(8,128)(2,1)S(1)}, bf16[16,512]{1,0:T(8,128)(2,1)S(1)}, u32[]{:S(2)}, u32[]{:S(2)}) collective-permute-start(bf16[16,512]{1,0:T(8,128)(2,1)S(1)} %maximum_bitcast_fusion), channel_id=1, source_target_pairs={{0,2},{1,3},{2,0},{3,1},{4,6},{5,7},{6,4},{7,5},{8,10},{9,11},{10,... | collective-permute-start | bytes 49160 | tf_op jit(solution)/shard_map/ppermute | solution.py:51
  13.7 5.6 %collective-permute-start.2 = (bf16[16,512]{1,0:T(8,128)(2,1)S(1)}, bf16[16,512]{1,0:T(8,128)(2,1)S(1)}, u32[]{:S(2)}, u32[]{:S(2)}) collective-permute-start(bf16[16,512]{1,0:T(8,128)(2,1)S(1)} %maximum_bitcast_fusion), channel_id=1, source_target_pairs={{0,3},{1,0},{2,1},{3,2},{4,7},{5,4},{6,5},{7,6},{8,11},{9,8},{10,9... | collective-permute-start | bytes 49160 | tf_op jit(solution)/shard_map/ppermute | solution.py:51
  20.8 58.1 %copy-start = (bf16[128,2048]{1,0:T(8,128)(2,1)S(1)}, bf16[128,2048]{1,0:T(8,128)(2,1)}, u32[]{:S(2)}) copy-start(bf16[128,2048]{1,0:T(8,128)(2,1)} %param.13) | copy-start | bytes 1572868
  76.8 26.3 %copy-start.1 = (bf16[64,16,768]{2,1,0:T(8,128)(2,1)}, bf16[64,16,768]{2,1,0:T(8,128)(2,1)S(1)}, u32[]{:S(2)}) copy-start(bf16[64,16,768]{2,1,0:T(8,128)(2,1)S(1)} %all_to_all.15.weight_own) | copy-start | bytes 4718596
  76.8 25.3 %copy-start.4 = (bf16[2048,64]{0,1:T(8,128)(2,1)S(1)}, bf16[2048,64]{0,1:T(8,128)(2,1)}, u32[]{:S(2)}) copy-start(bf16[2048,64]{0,1:T(8,128)(2,1)} %param.18) | copy-start | bytes 786436
  76.8 32.0 %collective-permute-start.7 = (bf16[64,16,768]{2,1,0:T(8,128)(2,1)S(1)}, bf16[64,16,768]{2,1,0:T(8,128)(2,1)}, u32[]{:S(2)}, u32[]{:S(2)}) collective-permute-start(bf16[64,16,768]{2,1,0:T(8,128)(2,1)S(1)} %all_to_all.15.weight_own), channel_id=1, source_target_pairs={{0,4},{4,0},{1,5},{5,1},{2,6},{6,2},{3,7},{7,3},{8,12},{12,8},{9,1... | collective-permute-start | bytes 4718600 | tf_op jit(solution)/shard_map/ppermute | solution.py:51
  79.1 24.1 %copy-start.10 = (f32[2,512]{1,0:T(2,128)S(1)}, f32[2,512]{1,0:T(2,128)}, u32[]{:S(2)}) copy-start(f32[2,512]{1,0:T(2,128)} %param.21) | copy-start | bytes 12292
  79.2 29.6 %copy-start.3 = (bf16[128,2048]{1,0:T(8,128)(2,1)}, bf16[128,2048]{1,0:T(8,128)(2,1)S(1)}, u32[]{:S(2)}) copy-start(bf16[128,2048]{1,0:T(8,128)(2,1)S(1)} %fusion.1.own) | copy-start | bytes 1572868
  79.3 16.2 %collective-permute-start.3 = (bf16[128,2048]{1,0:T(8,128)(2,1)S(1)}, bf16[128,2048]{1,0:T(8,128)(2,1)S(1)}, u32[]{:S(2)}, u32[]{:S(2)}) collective-permute-start(bf16[128,2048]{1,0:T(8,128)(2,1)S(1)} %fusion.1.own), channel_id=1, source_target_pairs={{0,1},{1,2},{2,3},{3,0},{4,5},{5,6},{6,7},{7,4},{8,9},{9,10},{10,1... | collective-permute-start | bytes 1572872 | tf_op jit(solution)/shard_map/ppermute | solution.py:51
  81.8 17.1 %collective-permute-start.4 = (bf16[128,2048]{1,0:T(8,128)(2,1)S(1)}, bf16[128,2048]{1,0:T(8,128)(2,1)S(1)}, u32[]{:S(2)}, u32[]{:S(2)}) collective-permute-start(bf16[128,2048]{1,0:T(8,128)(2,1)S(1)} %fusion.1.own), channel_id=1, source_target_pairs={{0,3},{1,0},{2,1},{3,2},{4,7},{5,4},{6,5},{7,6},{8,11},{9,8},{10,9... | collective-permute-start | bytes 1572872 | tf_op jit(solution)/shard_map/ppermute | solution.py:51
  95.5 13.4 %copy-start.8 = (bf16[128,2048]{1,0:T(8,128)(2,1)}, bf16[128,2048]{1,0:T(8,128)(2,1)S(1)}, u32[]{:S(2)}) copy-start(bf16[128,2048]{1,0:T(8,128)(2,1)S(1)} %collective-permute-done.3.before) | copy-start | bytes 1572868
  95.5 10.8 %collective-permute-start.5 = (bf16[64,2048]{1,0:T(8,128)(2,1)S(1)}, bf16[64,2048]{1,0:T(8,128)(2,1)}, u32[]{:S(2)}, u32[]{:S(2)}) collective-permute-start(bf16[64,2048]{1,0:T(8,128)(2,1)S(1)} %slice.16), channel_id=1, source_target_pairs={{0,1},{1,2},{2,3},{3,0},{4,5},{5,6},{6,7},{7,4},{8,9},{9,10},{10,1... | collective-permute-start | bytes 786440 | tf_op jit(solution)/shard_map/ppermute | solution.py:51
  98.9 3.2 %copy-start.9 = (bf16[128,2048]{1,0:T(8,128)(2,1)}, bf16[128,2048]{1,0:T(8,128)(2,1)S(1)}, u32[]{:S(2)}) copy-start(bf16[128,2048]{1,0:T(8,128)(2,1)S(1)} %collective-permute-done.4.after) | copy-start | bytes 1572868
  98.9 9.9 %collective-permute-start.6 = (bf16[64,2048]{1,0:T(8,128)(2,1)S(1)}, bf16[64,2048]{1,0:T(8,128)(2,1)}, u32[]{:S(2)}, u32[]{:S(2)}) collective-permute-start(bf16[64,2048]{1,0:T(8,128)(2,1)S(1)} %slice.17), channel_id=1, source_target_pairs={{0,3},{1,0},{2,1},{3,2},{4,7},{5,4},{6,5},{7,6},{8,11},{9,8},{10,9... | collective-permute-start | bytes 786440 | tf_op jit(solution)/shard_map/ppermute | solution.py:51
  141.1 21.3 %all-to-all-start.2 = ((f32[128,1,256]{2,1,0:T(1,128)}), f32[128,1,256]{2,1,0:T(1,128)S(1)}, u32[]{:S(2)}, u32[]{:S(2)}) async-start(f32[128,1,256]{2,1,0:T(1,128)} %shard_map.129), calls=%async_computation.2 | async-start | bytes 262144 | tf_op jit(solution)/shard_map/all_to_all | solution.py:459
  147.8 10.9 %collective-permute-start.8 = (bf16[8,256]{1,0:T(8,128)(2,1)S(1)}, bf16[8,256]{1,0:T(8,128)(2,1)S(1)}, u32[]{:S(2)}, u32[]{:S(2)}) collective-permute-start(bf16[8,256]{1,0:T(8,128)(2,1)S(1)} %get-tuple-element.26), channel_id=1, source_target_pairs={{0,4},{4,8},{8,12},{12,16},{16,20},{20,24},{24,28},{28,32},{32,36}... | collective-permute-start | bytes 12296 | tf_op jit(solution)/shard_map/ppermute | solution.py:57
  149.8 8.9 %collective-permute-start.9 = (bf16[8,256]{1,0:T(8,128)(2,1)S(1)}, bf16[8,256]{1,0:T(8,128)(2,1)S(1)}, u32[]{:S(2)}, u32[]{:S(2)}) collective-permute-start(bf16[8,256]{1,0:T(8,128)(2,1)S(1)} %get-tuple-element.25), channel_id=1, source_target_pairs={{4,0},{8,4},{12,8},{16,12},{20,16},{24,20},{28,24},{32,28},{36,32}... | collective-permute-start | bytes 12296 | tf_op jit(solution)/shard_map/ppermute | solution.py:57
  165.6 16.4 %collective-permute-start.10 = (bf16[128,512]{1,0:T(8,128)(2,1)}, bf16[128,512]{1,0:T(8,128)(2,1)S(1)}, u32[]{:S(2)}, u32[]{:S(2)}) collective-permute-start(bf16[128,512]{1,0:T(8,128)(2,1)} %get-tuple-element.22), channel_id=1, source_target_pairs={{0,1},{1,2},{2,3},{3,0},{4,5},{5,6},{6,7},{7,4},{8,9},{9,10},{10,1... | collective-permute-start | bytes 393224 | tf_op jit(solution)/shard_map/ppermute | solution.py:51
  169.4 12.8 %collective-permute-start.11 = (bf16[128,512]{1,0:T(8,128)(2,1)}, bf16[128,512]{1,0:T(8,128)(2,1)S(1)}, u32[]{:S(2)}, u32[]{:S(2)}) collective-permute-start(bf16[128,512]{1,0:T(8,128)(2,1)} %get-tuple-element.23), channel_id=1, source_target_pairs={{0,2},{1,3},{2,0},{3,1},{4,6},{5,7},{6,4},{7,5},{8,10},{9,11},{10,... | collective-permute-start | bytes 393224 | tf_op jit(solution)/shard_map/ppermute | solution.py:51
  173.4 8.7 %collective-permute-start.12 = (bf16[128,512]{1,0:T(8,128)(2,1)}, bf16[128,512]{1,0:T(8,128)(2,1)S(1)}, u32[]{:S(2)}, u32[]{:S(2)}) collective-permute-start(bf16[128,512]{1,0:T(8,128)(2,1)} %get-tuple-element.24), channel_id=1, source_target_pairs={{0,3},{1,0},{2,1},{3,2},{4,7},{5,4},{6,5},{7,6},{8,11},{9,8},{10,9... | collective-permute-start | bytes 393224 | tf_op jit(solution)/shard_map/ppermute | solution.py:51
  182.1 0.7 copy-start.5
  182.1 0.7 copy-start.6
  (4 other events, 2.5 us)
Sparse Core Ops, SparseCore 0:
  20.1 114.9 all-gather.1

commit v8 on v7

--- a/solution.py
+++ b/solution.py
@@ -161,18 +161,18 @@
     first = lax.broadcasted_iota(jnp.int32, (LANES, LANES), 0) < KEY_CHANNELS
     for d in range(2):
         mine = updates[d * LANES : (d + 1) * LANES]
-        packed_out[:, 0, d * LANES : (d + 1) * LANES] = jnp.where(
-            first, mine[:, :LANES], mine[:, LANES:]
-        )
+        packed_out[:, d, :] = jnp.where(first, mine[:, :LANES], mine[:, LANES:]).astype(bf16)
     totals = jnp.concatenate([total_fwd, total_bwd], axis=0)
-    stacked = jnp.concatenate([totals, jnp.zeros((LANES - 2, LANES), f32)], axis=0)
-    packed_out[:, 0, 2 * LANES :] = stacked.T
+    high = totals.astype(bf16).astype(f32)
+    stacked = jnp.concatenate([high, totals - high, jnp.zeros((LANES - 4, LANES), f32)], axis=0)
+    packed_out[:, 2, :] = stacked.T.astype(bf16)
 
 
 def scan_kernel(place, received, start, out):
     devices = received.shape[0]
     here = place[0]
-    logs = received[:, 0, 2 * LANES :]
+    parts = received[:, 2, :].astype(f32)
+    logs = parts + pltpu.roll(parts, LANES - 2, 1)
     row = lax.broadcasted_iota(jnp.int32, (devices, devices), 0)
     col = lax.broadcasted_iota(jnp.int32, (devices, devices), 1)
     earlier = (col < row).astype(f32)
@@ -195,11 +195,11 @@
         weights = jnp.where(allowed, jnp.exp(jnp.minimum(between, 0.0)), 0.0)
         high = weights.astype(bf16)
         low = (weights - high.astype(f32)).astype(bf16)
-        updates = received[:, 0, r * LANES : (r + 1) * LANES].astype(bf16)
+        updates = received[:, r, :]
         first = start[r, pl.ds(here, 1), :]
         entering = matmul(high, updates) + matmul(low, updates)
         entering = entering + jnp.exp(jnp.minimum(outside, 0.0)) * first
-        out[:, 0, r * LANES : (r + 1) * LANES] = entering
+        out[:, r, :] = entering.astype(bf16)
 
 
 def inner_kernel(qkv, logs, part_out, query_out):
@@ -312,7 +312,7 @@
     zero = jnp.zeros((), bf16)
     sides = []
     for d in range(2):
-        state = entering[:, 0, d * LANES : (d + 1) * LANES].astype(bf16)
+        state = entering[:, d, :]
         sides.append(
             jnp.concatenate(
                 [jnp.where(channel_one, state, zero), jnp.where(channel_one, zero, state)], axis=1
@@ -416,7 +416,7 @@
             shape_of(rows, 4 * LANES),
             shape_of(rows, 2 * LANES),
             shape_of(2, rows, LANES, kind=f32),
-            shape_of(LANES, 1, 3 * LANES, kind=f32),
+            shape_of(LANES, 3, LANES),
         ),
         (
             place,
@@ -440,8 +440,6 @@
         moved=10_000_000,
     )
     received = lax.all_to_all(packed, SP, 0, 0, tiled=True)
-    rim_before = neighbours(pool_input[rows - rim_width :], SP, 1)
-    rim_after = neighbours(pool_input[:rim_width], SP, -1)
     part, query = call(
         inner_kernel,
         (shape_of(rows, 2 * DV, kind=f32), shape_of(rows, 2 * LANES)),
@@ -450,9 +448,11 @@
         flops=2 * rows * model * 2 * LANES,
         moved=3_000_000,
     )
+    rim_before = neighbours(pool_input[rows - rim_width :], SP, 1)
+    rim_after = neighbours(pool_input[:rim_width], SP, -1)
     states = call(
         scan_kernel,
-        shape_of(positions, 1, 2 * LANES, kind=f32),
+        shape_of(positions, 2, LANES),
         (place[2:3], received, starting_state.reshape(2, -1, DV)),
         flops=40_000_000,
     )

time: 198 us -> 197 us (level)
  no operation moved by 1% of the time
where the time goes in v8:
time: 197 us; the launch traced here: 196 us
  blocking collectives  77.3 us (39%)
  starting transfers between devices  50.8 us (26%)
  Pallas kernels  28.8 us (15%)
  waiting for transfers between devices  16.7 us (8%)
  between operations  13.7 us (7%)
  local copies, waits for them, and re-layouts  5.84 us (3%)
  other arithmetic  3.03 us (2%)
    all_to_all x1, blocking collectives, shards(): weight_own = lax.all_to_all(copies, CHIPS, 0, 0, tiled=True)  56 us
    ppermute x11, starting transfers between devices, shifted(): lax.ppermute(value, axis, [(i, (i + step) % devices) for i in range(devic...  37.1 us
    pallas_call x7, Pallas kernels, call(): pl.pallas_call(kernel, in_specs=[smem] * scalars + [anywhere] * far + [vm...  28.8 us
    all_to_all x1, blocking collectives, shards(): received = lax.all_to_all(packed, SP, 0, 0, tiled=True)  21.3 us
    ppermute x11, waiting for transfers between devices, shifted(): lax.ppermute(value, axis, [(i, (i + step) % devices) for i in range(devic...  16.6 us
    ppermute x2, starting transfers between devices, neighbours(): return lax.ppermute(value, axes, pairs)  7.84 us
    all_to_all x1, starting transfers between devices, shards(): entering = lax.all_to_all(states, SP, 0, 0, tiled=True)  5.81 us
    unnamed x28, local copies, waits for them, and re-layouts  5.01 us
  transfers between devices with their start and end apart: 15, of which 5 were waited for; matrix products, arithmetic and copies ran while one was open for 2% of the time, Pallas kernels for 11%

profile of v8, /device:TPU:66, one launch (start us, length us, event | category | flops | bytes accessed | tf_op | source)
XLA Modules:
  0.0 196.1 jit_solution(7178769678932208803)
XLA Ops:
  7.3 3.4 %collective-permute-start = (bf16[16,512]{1,0:T(8,128)(2,1)S(1)}, bf16[16,512]{1,0:T(8,128)(2,1)S(1)}, u32[]{:S(2)}, u32[]{:S(2)}) collective-permute-start(bf16[16,512]{1,0:T(8,128)(2,1)S(1)} %maximum_bitcast_fusion), channel_id=1, source_target_pairs={{0,1},{1,2},{2,3},{3,0},{4,5},{5,6},{6,7},{7,4},{8,9},{9,10},{10,1... | collective-permute-start | bytes 49160 | tf_op jit(solution)/shard_map/ppermute | solution.py:51
  10.6 3.0 %collective-permute-start.1 = (bf16[16,512]{1,0:T(8,128)(2,1)S(1)}, bf16[16,512]{1,0:T(8,128)(2,1)S(1)}, u32[]{:S(2)}, u32[]{:S(2)}) collective-permute-start(bf16[16,512]{1,0:T(8,128)(2,1)S(1)} %maximum_bitcast_fusion), channel_id=1, source_target_pairs={{0,2},{1,3},{2,0},{3,1},{4,6},{5,7},{6,4},{7,5},{8,10},{9,11},{10,... | collective-permute-start | bytes 49160 | tf_op jit(solution)/shard_map/ppermute | solution.py:51
  13.7 4.1 %collective-permute-start.2 = (bf16[16,512]{1,0:T(8,128)(2,1)S(1)}, bf16[16,512]{1,0:T(8,128)(2,1)S(1)}, u32[]{:S(2)}, u32[]{:S(2)}) collective-permute-start(bf16[16,512]{1,0:T(8,128)(2,1)S(1)} %maximum_bitcast_fusion), channel_id=1, source_target_pairs={{0,3},{1,0},{2,1},{3,2},{4,7},{5,4},{6,5},{7,6},{8,11},{9,8},{10,9... | collective-permute-start | bytes 49160 | tf_op jit(solution)/shard_map/ppermute | solution.py:51
  20.8 56.0 %all_to_all.15.weight_own = bf16[64,16,768]{2,1,0:T(8,128)(2,1)S(1)} all-to-all(bf16[64,16,768]{2,1,0:T(8,128)(2,1)S(1)} %broadcast_in_dim.4), channel_id=1, replica_groups=mesh['sp_0'=8,'sp_1'=8,'sp_2'=2,'tp'=4] {'sp_0','sp_1'}, dimensions={0} | all-to-all | bytes 3145728 | tf_op jit(solution)/shard_map/all_to_all | solution.py:400
  76.8 2.0 %collective-permute-start.7 = (bf16[64,16,768]{2,1,0:T(8,128)(2,1)S(1)}, bf16[64,16,768]{2,1,0:T(8,128)(2,1)}, u32[]{:S(2)}, u32[]{:S(2)}) collective-permute-start(bf16[64,16,768]{2,1,0:T(8,128)(2,1)S(1)} %all_to_all.15.weight_own), channel_id=1, source_target_pairs={{0,4},{4,0},{1,5},{5,1},{2,6},{6,2},{3,7},{7,3},{8,12},{12,8},{9,1... | collective-permute-start | bytes 4718600 | tf_op jit(solution)/shard_map/ppermute | solution.py:51
  79.3 2.6 %collective-permute-start.3 = (bf16[128,2048]{1,0:T(8,128)(2,1)S(1)}, bf16[128,2048]{1,0:T(8,128)(2,1)S(1)}, u32[]{:S(2)}, u32[]{:S(2)}) collective-permute-start(bf16[128,2048]{1,0:T(8,128)(2,1)S(1)} %fusion.1.own), channel_id=1, source_target_pairs={{0,1},{1,2},{2,3},{3,0},{4,5},{5,6},{6,7},{7,4},{8,9},{9,10},{10,1... | collective-permute-start | bytes 1572872 | tf_op jit(solution)/shard_map/ppermute | solution.py:51
  81.8 3.3 %collective-permute-start.4 = (bf16[128,2048]{1,0:T(8,128)(2,1)S(1)}, bf16[128,2048]{1,0:T(8,128)(2,1)S(1)}, u32[]{:S(2)}, u32[]{:S(2)}) collective-permute-start(bf16[128,2048]{1,0:T(8,128)(2,1)S(1)} %fusion.1.own), channel_id=1, source_target_pairs={{0,3},{1,0},{2,1},{3,2},{4,7},{5,4},{6,5},{7,6},{8,11},{9,8},{10,9... | collective-permute-start | bytes 1572872 | tf_op jit(solution)/shard_map/ppermute | solution.py:51
  85.1 10.4 %collective-permute-done.3.before = bf16[128,2048]{1,0:T(8,128)(2,1)S(1)} collective-permute-done((bf16[128,2048]{1,0:T(8,128)(2,1)S(1)}, bf16[128,2048]{1,0:T(8,128)(2,1)S(1)}, u32[]{:S(2)}, u32[]{:S(2)}) %collective-permute-start.3) | collective-permute-done | bytes 524320 | tf_op jit(solution)/shard_map/ppermute | solution.py:51
  95.5 3.0 %collective-permute-start.5 = (bf16[64,2048]{1,0:T(8,128)(2,1)S(1)}, bf16[64,2048]{1,0:T(8,128)(2,1)}, u32[]{:S(2)}, u32[]{:S(2)}) collective-permute-start(bf16[64,2048]{1,0:T(8,128)(2,1)S(1)} %slice.16), channel_id=1, source_target_pairs={{0,1},{1,2},{2,3},{3,0},{4,5},{5,6},{6,7},{7,4},{8,9},{9,10},{10,1... | collective-permute-start | bytes 786440 | tf_op jit(solution)/shard_map/ppermute | solution.py:51
  99.0 3.1 %collective-permute-start.6 = (bf16[64,2048]{1,0:T(8,128)(2,1)S(1)}, bf16[64,2048]{1,0:T(8,128)(2,1)}, u32[]{:S(2)}, u32[]{:S(2)}) collective-permute-start(bf16[64,2048]{1,0:T(8,128)(2,1)S(1)} %slice.17), channel_id=1, source_target_pairs={{0,3},{1,0},{2,1},{3,2},{4,7},{5,4},{6,5},{7,6},{8,11},{9,8},{10,9... | collective-permute-start | bytes 786440 | tf_op jit(solution)/shard_map/ppermute | solution.py:51
  106.3 2.5 %collective-permute-done.6.far_end = bf16[64,2048]{1,0:T(8,128)(2,1)} collective-permute-done((bf16[64,2048]{1,0:T(8,128)(2,1)S(1)}, bf16[64,2048]{1,0:T(8,128)(2,1)}, u32[]{:S(2)}, u32[]{:S(2)}) %collective-permute-start.6) | collective-permute-done | bytes 262176 | tf_op jit(solution)/shard_map/ppermute | solution.py:51
  108.9 7.4 %shard_map.127 = (bf16[512,512]{1,0:T(8,128)(2,1)}, bf16[512,256]{1,0:T(8,128)(2,1)}, f32[2,512,128]{2,1,0:T(8,128)}, bf16[128,3,128]{2,1,0:T(4,128)(2,1)}) custom-call(s32[4]{0:T(128)} %pad_add_fusion.place, bf16[128,2048]{1,0:T(8,128)(2,1)} %copy-done.2, bf16[128,2048]{1,0:T(8,128)(2,1)} %copy-done.8, bf16[128,2048]{1,0:T(8,128)(2,1)} %copy-done.9, ...), custom_call_target="tpu_custom_call" | custom-call | flops 1879048192 | bytes 10000000 | tf_op jit(solution)/shard_map/pallas_call | solution.py:38
  116.2 21.3 %all_to_all.16.received = bf16[128,3,128]{2,1,0:T(4,128)(2,1)} all-to-all(bf16[128,3,128]{2,1,0:T(4,128)(2,1)} %get-tuple-element.19), channel_id=1, replica_groups=mesh['sp_0'=8,'sp_1'=8,'sp_2'=2,'tp'=4] {'sp_0','sp_1','sp_2'}, dimensions={0} | all-to-all | bytes 196608 | tf_op jit(solution)/shard_map/all_to_all | solution.py:442
  137.5 2.3 %shard_map.129 = bf16[128,2,128]{2,1,0:T(2,128)(2,1)} custom-call(s32[1]{0:T(128)} %bitcast.3.place, bf16[128,3,128]{2,1,0:T(4,128)(2,1)} %all_to_all.16.received, f32[2,128,128]{2,1,0:T(8,128)} %bitcast.8), custom_call_target="tpu_custom_call" | custom-call | flops 40000000 | tf_op jit(solution)/shard_map/pallas_call | solution.py:38
  139.9 5.8 %all-to-all-start.2 = ((bf16[128,2,128]{2,1,0:T(2,128)(2,1)}), bf16[128,2,128]{2,1,0:T(2,128)(2,1)S(1)}, u32[]{:S(2)}, u32[]{:S(2)}) async-start(bf16[128,2,128]{2,1,0:T(2,128)(2,1)} %shard_map.129), calls=%async_computation.2 | async-start | bytes 131072 | tf_op jit(solution)/shard_map/all_to_all | solution.py:459
  148.4 5.8 %collective-permute-start.9 = (bf16[8,256]{1,0:T(8,128)(2,1)S(1)}, bf16[8,256]{1,0:T(8,128)(2,1)S(1)}, u32[]{:S(2)}, u32[]{:S(2)}) collective-permute-start(bf16[8,256]{1,0:T(8,128)(2,1)S(1)} %get-tuple-element.25), channel_id=1, source_target_pairs={{4,0},{8,4},{12,8},{16,12},{20,16},{24,20},{28,24},{32,28},{36,32}... | collective-permute-start | bytes 12296 | tf_op jit(solution)/shard_map/ppermute | solution.py:57
  154.2 3.0 %shard_map.128 = (f32[512,256]{1,0:T(8,128)}, bf16[512,256]{1,0:T(8,128)(2,1)}) custom-call(bf16[512,512]{1,0:T(8,128)(2,1)} %get-tuple-element.15.qkv, f32[2,512,128]{2,1,0:T(8,128)} %get-tuple-element.16.logs), custom_call_target="tpu_custom_call" | custom-call | flops 536870912 | bytes 3000000 | tf_op jit(solution)/shard_map/pallas_call | solution.py:38
  158.4 2.5 %shard_map.130.pooled = bf16[512,256]{1,0:T(8,128)(2,1)} custom-call(s32[4]{0:T(128)} %pad_add_fusion.place, bf16[512,256]{1,0:T(8,128)(2,1)} %get-tuple-element.20.pool_input, bf16[8,256]{1,0:T(8,128)(2,1)} %copy-done.11, bf16[8,256]{1,0:T(8,128)(2,1)} %copy-done.12, bf16[4,256,256]{2,1,0:T(8,128)(2,1)} %group_map.1), custom_call_target="tpu_custom_call" | custom-call | flops 67108864 | bytes 1000000 | tf_op jit(solution)/shard_map/pallas_call | solution.py:38
  161.6 2.7 %shard_map.131 = (bf16[128,512]{1,0:T(8,128)(2,1)}, bf16[128,512]{1,0:T(8,128)(2,1)}, bf16[128,512]{1,0:T(8,128)(2,1)}, bf16[128,512]{1,0:T(8,128)(2,1)}) custom-call(s32[4]{0:T(128)} %pad_add_fusion.place, f32[512,256]{1,0:T(8,128)} %get-tuple-element.17.part, bf16[512,256]{1,0:T(8,128)(2,1)} %get-tuple-element.18.query, bf16[128,2,128]{2,1,0:T(2,128)(2,1)} %copy-done.4, ...), custom_call_target="tpu_custom_call" | custom-call | flops 100000000 | bytes 2000000 | tf_op jit(solution)/shard_map/pallas_call | solution.py:38
  164.3 3.6 %collective-permute-start.10 = (bf16[128,512]{1,0:T(8,128)(2,1)}, bf16[128,512]{1,0:T(8,128)(2,1)S(1)}, u32[]{:S(2)}, u32[]{:S(2)}) collective-permute-start(bf16[128,512]{1,0:T(8,128)(2,1)} %get-tuple-element.22), channel_id=1, source_target_pairs={{0,1},{1,2},{2,3},{3,0},{4,5},{5,6},{6,7},{7,4},{8,9},{9,10},{10,1... | collective-permute-start | bytes 393224 | tf_op jit(solution)/shard_map/ppermute | solution.py:51
  167.9 4.5 %collective-permute-start.11 = (bf16[128,512]{1,0:T(8,128)(2,1)}, bf16[128,512]{1,0:T(8,128)(2,1)S(1)}, u32[]{:S(2)}, u32[]{:S(2)}) collective-permute-start(bf16[128,512]{1,0:T(8,128)(2,1)} %get-tuple-element.23), channel_id=1, source_target_pairs={{0,2},{1,3},{2,0},{3,1},{4,6},{5,7},{6,4},{7,5},{8,10},{9,11},{10,... | collective-permute-start | bytes 393224 | tf_op jit(solution)/shard_map/ppermute | solution.py:51
  172.4 4.5 %collective-permute-start.12 = (bf16[128,512]{1,0:T(8,128)(2,1)}, bf16[128,512]{1,0:T(8,128)(2,1)S(1)}, u32[]{:S(2)}, u32[]{:S(2)}) collective-permute-start(bf16[128,512]{1,0:T(8,128)(2,1)} %get-tuple-element.24), channel_id=1, source_target_pairs={{0,3},{1,0},{2,1},{3,2},{4,7},{5,4},{6,5},{7,6},{8,11},{9,8},{10,9... | collective-permute-start | bytes 393224 | tf_op jit(solution)/shard_map/ppermute | solution.py:51
  177.0 4.1 %shard_map.132.own_part = bf16[128,2048]{1,0:T(8,128)(2,1)} custom-call(bf16[2048,2048]{1,0:T(8,128)(2,1)} %all-gather.2.cloned.1.call-done.weights, bf16[128,512]{1,0:T(8,128)(2,1)} %get-tuple-element.21.mine), custom_call_target="tpu_custom_call" | custom-call | flops 268435456 | bytes 2097152 | tf_op jit(solution)/shard_map/pallas_call | solution.py:38
  182.5 6.8 %shard_map.133 = bf16[128,2048]{1,0:T(8,128)(2,1)} custom-call(bf16[2048,2048]{1,0:T(8,128)(2,1)} %all-gather.2.cloned.1.call-done.weights, bf16[128,2048]{1,0:T(8,128)(2,1)} %shard_map.132.own_part, bf16[128,512]{1,0:T(8,128)(2,1)} %copy-done.5, bf16[128,512]{1,0:T(8,128)(2,1)} %copy-done.6, bf16[128,512]{1,0:T(8,128)(2,1)} %copy-done.7), custom_call_target="tpu_custom_call" | custom-call | flops 805306368 | bytes 6291456 | tf_op jit(solution)/shard_map/pallas_call | solution.py:38
  (55 shorter events, 14.7 us)
Async XLA Ops:
  6.5 170.4 %all-gather.2.cloned.1.call-start = ((), (), s32[]{:S(2)}) async-start(), calls=%async_computation.3 | async-start | bytes 8454144 | tf_op jit(solution)/shard_map/all_gather | solution.py:411
  7.3 10.5 %collective-permute-start = (bf16[16,512]{1,0:T(8,128)(2,1)S(1)}, bf16[16,512]{1,0:T(8,128)(2,1)S(1)}, u32[]{:S(2)}, u32[]{:S(2)}) collective-permute-start(bf16[16,512]{1,0:T(8,128)(2,1)S(1)} %maximum_bitcast_fusion), channel_id=1, source_target_pairs={{0,1},{1,2},{2,3},{3,0},{4,5},{5,6},{6,7},{7,4},{8,9},{9,10},{10,1... | collective-permute-start | bytes 49160 | tf_op jit(solution)/shard_map/ppermute | solution.py:51
  10.6 7.1 %collective-permute-start.1 = (bf16[16,512]{1,0:T(8,128)(2,1)S(1)}, bf16[16,512]{1,0:T(8,128)(2,1)S(1)}, u32[]{:S(2)}, u32[]{:S(2)}) collective-permute-start(bf16[16,512]{1,0:T(8,128)(2,1)S(1)} %maximum_bitcast_fusion), channel_id=1, source_target_pairs={{0,2},{1,3},{2,0},{3,1},{4,6},{5,7},{6,4},{7,5},{8,10},{9,11},{10,... | collective-permute-start | bytes 49160 | tf_op jit(solution)/shard_map/ppermute | solution.py:51
  13.7 5.6 %collective-permute-start.2 = (bf16[16,512]{1,0:T(8,128)(2,1)S(1)}, bf16[16,512]{1,0:T(8,128)(2,1)S(1)}, u32[]{:S(2)}, u32[]{:S(2)}) collective-permute-start(bf16[16,512]{1,0:T(8,128)(2,1)S(1)} %maximum_bitcast_fusion), channel_id=1, source_target_pairs={{0,3},{1,0},{2,1},{3,2},{4,7},{5,4},{6,5},{7,6},{8,11},{9,8},{10,9... | collective-permute-start | bytes 49160 | tf_op jit(solution)/shard_map/ppermute | solution.py:51
  20.8 58.1 %copy-start = (bf16[128,2048]{1,0:T(8,128)(2,1)S(1)}, bf16[128,2048]{1,0:T(8,128)(2,1)}, u32[]{:S(2)}) copy-start(bf16[128,2048]{1,0:T(8,128)(2,1)} %param.13) | copy-start | bytes 1572868
  76.8 26.3 %copy-start.1 = (bf16[64,16,768]{2,1,0:T(8,128)(2,1)}, bf16[64,16,768]{2,1,0:T(8,128)(2,1)S(1)}, u32[]{:S(2)}) copy-start(bf16[64,16,768]{2,1,0:T(8,128)(2,1)S(1)} %all_to_all.15.weight_own) | copy-start | bytes 4718596
  76.8 25.3 %copy-start.3 = (bf16[2048,64]{0,1:T(8,128)(2,1)S(1)}, bf16[2048,64]{0,1:T(8,128)(2,1)}, u32[]{:S(2)}) copy-start(bf16[2048,64]{0,1:T(8,128)(2,1)} %param.18) | copy-start | bytes 786436
  76.8 32.0 %collective-permute-start.7 = (bf16[64,16,768]{2,1,0:T(8,128)(2,1)S(1)}, bf16[64,16,768]{2,1,0:T(8,128)(2,1)}, u32[]{:S(2)}, u32[]{:S(2)}) collective-permute-start(bf16[64,16,768]{2,1,0:T(8,128)(2,1)S(1)} %all_to_all.15.weight_own), channel_id=1, source_target_pairs={{0,4},{4,0},{1,5},{5,1},{2,6},{6,2},{3,7},{7,3},{8,12},{12,8},{9,1... | collective-permute-start | bytes 4718600 | tf_op jit(solution)/shard_map/ppermute | solution.py:51
  79.1 24.1 %copy-start.10 = (f32[2,512]{1,0:T(2,128)S(1)}, f32[2,512]{1,0:T(2,128)}, u32[]{:S(2)}) copy-start(f32[2,512]{1,0:T(2,128)} %param.21) | copy-start | bytes 12292
  79.3 29.6 %copy-start.2 = (bf16[128,2048]{1,0:T(8,128)(2,1)}, bf16[128,2048]{1,0:T(8,128)(2,1)S(1)}, u32[]{:S(2)}) copy-start(bf16[128,2048]{1,0:T(8,128)(2,1)S(1)} %fusion.1.own) | copy-start | bytes 1572868
  79.3 16.2 %collective-permute-start.3 = (bf16[128,2048]{1,0:T(8,128)(2,1)S(1)}, bf16[128,2048]{1,0:T(8,128)(2,1)S(1)}, u32[]{:S(2)}, u32[]{:S(2)}) collective-permute-start(bf16[128,2048]{1,0:T(8,128)(2,1)S(1)} %fusion.1.own), channel_id=1, source_target_pairs={{0,1},{1,2},{2,3},{3,0},{4,5},{5,6},{6,7},{7,4},{8,9},{9,10},{10,1... | collective-permute-start | bytes 1572872 | tf_op jit(solution)/shard_map/ppermute | solution.py:51
  81.8 17.1 %collective-permute-start.4 = (bf16[128,2048]{1,0:T(8,128)(2,1)S(1)}, bf16[128,2048]{1,0:T(8,128)(2,1)S(1)}, u32[]{:S(2)}, u32[]{:S(2)}) collective-permute-start(bf16[128,2048]{1,0:T(8,128)(2,1)S(1)} %fusion.1.own), channel_id=1, source_target_pairs={{0,3},{1,0},{2,1},{3,2},{4,7},{5,4},{6,5},{7,6},{8,11},{9,8},{10,9... | collective-permute-start | bytes 1572872 | tf_op jit(solution)/shard_map/ppermute | solution.py:51
  95.5 13.4 %copy-start.8 = (bf16[128,2048]{1,0:T(8,128)(2,1)}, bf16[128,2048]{1,0:T(8,128)(2,1)S(1)}, u32[]{:S(2)}) copy-start(bf16[128,2048]{1,0:T(8,128)(2,1)S(1)} %collective-permute-done.3.before) | copy-start | bytes 1572868
  95.5 10.8 %collective-permute-start.5 = (bf16[64,2048]{1,0:T(8,128)(2,1)S(1)}, bf16[64,2048]{1,0:T(8,128)(2,1)}, u32[]{:S(2)}, u32[]{:S(2)}) collective-permute-start(bf16[64,2048]{1,0:T(8,128)(2,1)S(1)} %slice.16), channel_id=1, source_target_pairs={{0,1},{1,2},{2,3},{3,0},{4,5},{5,6},{6,7},{7,4},{8,9},{9,10},{10,1... | collective-permute-start | bytes 786440 | tf_op jit(solution)/shard_map/ppermute | solution.py:51
  98.9 3.2 %copy-start.9 = (bf16[128,2048]{1,0:T(8,128)(2,1)}, bf16[128,2048]{1,0:T(8,128)(2,1)S(1)}, u32[]{:S(2)}) copy-start(bf16[128,2048]{1,0:T(8,128)(2,1)S(1)} %collective-permute-done.4.after) | copy-start | bytes 1572868
  99.0 9.9 %collective-permute-start.6 = (bf16[64,2048]{1,0:T(8,128)(2,1)S(1)}, bf16[64,2048]{1,0:T(8,128)(2,1)}, u32[]{:S(2)}, u32[]{:S(2)}) collective-permute-start(bf16[64,2048]{1,0:T(8,128)(2,1)S(1)} %slice.17), channel_id=1, source_target_pairs={{0,3},{1,0},{2,1},{3,2},{4,7},{5,4},{6,5},{7,6},{8,11},{9,8},{10,9... | collective-permute-start | bytes 786440 | tf_op jit(solution)/shard_map/ppermute | solution.py:51
  139.9 21.1 %all-to-all-start.2 = ((bf16[128,2,128]{2,1,0:T(2,128)(2,1)}), bf16[128,2,128]{2,1,0:T(2,128)(2,1)S(1)}, u32[]{:S(2)}, u32[]{:S(2)}) async-start(bf16[128,2,128]{2,1,0:T(2,128)(2,1)} %shard_map.129), calls=%async_computation.2 | async-start | bytes 131072 | tf_op jit(solution)/shard_map/all_to_all | solution.py:459
  146.4 10.9 %collective-permute-start.8 = (bf16[8,256]{1,0:T(8,128)(2,1)S(1)}, bf16[8,256]{1,0:T(8,128)(2,1)S(1)}, u32[]{:S(2)}, u32[]{:S(2)}) collective-permute-start(bf16[8,256]{1,0:T(8,128)(2,1)S(1)} %get-tuple-element.26), channel_id=1, source_target_pairs={{0,4},{4,8},{8,12},{12,16},{16,20},{20,24},{24,28},{28,32},{32,36}... | collective-permute-start | bytes 12296 | tf_op jit(solution)/shard_map/ppermute | solution.py:57
  148.4 8.9 %collective-permute-start.9 = (bf16[8,256]{1,0:T(8,128)(2,1)S(1)}, bf16[8,256]{1,0:T(8,128)(2,1)S(1)}, u32[]{:S(2)}, u32[]{:S(2)}) collective-permute-start(bf16[8,256]{1,0:T(8,128)(2,1)S(1)} %get-tuple-element.25), channel_id=1, source_target_pairs={{4,0},{8,4},{12,8},{16,12},{20,16},{24,20},{28,24},{32,28},{36,32}... | collective-permute-start | bytes 12296 | tf_op jit(solution)/shard_map/ppermute | solution.py:57
  164.3 16.8 %collective-permute-start.10 = (bf16[128,512]{1,0:T(8,128)(2,1)}, bf16[128,512]{1,0:T(8,128)(2,1)S(1)}, u32[]{:S(2)}, u32[]{:S(2)}) collective-permute-start(bf16[128,512]{1,0:T(8,128)(2,1)} %get-tuple-element.22), channel_id=1, source_target_pairs={{0,1},{1,2},{2,3},{3,0},{4,5},{5,6},{6,7},{7,4},{8,9},{9,10},{10,1... | collective-permute-start | bytes 393224 | tf_op jit(solution)/shard_map/ppermute | solution.py:51
  167.9 13.2 %collective-permute-start.11 = (bf16[128,512]{1,0:T(8,128)(2,1)}, bf16[128,512]{1,0:T(8,128)(2,1)S(1)}, u32[]{:S(2)}, u32[]{:S(2)}) collective-permute-start(bf16[128,512]{1,0:T(8,128)(2,1)} %get-tuple-element.23), channel_id=1, source_target_pairs={{0,2},{1,3},{2,0},{3,1},{4,6},{5,7},{6,4},{7,5},{8,10},{9,11},{10,... | collective-permute-start | bytes 393224 | tf_op jit(solution)/shard_map/ppermute | solution.py:51
  172.4 8.7 %collective-permute-start.12 = (bf16[128,512]{1,0:T(8,128)(2,1)}, bf16[128,512]{1,0:T(8,128)(2,1)S(1)}, u32[]{:S(2)}, u32[]{:S(2)}) collective-permute-start(bf16[128,512]{1,0:T(8,128)(2,1)} %get-tuple-element.24), channel_id=1, source_target_pairs={{0,3},{1,0},{2,1},{3,2},{4,7},{5,4},{6,5},{7,6},{8,11},{9,8},{10,9... | collective-permute-start | bytes 393224 | tf_op jit(solution)/shard_map/ppermute | solution.py:51
  181.1 0.7 copy-start.5
  181.1 0.7 copy-start.6
  (4 other events, 2.5 us)
Sparse Core Ops, SparseCore 0:
  20.1 113.7 all-gather.1

commit v9 on v8

--- a/solution.py
+++ b/solution.py
@@ -448,8 +448,9 @@
         flops=2 * rows * model * 2 * LANES,
         moved=3_000_000,
     )
-    rim_before = neighbours(pool_input[rows - rim_width :], SP, 1)
-    rim_after = neighbours(pool_input[:rim_width], SP, -1)
+    last, leading = (pool_input[rows - rim_width :], pool_input[:rim_width])
+    rim_before = neighbours(last, SP, 1)
+    rim_after = neighbours(leading, SP, -1)
     states = call(
         scan_kernel,
         shape_of(positions, 2, LANES),

time: 197 us -> 197 us (level)
  no operation moved by 1% of the time
where the time goes in v9:
time: 197 us; the launch traced here: 196 us
  blocking collectives  77.3 us (39%)
  starting transfers between devices  50.8 us (26%)
  Pallas kernels  28.8 us (15%)
  waiting for transfers between devices  16.7 us (8%)
  between operations  13.7 us (7%)
  local copies, waits for them, and re-layouts  5.84 us (3%)
  other arithmetic  3.03 us (2%)
    all_to_all x1, blocking collectives, shards(): weight_own = lax.all_to_all(copies, CHIPS, 0, 0, tiled=True)  56 us
    ppermute x11, starting transfers between devices, shifted(): lax.ppermute(value, axis, [(i, (i + step) % devices) for i in range(devic...  37.1 us
    pallas_call x7, Pallas kernels, call(): pl.pallas_call(kernel, in_specs=[smem] * scalars + [anywhere] * far + [vm...  28.8 us
    all_to_all x1, blocking collectives, shards(): received = lax.all_to_all(packed, SP, 0, 0, tiled=True)  21.3 us
    ppermute x11, waiting for transfers between devices, shifted(): lax.ppermute(value, axis, [(i, (i + step) % devices) for i in range(devic...  16.6 us
    ppermute x2, starting transfers between devices, neighbours(): return lax.ppermute(value, axes, pairs)  7.84 us
    all_to_all x1, starting transfers between devices, shards(): entering = lax.all_to_all(states, SP, 0, 0, tiled=True)  5.81 us
    unnamed x28, local copies, waits for them, and re-layouts  5.01 us
  transfers between devices with their start and end apart: 15, of which 5 were waited for; matrix products, arithmetic and copies ran while one was open for 2% of the time, Pallas kernels for 11%

profile of v9, /device:TPU:66, one launch (start us, length us, event | category | flops | bytes accessed | tf_op | source)
XLA Modules:
  0.0 196.1 jit_solution(7178769678932208803)
XLA Ops:
  7.3 3.4 %collective-permute-start = (bf16[16,512]{1,0:T(8,128)(2,1)S(1)}, bf16[16,512]{1,0:T(8,128)(2,1)S(1)}, u32[]{:S(2)}, u32[]{:S(2)}) collective-permute-start(bf16[16,512]{1,0:T(8,128)(2,1)S(1)} %maximum_bitcast_fusion), channel_id=1, source_target_pairs={{0,1},{1,2},{2,3},{3,0},{4,5},{5,6},{6,7},{7,4},{8,9},{9,10},{10,1... | collective-permute-start | bytes 49160 | tf_op jit(solution)/shard_map/ppermute | solution.py:51
  10.6 3.0 %collective-permute-start.1 = (bf16[16,512]{1,0:T(8,128)(2,1)S(1)}, bf16[16,512]{1,0:T(8,128)(2,1)S(1)}, u32[]{:S(2)}, u32[]{:S(2)}) collective-permute-start(bf16[16,512]{1,0:T(8,128)(2,1)S(1)} %maximum_bitcast_fusion), channel_id=1, source_target_pairs={{0,2},{1,3},{2,0},{3,1},{4,6},{5,7},{6,4},{7,5},{8,10},{9,11},{10,... | collective-permute-start | bytes 49160 | tf_op jit(solution)/shard_map/ppermute | solution.py:51
  13.7 4.1 %collective-permute-start.2 = (bf16[16,512]{1,0:T(8,128)(2,1)S(1)}, bf16[16,512]{1,0:T(8,128)(2,1)S(1)}, u32[]{:S(2)}, u32[]{:S(2)}) collective-permute-start(bf16[16,512]{1,0:T(8,128)(2,1)S(1)} %maximum_bitcast_fusion), channel_id=1, source_target_pairs={{0,3},{1,0},{2,1},{3,2},{4,7},{5,4},{6,5},{7,6},{8,11},{9,8},{10,9... | collective-permute-start | bytes 49160 | tf_op jit(solution)/shard_map/ppermute | solution.py:51
  20.8 56.0 %all_to_all.15.weight_own = bf16[64,16,768]{2,1,0:T(8,128)(2,1)S(1)} all-to-all(bf16[64,16,768]{2,1,0:T(8,128)(2,1)S(1)} %broadcast_in_dim.4), channel_id=1, replica_groups=mesh['sp_0'=8,'sp_1'=8,'sp_2'=2,'tp'=4] {'sp_0','sp_1'}, dimensions={0} | all-to-all | bytes 3145728 | tf_op jit(solution)/shard_map/all_to_all | solution.py:400
  76.8 2.0 %collective-permute-start.7 = (bf16[64,16,768]{2,1,0:T(8,128)(2,1)S(1)}, bf16[64,16,768]{2,1,0:T(8,128)(2,1)}, u32[]{:S(2)}, u32[]{:S(2)}) collective-permute-start(bf16[64,16,768]{2,1,0:T(8,128)(2,1)S(1)} %all_to_all.15.weight_own), channel_id=1, source_target_pairs={{0,4},{4,0},{1,5},{5,1},{2,6},{6,2},{3,7},{7,3},{8,12},{12,8},{9,1... | collective-permute-start | bytes 4718600 | tf_op jit(solution)/shard_map/ppermute | solution.py:51
  79.3 2.6 %collective-permute-start.3 = (bf16[128,2048]{1,0:T(8,128)(2,1)S(1)}, bf16[128,2048]{1,0:T(8,128)(2,1)S(1)}, u32[]{:S(2)}, u32[]{:S(2)}) collective-permute-start(bf16[128,2048]{1,0:T(8,128)(2,1)S(1)} %fusion.1.own), channel_id=1, source_target_pairs={{0,1},{1,2},{2,3},{3,0},{4,5},{5,6},{6,7},{7,4},{8,9},{9,10},{10,1... | collective-permute-start | bytes 1572872 | tf_op jit(solution)/shard_map/ppermute | solution.py:51
  81.8 3.3 %collective-permute-start.4 = (bf16[128,2048]{1,0:T(8,128)(2,1)S(1)}, bf16[128,2048]{1,0:T(8,128)(2,1)S(1)}, u32[]{:S(2)}, u32[]{:S(2)}) collective-permute-start(bf16[128,2048]{1,0:T(8,128)(2,1)S(1)} %fusion.1.own), channel_id=1, source_target_pairs={{0,3},{1,0},{2,1},{3,2},{4,7},{5,4},{6,5},{7,6},{8,11},{9,8},{10,9... | collective-permute-start | bytes 1572872 | tf_op jit(solution)/shard_map/ppermute | solution.py:51
  85.1 10.4 %collective-permute-done.3.before = bf16[128,2048]{1,0:T(8,128)(2,1)S(1)} collective-permute-done((bf16[128,2048]{1,0:T(8,128)(2,1)S(1)}, bf16[128,2048]{1,0:T(8,128)(2,1)S(1)}, u32[]{:S(2)}, u32[]{:S(2)}) %collective-permute-start.3) | collective-permute-done | bytes 524320 | tf_op jit(solution)/shard_map/ppermute | solution.py:51
  95.5 3.0 %collective-permute-start.5 = (bf16[64,2048]{1,0:T(8,128)(2,1)S(1)}, bf16[64,2048]{1,0:T(8,128)(2,1)}, u32[]{:S(2)}, u32[]{:S(2)}) collective-permute-start(bf16[64,2048]{1,0:T(8,128)(2,1)S(1)} %slice.16), channel_id=1, source_target_pairs={{0,1},{1,2},{2,3},{3,0},{4,5},{5,6},{6,7},{7,4},{8,9},{9,10},{10,1... | collective-permute-start | bytes 786440 | tf_op jit(solution)/shard_map/ppermute | solution.py:51
  99.0 3.1 %collective-permute-start.6 = (bf16[64,2048]{1,0:T(8,128)(2,1)S(1)}, bf16[64,2048]{1,0:T(8,128)(2,1)}, u32[]{:S(2)}, u32[]{:S(2)}) collective-permute-start(bf16[64,2048]{1,0:T(8,128)(2,1)S(1)} %slice.17), channel_id=1, source_target_pairs={{0,3},{1,0},{2,1},{3,2},{4,7},{5,4},{6,5},{7,6},{8,11},{9,8},{10,9... | collective-permute-start | bytes 786440 | tf_op jit(solution)/shard_map/ppermute | solution.py:51
  106.3 2.5 %collective-permute-done.6.far_end = bf16[64,2048]{1,0:T(8,128)(2,1)} collective-permute-done((bf16[64,2048]{1,0:T(8,128)(2,1)S(1)}, bf16[64,2048]{1,0:T(8,128)(2,1)}, u32[]{:S(2)}, u32[]{:S(2)}) %collective-permute-start.6) | collective-permute-done | bytes 262176 | tf_op jit(solution)/shard_map/ppermute | solution.py:51
  108.9 7.4 %shard_map.127 = (bf16[512,512]{1,0:T(8,128)(2,1)}, bf16[512,256]{1,0:T(8,128)(2,1)}, f32[2,512,128]{2,1,0:T(8,128)}, bf16[128,3,128]{2,1,0:T(4,128)(2,1)}) custom-call(s32[4]{0:T(128)} %pad_add_fusion.place, bf16[128,2048]{1,0:T(8,128)(2,1)} %copy-done.2, bf16[128,2048]{1,0:T(8,128)(2,1)} %copy-done.8, bf16[128,2048]{1,0:T(8,128)(2,1)} %copy-done.9, ...), custom_call_target="tpu_custom_call" | custom-call | flops 1879048192 | bytes 10000000 | tf_op jit(solution)/shard_map/pallas_call | solution.py:38
  116.2 21.3 %all_to_all.16.received = bf16[128,3,128]{2,1,0:T(4,128)(2,1)} all-to-all(bf16[128,3,128]{2,1,0:T(4,128)(2,1)} %get-tuple-element.19), channel_id=1, replica_groups=mesh['sp_0'=8,'sp_1'=8,'sp_2'=2,'tp'=4] {'sp_0','sp_1','sp_2'}, dimensions={0} | all-to-all | bytes 196608 | tf_op jit(solution)/shard_map/all_to_all | solution.py:442
  137.5 2.3 %shard_map.129 = bf16[128,2,128]{2,1,0:T(2,128)(2,1)} custom-call(s32[1]{0:T(128)} %bitcast.3.place, bf16[128,3,128]{2,1,0:T(4,128)(2,1)} %all_to_all.16.received, f32[2,128,128]{2,1,0:T(8,128)} %bitcast.8), custom_call_target="tpu_custom_call" | custom-call | flops 40000000 | tf_op jit(solution)/shard_map/pallas_call | solution.py:38
  139.9 5.8 %all-to-all-start.2 = ((bf16[128,2,128]{2,1,0:T(2,128)(2,1)}), bf16[128,2,128]{2,1,0:T(2,128)(2,1)S(1)}, u32[]{:S(2)}, u32[]{:S(2)}) async-start(bf16[128,2,128]{2,1,0:T(2,128)(2,1)} %shard_map.129), calls=%async_computation.2 | async-start | bytes 131072 | tf_op jit(solution)/shard_map/all_to_all | solution.py:460
  148.4 5.8 %collective-permute-start.9 = (bf16[8,256]{1,0:T(8,128)(2,1)S(1)}, bf16[8,256]{1,0:T(8,128)(2,1)S(1)}, u32[]{:S(2)}, u32[]{:S(2)}) collective-permute-start(bf16[8,256]{1,0:T(8,128)(2,1)S(1)} %get-tuple-element.25), channel_id=1, source_target_pairs={{4,0},{8,4},{12,8},{16,12},{20,16},{24,20},{28,24},{32,28},{36,32}... | collective-permute-start | bytes 12296 | tf_op jit(solution)/shard_map/ppermute | solution.py:57
  154.2 3.0 %shard_map.128 = (f32[512,256]{1,0:T(8,128)}, bf16[512,256]{1,0:T(8,128)(2,1)}) custom-call(bf16[512,512]{1,0:T(8,128)(2,1)} %get-tuple-element.15.qkv, f32[2,512,128]{2,1,0:T(8,128)} %get-tuple-element.16.logs), custom_call_target="tpu_custom_call" | custom-call | flops 536870912 | bytes 3000000 | tf_op jit(solution)/shard_map/pallas_call | solution.py:38
  158.4 2.5 %shard_map.130.pooled = bf16[512,256]{1,0:T(8,128)(2,1)} custom-call(s32[4]{0:T(128)} %pad_add_fusion.place, bf16[512,256]{1,0:T(8,128)(2,1)} %get-tuple-element.20.pool_input, bf16[8,256]{1,0:T(8,128)(2,1)} %copy-done.11, bf16[8,256]{1,0:T(8,128)(2,1)} %copy-done.12, bf16[4,256,256]{2,1,0:T(8,128)(2,1)} %group_map.1), custom_call_target="tpu_custom_call" | custom-call | flops 67108864 | bytes 1000000 | tf_op jit(solution)/shard_map/pallas_call | solution.py:38
  161.6 2.7 %shard_map.131 = (bf16[128,512]{1,0:T(8,128)(2,1)}, bf16[128,512]{1,0:T(8,128)(2,1)}, bf16[128,512]{1,0:T(8,128)(2,1)}, bf16[128,512]{1,0:T(8,128)(2,1)}) custom-call(s32[4]{0:T(128)} %pad_add_fusion.place, f32[512,256]{1,0:T(8,128)} %get-tuple-element.17.part, bf16[512,256]{1,0:T(8,128)(2,1)} %get-tuple-element.18.query, bf16[128,2,128]{2,1,0:T(2,128)(2,1)} %copy-done.4, ...), custom_call_target="tpu_custom_call" | custom-call | flops 100000000 | bytes 2000000 | tf_op jit(solution)/shard_map/pallas_call | solution.py:38
  164.3 3.6 %collective-permute-start.10 = (bf16[128,512]{1,0:T(8,128)(2,1)}, bf16[128,512]{1,0:T(8,128)(2,1)S(1)}, u32[]{:S(2)}, u32[]{:S(2)}) collective-permute-start(bf16[128,512]{1,0:T(8,128)(2,1)} %get-tuple-element.22), channel_id=1, source_target_pairs={{0,1},{1,2},{2,3},{3,0},{4,5},{5,6},{6,7},{7,4},{8,9},{9,10},{10,1... | collective-permute-start | bytes 393224 | tf_op jit(solution)/shard_map/ppermute | solution.py:51
  167.9 4.5 %collective-permute-start.11 = (bf16[128,512]{1,0:T(8,128)(2,1)}, bf16[128,512]{1,0:T(8,128)(2,1)S(1)}, u32[]{:S(2)}, u32[]{:S(2)}) collective-permute-start(bf16[128,512]{1,0:T(8,128)(2,1)} %get-tuple-element.23), channel_id=1, source_target_pairs={{0,2},{1,3},{2,0},{3,1},{4,6},{5,7},{6,4},{7,5},{8,10},{9,11},{10,... | collective-permute-start | bytes 393224 | tf_op jit(solution)/shard_map/ppermute | solution.py:51
  172.4 4.5 %collective-permute-start.12 = (bf16[128,512]{1,0:T(8,128)(2,1)}, bf16[128,512]{1,0:T(8,128)(2,1)S(1)}, u32[]{:S(2)}, u32[]{:S(2)}) collective-permute-start(bf16[128,512]{1,0:T(8,128)(2,1)} %get-tuple-element.24), channel_id=1, source_target_pairs={{0,3},{1,0},{2,1},{3,2},{4,7},{5,4},{6,5},{7,6},{8,11},{9,8},{10,9... | collective-permute-start | bytes 393224 | tf_op jit(solution)/shard_map/ppermute | solution.py:51
  177.0 4.1 %shard_map.132.own_part = bf16[128,2048]{1,0:T(8,128)(2,1)} custom-call(bf16[2048,2048]{1,0:T(8,128)(2,1)} %all-gather.2.cloned.1.call-done.weights, bf16[128,512]{1,0:T(8,128)(2,1)} %get-tuple-element.21.mine), custom_call_target="tpu_custom_call" | custom-call | flops 268435456 | bytes 2097152 | tf_op jit(solution)/shard_map/pallas_call | solution.py:38
  182.5 6.8 %shard_map.133 = bf16[128,2048]{1,0:T(8,128)(2,1)} custom-call(bf16[2048,2048]{1,0:T(8,128)(2,1)} %all-gather.2.cloned.1.call-done.weights, bf16[128,2048]{1,0:T(8,128)(2,1)} %shard_map.132.own_part, bf16[128,512]{1,0:T(8,128)(2,1)} %copy-done.5, bf16[128,512]{1,0:T(8,128)(2,1)} %copy-done.6, bf16[128,512]{1,0:T(8,128)(2,1)} %copy-done.7), custom_call_target="tpu_custom_call" | custom-call | flops 805306368 | bytes 6291456 | tf_op jit(solution)/shard_map/pallas_call | solution.py:38
  (55 shorter events, 14.7 us)
Async XLA Ops:
  6.5 170.4 %all-gather.2.cloned.1.call-start = ((), (), s32[]{:S(2)}) async-start(), calls=%async_computation.3 | async-start | bytes 8454144 | tf_op jit(solution)/shard_map/all_gather | solution.py:411
  7.3 10.5 %collective-permute-start = (bf16[16,512]{1,0:T(8,128)(2,1)S(1)}, bf16[16,512]{1,0:T(8,128)(2,1)S(1)}, u32[]{:S(2)}, u32[]{:S(2)}) collective-permute-start(bf16[16,512]{1,0:T(8,128)(2,1)S(1)} %maximum_bitcast_fusion), channel_id=1, source_target_pairs={{0,1},{1,2},{2,3},{3,0},{4,5},{5,6},{6,7},{7,4},{8,9},{9,10},{10,1... | collective-permute-start | bytes 49160 | tf_op jit(solution)/shard_map/ppermute | solution.py:51
  10.6 7.1 %collective-permute-start.1 = (bf16[16,512]{1,0:T(8,128)(2,1)S(1)}, bf16[16,512]{1,0:T(8,128)(2,1)S(1)}, u32[]{:S(2)}, u32[]{:S(2)}) collective-permute-start(bf16[16,512]{1,0:T(8,128)(2,1)S(1)} %maximum_bitcast_fusion), channel_id=1, source_target_pairs={{0,2},{1,3},{2,0},{3,1},{4,6},{5,7},{6,4},{7,5},{8,10},{9,11},{10,... | collective-permute-start | bytes 49160 | tf_op jit(solution)/shard_map/ppermute | solution.py:51
  13.7 5.6 %collective-permute-start.2 = (bf16[16,512]{1,0:T(8,128)(2,1)S(1)}, bf16[16,512]{1,0:T(8,128)(2,1)S(1)}, u32[]{:S(2)}, u32[]{:S(2)}) collective-permute-start(bf16[16,512]{1,0:T(8,128)(2,1)S(1)} %maximum_bitcast_fusion), channel_id=1, source_target_pairs={{0,3},{1,0},{2,1},{3,2},{4,7},{5,4},{6,5},{7,6},{8,11},{9,8},{10,9... | collective-permute-start | bytes 49160 | tf_op jit(solution)/shard_map/ppermute | solution.py:51
  20.8 58.1 %copy-start = (bf16[128,2048]{1,0:T(8,128)(2,1)S(1)}, bf16[128,2048]{1,0:T(8,128)(2,1)}, u32[]{:S(2)}) copy-start(bf16[128,2048]{1,0:T(8,128)(2,1)} %param.13) | copy-start | bytes 1572868
  76.8 26.3 %copy-start.1 = (bf16[64,16,768]{2,1,0:T(8,128)(2,1)}, bf16[64,16,768]{2,1,0:T(8,128)(2,1)S(1)}, u32[]{:S(2)}) copy-start(bf16[64,16,768]{2,1,0:T(8,128)(2,1)S(1)} %all_to_all.15.weight_own) | copy-start | bytes 4718596
  76.8 25.3 %copy-start.3 = (bf16[2048,64]{0,1:T(8,128)(2,1)S(1)}, bf16[2048,64]{0,1:T(8,128)(2,1)}, u32[]{:S(2)}) copy-start(bf16[2048,64]{0,1:T(8,128)(2,1)} %param.18) | copy-start | bytes 786436
  76.8 32.0 %collective-permute-start.7 = (bf16[64,16,768]{2,1,0:T(8,128)(2,1)S(1)}, bf16[64,16,768]{2,1,0:T(8,128)(2,1)}, u32[]{:S(2)}, u32[]{:S(2)}) collective-permute-start(bf16[64,16,768]{2,1,0:T(8,128)(2,1)S(1)} %all_to_all.15.weight_own), channel_id=1, source_target_pairs={{0,4},{4,0},{1,5},{5,1},{2,6},{6,2},{3,7},{7,3},{8,12},{12,8},{9,1... | collective-permute-start | bytes 4718600 | tf_op jit(solution)/shard_map/ppermute | solution.py:51
  79.1 24.1 %copy-start.10 = (f32[2,512]{1,0:T(2,128)S(1)}, f32[2,512]{1,0:T(2,128)}, u32[]{:S(2)}) copy-start(f32[2,512]{1,0:T(2,128)} %param.21) | copy-start | bytes 12292
  79.3 29.6 %copy-start.2 = (bf16[128,2048]{1,0:T(8,128)(2,1)}, bf16[128,2048]{1,0:T(8,128)(2,1)S(1)}, u32[]{:S(2)}) copy-start(bf16[128,2048]{1,0:T(8,128)(2,1)S(1)} %fusion.1.own) | copy-start | bytes 1572868
  79.3 16.2 %collective-permute-start.3 = (bf16[128,2048]{1,0:T(8,128)(2,1)S(1)}, bf16[128,2048]{1,0:T(8,128)(2,1)S(1)}, u32[]{:S(2)}, u32[]{:S(2)}) collective-permute-start(bf16[128,2048]{1,0:T(8,128)(2,1)S(1)} %fusion.1.own), channel_id=1, source_target_pairs={{0,1},{1,2},{2,3},{3,0},{4,5},{5,6},{6,7},{7,4},{8,9},{9,10},{10,1... | collective-permute-start | bytes 1572872 | tf_op jit(solution)/shard_map/ppermute | solution.py:51
  81.8 17.1 %collective-permute-start.4 = (bf16[128,2048]{1,0:T(8,128)(2,1)S(1)}, bf16[128,2048]{1,0:T(8,128)(2,1)S(1)}, u32[]{:S(2)}, u32[]{:S(2)}) collective-permute-start(bf16[128,2048]{1,0:T(8,128)(2,1)S(1)} %fusion.1.own), channel_id=1, source_target_pairs={{0,3},{1,0},{2,1},{3,2},{4,7},{5,4},{6,5},{7,6},{8,11},{9,8},{10,9... | collective-permute-start | bytes 1572872 | tf_op jit(solution)/shard_map/ppermute | solution.py:51
  95.5 13.4 %copy-start.8 = (bf16[128,2048]{1,0:T(8,128)(2,1)}, bf16[128,2048]{1,0:T(8,128)(2,1)S(1)}, u32[]{:S(2)}) copy-start(bf16[128,2048]{1,0:T(8,128)(2,1)S(1)} %collective-permute-done.3.before) | copy-start | bytes 1572868
  95.5 10.8 %collective-permute-start.5 = (bf16[64,2048]{1,0:T(8,128)(2,1)S(1)}, bf16[64,2048]{1,0:T(8,128)(2,1)}, u32[]{:S(2)}, u32[]{:S(2)}) collective-permute-start(bf16[64,2048]{1,0:T(8,128)(2,1)S(1)} %slice.16), channel_id=1, source_target_pairs={{0,1},{1,2},{2,3},{3,0},{4,5},{5,6},{6,7},{7,4},{8,9},{9,10},{10,1... | collective-permute-start | bytes 786440 | tf_op jit(solution)/shard_map/ppermute | solution.py:51
  98.9 3.2 %copy-start.9 = (bf16[128,2048]{1,0:T(8,128)(2,1)}, bf16[128,2048]{1,0:T(8,128)(2,1)S(1)}, u32[]{:S(2)}) copy-start(bf16[128,2048]{1,0:T(8,128)(2,1)S(1)} %collective-permute-done.4.after) | copy-start | bytes 1572868
  99.0 9.9 %collective-permute-start.6 = (bf16[64,2048]{1,0:T(8,128)(2,1)S(1)}, bf16[64,2048]{1,0:T(8,128)(2,1)}, u32[]{:S(2)}, u32[]{:S(2)}) collective-permute-start(bf16[64,2048]{1,0:T(8,128)(2,1)S(1)} %slice.17), channel_id=1, source_target_pairs={{0,3},{1,0},{2,1},{3,2},{4,7},{5,4},{6,5},{7,6},{8,11},{9,8},{10,9... | collective-permute-start | bytes 786440 | tf_op jit(solution)/shard_map/ppermute | solution.py:51
  139.9 21.1 %all-to-all-start.2 = ((bf16[128,2,128]{2,1,0:T(2,128)(2,1)}), bf16[128,2,128]{2,1,0:T(2,128)(2,1)S(1)}, u32[]{:S(2)}, u32[]{:S(2)}) async-start(bf16[128,2,128]{2,1,0:T(2,128)(2,1)} %shard_map.129), calls=%async_computation.2 | async-start | bytes 131072 | tf_op jit(solution)/shard_map/all_to_all | solution.py:460
  146.4 10.9 %collective-permute-start.8 = (bf16[8,256]{1,0:T(8,128)(2,1)S(1)}, bf16[8,256]{1,0:T(8,128)(2,1)S(1)}, u32[]{:S(2)}, u32[]{:S(2)}) collective-permute-start(bf16[8,256]{1,0:T(8,128)(2,1)S(1)} %get-tuple-element.26), channel_id=1, source_target_pairs={{0,4},{4,8},{8,12},{12,16},{16,20},{20,24},{24,28},{28,32},{32,36}... | collective-permute-start | bytes 12296 | tf_op jit(solution)/shard_map/ppermute | solution.py:57
  148.4 8.9 %collective-permute-start.9 = (bf16[8,256]{1,0:T(8,128)(2,1)S(1)}, bf16[8,256]{1,0:T(8,128)(2,1)S(1)}, u32[]{:S(2)}, u32[]{:S(2)}) collective-permute-start(bf16[8,256]{1,0:T(8,128)(2,1)S(1)} %get-tuple-element.25), channel_id=1, source_target_pairs={{4,0},{8,4},{12,8},{16,12},{20,16},{24,20},{28,24},{32,28},{36,32}... | collective-permute-start | bytes 12296 | tf_op jit(solution)/shard_map/ppermute | solution.py:57
  164.3 16.8 %collective-permute-start.10 = (bf16[128,512]{1,0:T(8,128)(2,1)}, bf16[128,512]{1,0:T(8,128)(2,1)S(1)}, u32[]{:S(2)}, u32[]{:S(2)}) collective-permute-start(bf16[128,512]{1,0:T(8,128)(2,1)} %get-tuple-element.22), channel_id=1, source_target_pairs={{0,1},{1,2},{2,3},{3,0},{4,5},{5,6},{6,7},{7,4},{8,9},{9,10},{10,1... | collective-permute-start | bytes 393224 | tf_op jit(solution)/shard_map/ppermute | solution.py:51
  167.9 13.2 %collective-permute-start.11 = (bf16[128,512]{1,0:T(8,128)(2,1)}, bf16[128,512]{1,0:T(8,128)(2,1)S(1)}, u32[]{:S(2)}, u32[]{:S(2)}) collective-permute-start(bf16[128,512]{1,0:T(8,128)(2,1)} %get-tuple-element.23), channel_id=1, source_target_pairs={{0,2},{1,3},{2,0},{3,1},{4,6},{5,7},{6,4},{7,5},{8,10},{9,11},{10,... | collective-permute-start | bytes 393224 | tf_op jit(solution)/shard_map/ppermute | solution.py:51
  172.4 8.7 %collective-permute-start.12 = (bf16[128,512]{1,0:T(8,128)(2,1)}, bf16[128,512]{1,0:T(8,128)(2,1)S(1)}, u32[]{:S(2)}, u32[]{:S(2)}) collective-permute-start(bf16[128,512]{1,0:T(8,128)(2,1)} %get-tuple-element.24), channel_id=1, source_target_pairs={{0,3},{1,0},{2,1},{3,2},{4,7},{5,4},{6,5},{7,6},{8,11},{9,8},{10,9... | collective-permute-start | bytes 393224 | tf_op jit(solution)/shard_map/ppermute | solution.py:51
  181.1 0.7 copy-start.5
  181.1 0.7 copy-start.6
  (4 other events, 2.5 us)
Sparse Core Ops, SparseCore 0:
  20.1 113.7 all-gather.1

commit v10 on v8

--- a/solution.py
+++ b/solution.py
@@ -111,7 +111,7 @@
     weight_ref[:, pl.ds(1 - core, 1)] = weight_other[...][:, None]
     rows, width = tokens_ref.shape
     tokens = tokens_ref[...]
-    low_rank = matmul(tokens, inner[...]).astype(bf16)
+    low_rank = matmul(tokens, inner[...], ((1,), (1,))).astype(bf16)
     projected = matmul(tokens, weight_ref[...].reshape(width, -1)).astype(bf16)
     qkv = projected[:, : 4 * LANES]
     qkv_out[...] = qkv
@@ -129,7 +129,8 @@
     pre = matmul(low_rank, outer_both) + bias_both
     gate = jnp.minimum(pre, 0.0) - jnp.log1p(jnp.exp(-jnp.abs(pre)))
     lane = lax.broadcasted_iota(jnp.int32, (rows, LANES), 1)
-    spikes = jnp.where(lane < KEY_CHANNELS, spike[:, 0:1], spike[:, 1:2])
+    spike_rows = jnp.concatenate([spike[...], jnp.zeros((6, rows), f32)], axis=0).T
+    spikes = jnp.where(lane < KEY_CHANNELS, spike_rows[:, 0:1], spike_rows[:, 1:2])
     decay = gate * (1.0 / gate_norm_factor) + jnp.concatenate([spikes, spikes], axis=1)
     size = LANES
     row_ids = lax.broadcasted_iota(jnp.int32, (size, size), 0)
@@ -427,10 +428,10 @@
             far_end,
             weight_own,
             weight_other,
-            decay_inner_weight,
+            decay_inner_weight.T,
             decay_outer_weight,
             channel_decay_bias,
-            spike_log_decay.T,
+            spike_log_decay,
         ),
         scratch=(
             pltpu.VMEM((rows, model), bf16),

time: 197 us -> 197 us (level)
    unnamed x28 -> x24, local copies, waits for them, and re-layouts: 5.01 us -> 3.13 us
  transfers between devices with their start and end apart: 15 -> 15, of which waited for: 5 -> 5; matrix products, arithmetic and copies ran while one was open for 2% -> 1% of each run, Pallas kernels for 11% -> 11%
where the time goes in v10:
time: 197 us; the launch traced here: 196 us
  blocking collectives  77.4 us (39%)
  starting transfers between devices  50.6 us (26%)
  Pallas kernels  28.8 us (15%)
  waiting for transfers between devices  18.5 us (9%)
  between operations  13.7 us (7%)
  local copies, waits for them, and re-layouts  3.96 us (2%)
  other arithmetic  3.11 us (2%)
    all_to_all x1, blocking collectives, shards(): weight_own = lax.all_to_all(copies, CHIPS, 0, 0, tiled=True)  56 us
    ppermute x11, starting transfers between devices, shifted(): lax.ppermute(value, axis, [(i, (i + step) % devices) for i in range(devic...  37 us
    pallas_call x7, Pallas kernels, call(): pl.pallas_call(kernel, in_specs=[smem] * scalars + [anywhere] * far + [vm...  28.8 us
    all_to_all x1, blocking collectives, shards(): received = lax.all_to_all(packed, SP, 0, 0, tiled=True)  21.4 us
    ppermute x11, waiting for transfers between devices, shifted(): lax.ppermute(value, axis, [(i, (i + step) % devices) for i in range(devic...  18.4 us
    ppermute x2, starting transfers between devices, neighbours(): return lax.ppermute(value, axes, pairs)  7.84 us
    all_to_all x1, starting transfers between devices, shards(): entering = lax.all_to_all(states, SP, 0, 0, tiled=True)  5.71 us
  transfers between devices with their start and end apart: 15, of which 5 were waited for; matrix products, arithmetic and copies ran while one was open for 1% of the time, Pallas kernels for 11%

profile of v10, /device:TPU:66, one launch (start us, length us, event | category | flops | bytes accessed | tf_op | source)
XLA Modules:
  0.0 196.0 jit_solution(10490734479290217379)
XLA Ops:
  7.3 3.4 %collective-permute-start = (bf16[16,512]{1,0:T(8,128)(2,1)S(1)}, bf16[16,512]{1,0:T(8,128)(2,1)S(1)}, u32[]{:S(2)}, u32[]{:S(2)}) collective-permute-start(bf16[16,512]{1,0:T(8,128)(2,1)S(1)} %maximum_bitcast_fusion), channel_id=1, source_target_pairs={{0,1},{1,2},{2,3},{3,0},{4,5},{5,6},{6,7},{7,4},{8,9},{9,10},{10,1... | collective-permute-start | bytes 49160 | tf_op jit(solution)/shard_map/ppermute | solution.py:51
  10.6 3.0 %collective-permute-start.1 = (bf16[16,512]{1,0:T(8,128)(2,1)S(1)}, bf16[16,512]{1,0:T(8,128)(2,1)S(1)}, u32[]{:S(2)}, u32[]{:S(2)}) collective-permute-start(bf16[16,512]{1,0:T(8,128)(2,1)S(1)} %maximum_bitcast_fusion), channel_id=1, source_target_pairs={{0,2},{1,3},{2,0},{3,1},{4,6},{5,7},{6,4},{7,5},{8,10},{9,11},{10,... | collective-permute-start | bytes 49160 | tf_op jit(solution)/shard_map/ppermute | solution.py:51
  13.7 4.1 %collective-permute-start.2 = (bf16[16,512]{1,0:T(8,128)(2,1)S(1)}, bf16[16,512]{1,0:T(8,128)(2,1)S(1)}, u32[]{:S(2)}, u32[]{:S(2)}) collective-permute-start(bf16[16,512]{1,0:T(8,128)(2,1)S(1)} %maximum_bitcast_fusion), channel_id=1, source_target_pairs={{0,3},{1,0},{2,1},{3,2},{4,7},{5,4},{6,5},{7,6},{8,11},{9,8},{10,9... | collective-permute-start | bytes 49160 | tf_op jit(solution)/shard_map/ppermute | solution.py:51
  20.8 56.0 %all_to_all.15.weight_own = bf16[64,16,768]{2,1,0:T(8,128)(2,1)S(1)} all-to-all(bf16[64,16,768]{2,1,0:T(8,128)(2,1)S(1)} %broadcast_in_dim.4), channel_id=1, replica_groups=mesh['sp_0'=8,'sp_1'=8,'sp_2'=2,'tp'=4] {'sp_0','sp_1'}, dimensions={0} | all-to-all | bytes 3145728 | tf_op jit(solution)/shard_map/all_to_all | solution.py:401
  79.1 2.6 %collective-permute-start.3 = (bf16[128,2048]{1,0:T(8,128)(2,1)S(1)}, bf16[128,2048]{1,0:T(8,128)(2,1)S(1)}, u32[]{:S(2)}, u32[]{:S(2)}) collective-permute-start(bf16[128,2048]{1,0:T(8,128)(2,1)S(1)} %fusion.1.own), channel_id=1, source_target_pairs={{0,1},{1,2},{2,3},{3,0},{4,5},{5,6},{6,7},{7,4},{8,9},{9,10},{10,1... | collective-permute-start | bytes 1572872 | tf_op jit(solution)/shard_map/ppermute | solution.py:51
  81.7 3.3 %collective-permute-start.4 = (bf16[128,2048]{1,0:T(8,128)(2,1)S(1)}, bf16[128,2048]{1,0:T(8,128)(2,1)S(1)}, u32[]{:S(2)}, u32[]{:S(2)}) collective-permute-start(bf16[128,2048]{1,0:T(8,128)(2,1)S(1)} %fusion.1.own), channel_id=1, source_target_pairs={{0,3},{1,0},{2,1},{3,2},{4,7},{5,4},{6,5},{7,6},{8,11},{9,8},{10,9... | collective-permute-start | bytes 1572872 | tf_op jit(solution)/shard_map/ppermute | solution.py:51
  85.0 10.4 %collective-permute-done.3.before = bf16[128,2048]{1,0:T(8,128)(2,1)S(1)} collective-permute-done((bf16[128,2048]{1,0:T(8,128)(2,1)S(1)}, bf16[128,2048]{1,0:T(8,128)(2,1)S(1)}, u32[]{:S(2)}, u32[]{:S(2)}) %collective-permute-start.3) | collective-permute-done | bytes 524320 | tf_op jit(solution)/shard_map/ppermute | solution.py:51
  95.4 3.0 %collective-permute-start.5 = (bf16[64,2048]{1,0:T(8,128)(2,1)S(1)}, bf16[64,2048]{1,0:T(8,128)(2,1)S(1)}, u32[]{:S(2)}, u32[]{:S(2)}) collective-permute-start(bf16[64,2048]{1,0:T(8,128)(2,1)S(1)} %slice.16), channel_id=1, source_target_pairs={{0,1},{1,2},{2,3},{3,0},{4,5},{5,6},{6,7},{7,4},{8,9},{9,10},{10,1... | collective-permute-start | bytes 786440 | tf_op jit(solution)/shard_map/ppermute | solution.py:51
  98.8 3.1 %collective-permute-start.6 = (bf16[64,2048]{1,0:T(8,128)(2,1)S(1)}, bf16[64,2048]{1,0:T(8,128)(2,1)}, u32[]{:S(2)}, u32[]{:S(2)}) collective-permute-start(bf16[64,2048]{1,0:T(8,128)(2,1)S(1)} %slice.17), channel_id=1, source_target_pairs={{0,3},{1,0},{2,1},{3,2},{4,7},{5,4},{6,5},{7,6},{8,11},{9,8},{10,9... | collective-permute-start | bytes 786440 | tf_op jit(solution)/shard_map/ppermute | solution.py:51
  102.6 3.4 %collective-permute-done.5.far_top = bf16[64,2048]{1,0:T(8,128)(2,1)S(1)} collective-permute-done((bf16[64,2048]{1,0:T(8,128)(2,1)S(1)}, bf16[64,2048]{1,0:T(8,128)(2,1)S(1)}, u32[]{:S(2)}, u32[]{:S(2)}) %collective-permute-start.5) | collective-permute-done | bytes 262176 | tf_op jit(solution)/shard_map/ppermute | solution.py:51
  106.1 2.6 %collective-permute-done.6.far_end = bf16[64,2048]{1,0:T(8,128)(2,1)} collective-permute-done((bf16[64,2048]{1,0:T(8,128)(2,1)S(1)}, bf16[64,2048]{1,0:T(8,128)(2,1)}, u32[]{:S(2)}, u32[]{:S(2)}) %collective-permute-start.6) | collective-permute-done | bytes 262176 | tf_op jit(solution)/shard_map/ppermute | solution.py:51
  108.7 7.4 %shard_map.127 = (bf16[512,512]{1,0:T(8,128)(2,1)}, bf16[512,256]{1,0:T(8,128)(2,1)}, f32[2,512,128]{2,1,0:T(8,128)}, bf16[128,3,128]{2,1,0:T(4,128)(2,1)}) custom-call(s32[4]{0:T(128)} %pad_add_fusion.place, bf16[128,2048]{1,0:T(8,128)(2,1)} %copy-done.2, bf16[128,2048]{1,0:T(8,128)(2,1)} %copy-done.7, bf16[128,2048]{1,0:T(8,128)(2,1)} %copy-done.8, ...), custom_call_target="tpu_custom_call" | custom-call | flops 1879048192 | bytes 10000000 | tf_op jit(solution)/shard_map/pallas_call | solution.py:38
  116.1 21.4 %all_to_all.16.received = bf16[128,3,128]{2,1,0:T(4,128)(2,1)} all-to-all(bf16[128,3,128]{2,1,0:T(4,128)(2,1)} %get-tuple-element.19), channel_id=1, replica_groups=mesh['sp_0'=8,'sp_1'=8,'sp_2'=2,'tp'=4] {'sp_0','sp_1','sp_2'}, dimensions={0} | all-to-all | bytes 196608 | tf_op jit(solution)/shard_map/all_to_all | solution.py:443
  137.5 2.3 %shard_map.129 = bf16[128,2,128]{2,1,0:T(2,128)(2,1)} custom-call(s32[1]{0:T(128)} %bitcast.3.place, bf16[128,3,128]{2,1,0:T(4,128)(2,1)} %all_to_all.16.received, f32[2,128,128]{2,1,0:T(8,128)} %bitcast.7), custom_call_target="tpu_custom_call" | custom-call | flops 40000000 | tf_op jit(solution)/shard_map/pallas_call | solution.py:38
  139.8 5.7 %all-to-all-start.2 = ((bf16[128,2,128]{2,1,0:T(2,128)(2,1)}), bf16[128,2,128]{2,1,0:T(2,128)(2,1)S(1)}, u32[]{:S(2)}, u32[]{:S(2)}) async-start(bf16[128,2,128]{2,1,0:T(2,128)(2,1)} %shard_map.129), calls=%async_computation.2 | async-start | bytes 131072 | tf_op jit(solution)/shard_map/all_to_all | solution.py:460
  148.2 5.8 %collective-permute-start.9 = (bf16[8,256]{1,0:T(8,128)(2,1)S(1)}, bf16[8,256]{1,0:T(8,128)(2,1)S(1)}, u32[]{:S(2)}, u32[]{:S(2)}) collective-permute-start(bf16[8,256]{1,0:T(8,128)(2,1)S(1)} %get-tuple-element.25), channel_id=1, source_target_pairs={{4,0},{8,4},{12,8},{16,12},{20,16},{24,20},{28,24},{32,28},{36,32}... | collective-permute-start | bytes 12296 | tf_op jit(solution)/shard_map/ppermute | solution.py:57
  154.1 3.0 %shard_map.128 = (f32[512,256]{1,0:T(8,128)}, bf16[512,256]{1,0:T(8,128)(2,1)}) custom-call(bf16[512,512]{1,0:T(8,128)(2,1)} %get-tuple-element.15.qkv, f32[2,512,128]{2,1,0:T(8,128)} %get-tuple-element.16.logs), custom_call_target="tpu_custom_call" | custom-call | flops 536870912 | bytes 3000000 | tf_op jit(solution)/shard_map/pallas_call | solution.py:38
  158.3 2.6 %shard_map.130.pooled = bf16[512,256]{1,0:T(8,128)(2,1)} custom-call(s32[4]{0:T(128)} %pad_add_fusion.place, bf16[512,256]{1,0:T(8,128)(2,1)} %get-tuple-element.20.pool_input, bf16[8,256]{1,0:T(8,128)(2,1)} %copy-done.9, bf16[8,256]{1,0:T(8,128)(2,1)} %copy-done.10, bf16[4,256,256]{2,1,0:T(8,128)(2,1)} %group_map.1), custom_call_target="tpu_custom_call" | custom-call | flops 67108864 | bytes 1000000 | tf_op jit(solution)/shard_map/pallas_call | solution.py:38
  161.5 2.7 %shard_map.131 = (bf16[128,512]{1,0:T(8,128)(2,1)}, bf16[128,512]{1,0:T(8,128)(2,1)}, bf16[128,512]{1,0:T(8,128)(2,1)}, bf16[128,512]{1,0:T(8,128)(2,1)}) custom-call(s32[4]{0:T(128)} %pad_add_fusion.place, f32[512,256]{1,0:T(8,128)} %get-tuple-element.17.part, bf16[512,256]{1,0:T(8,128)(2,1)} %get-tuple-element.18.query, bf16[128,2,128]{2,1,0:T(2,128)(2,1)} %copy-done.3, ...), custom_call_target="tpu_custom_call" | custom-call | flops 100000000 | bytes 2000000 | tf_op jit(solution)/shard_map/pallas_call | solution.py:38
  164.1 3.6 %collective-permute-start.10 = (bf16[128,512]{1,0:T(8,128)(2,1)}, bf16[128,512]{1,0:T(8,128)(2,1)S(1)}, u32[]{:S(2)}, u32[]{:S(2)}) collective-permute-start(bf16[128,512]{1,0:T(8,128)(2,1)} %get-tuple-element.22), channel_id=1, source_target_pairs={{0,1},{1,2},{2,3},{3,0},{4,5},{5,6},{6,7},{7,4},{8,9},{9,10},{10,1... | collective-permute-start | bytes 393224 | tf_op jit(solution)/shard_map/ppermute | solution.py:51
  167.8 4.5 %collective-permute-start.11 = (bf16[128,512]{1,0:T(8,128)(2,1)}, bf16[128,512]{1,0:T(8,128)(2,1)S(1)}, u32[]{:S(2)}, u32[]{:S(2)}) collective-permute-start(bf16[128,512]{1,0:T(8,128)(2,1)} %get-tuple-element.23), channel_id=1, source_target_pairs={{0,2},{1,3},{2,0},{3,1},{4,6},{5,7},{6,4},{7,5},{8,10},{9,11},{10,... | collective-permute-start | bytes 393224 | tf_op jit(solution)/shard_map/ppermute | solution.py:51
  172.3 4.5 %collective-permute-start.12 = (bf16[128,512]{1,0:T(8,128)(2,1)}, bf16[128,512]{1,0:T(8,128)(2,1)S(1)}, u32[]{:S(2)}, u32[]{:S(2)}) collective-permute-start(bf16[128,512]{1,0:T(8,128)(2,1)} %get-tuple-element.24), channel_id=1, source_target_pairs={{0,3},{1,0},{2,1},{3,2},{4,7},{5,4},{6,5},{7,6},{8,11},{9,8},{10,9... | collective-permute-start | bytes 393224 | tf_op jit(solution)/shard_map/ppermute | solution.py:51
  176.9 4.1 %shard_map.132.own_part = bf16[128,2048]{1,0:T(8,128)(2,1)} custom-call(bf16[2048,2048]{1,0:T(8,128)(2,1)} %all-gather.2.cloned.1.call-done.weights, bf16[128,512]{1,0:T(8,128)(2,1)} %get-tuple-element.21.mine), custom_call_target="tpu_custom_call" | custom-call | flops 268435456 | bytes 2097152 | tf_op jit(solution)/shard_map/pallas_call | solution.py:38
  182.3 6.8 %shard_map.133 = bf16[128,2048]{1,0:T(8,128)(2,1)} custom-call(bf16[2048,2048]{1,0:T(8,128)(2,1)} %all-gather.2.cloned.1.call-done.weights, bf16[128,2048]{1,0:T(8,128)(2,1)} %shard_map.132.own_part, bf16[128,512]{1,0:T(8,128)(2,1)} %copy-done.4, bf16[128,512]{1,0:T(8,128)(2,1)} %copy-done.5, bf16[128,512]{1,0:T(8,128)(2,1)} %copy-done.6), custom_call_target="tpu_custom_call" | custom-call | flops 805306368 | bytes 6291456 | tf_op jit(solution)/shard_map/pallas_call | solution.py:38
  (51 shorter events, 13.0 us)
Async XLA Ops:
  6.5 170.3 %all-gather.2.cloned.1.call-start = ((), (), s32[]{:S(2)}) async-start(), calls=%async_computation.3 | async-start | bytes 8454144 | tf_op jit(solution)/shard_map/all_gather | solution.py:412
  7.3 10.5 %collective-permute-start = (bf16[16,512]{1,0:T(8,128)(2,1)S(1)}, bf16[16,512]{1,0:T(8,128)(2,1)S(1)}, u32[]{:S(2)}, u32[]{:S(2)}) collective-permute-start(bf16[16,512]{1,0:T(8,128)(2,1)S(1)} %maximum_bitcast_fusion), channel_id=1, source_target_pairs={{0,1},{1,2},{2,3},{3,0},{4,5},{5,6},{6,7},{7,4},{8,9},{9,10},{10,1... | collective-permute-start | bytes 49160 | tf_op jit(solution)/shard_map/ppermute | solution.py:51
  10.6 7.1 %collective-permute-start.1 = (bf16[16,512]{1,0:T(8,128)(2,1)S(1)}, bf16[16,512]{1,0:T(8,128)(2,1)S(1)}, u32[]{:S(2)}, u32[]{:S(2)}) collective-permute-start(bf16[16,512]{1,0:T(8,128)(2,1)S(1)} %maximum_bitcast_fusion), channel_id=1, source_target_pairs={{0,2},{1,3},{2,0},{3,1},{4,6},{5,7},{6,4},{7,5},{8,10},{9,11},{10,... | collective-permute-start | bytes 49160 | tf_op jit(solution)/shard_map/ppermute | solution.py:51
  13.7 5.6 %collective-permute-start.2 = (bf16[16,512]{1,0:T(8,128)(2,1)S(1)}, bf16[16,512]{1,0:T(8,128)(2,1)S(1)}, u32[]{:S(2)}, u32[]{:S(2)}) collective-permute-start(bf16[16,512]{1,0:T(8,128)(2,1)S(1)} %maximum_bitcast_fusion), channel_id=1, source_target_pairs={{0,3},{1,0},{2,1},{3,2},{4,7},{5,4},{6,5},{7,6},{8,11},{9,8},{10,9... | collective-permute-start | bytes 49160 | tf_op jit(solution)/shard_map/ppermute | solution.py:51
  20.8 57.9 %copy-start = (bf16[128,2048]{1,0:T(8,128)(2,1)S(1)}, bf16[128,2048]{1,0:T(8,128)(2,1)}, u32[]{:S(2)}) copy-start(bf16[128,2048]{1,0:T(8,128)(2,1)} %param.13) | copy-start | bytes 1572868
  76.8 31.9 %copy-start.1 = (bf16[64,16,768]{2,1,0:T(8,128)(2,1)}, bf16[64,16,768]{2,1,0:T(8,128)(2,1)S(1)}, u32[]{:S(2)}) copy-start(bf16[64,16,768]{2,1,0:T(8,128)(2,1)S(1)} %all_to_all.15.weight_own) | copy-start | bytes 4718596
  76.8 31.9 %collective-permute-start.7 = (bf16[64,16,768]{2,1,0:T(8,128)(2,1)S(1)}, bf16[64,16,768]{2,1,0:T(8,128)(2,1)}, u32[]{:S(2)}, u32[]{:S(2)}) collective-permute-start(bf16[64,16,768]{2,1,0:T(8,128)(2,1)S(1)} %all_to_all.15.weight_own), channel_id=1, source_target_pairs={{0,4},{4,0},{1,5},{5,1},{2,6},{6,2},{3,7},{7,3},{8,12},{12,8},{9,1... | collective-permute-start | bytes 4718600 | tf_op jit(solution)/shard_map/ppermute | solution.py:51
  79.1 29.6 %copy-start.2 = (bf16[128,2048]{1,0:T(8,128)(2,1)}, bf16[128,2048]{1,0:T(8,128)(2,1)S(1)}, u32[]{:S(2)}) copy-start(bf16[128,2048]{1,0:T(8,128)(2,1)S(1)} %fusion.1.own) | copy-start | bytes 1572868
  79.1 16.2 %collective-permute-start.3 = (bf16[128,2048]{1,0:T(8,128)(2,1)S(1)}, bf16[128,2048]{1,0:T(8,128)(2,1)S(1)}, u32[]{:S(2)}, u32[]{:S(2)}) collective-permute-start(bf16[128,2048]{1,0:T(8,128)(2,1)S(1)} %fusion.1.own), channel_id=1, source_target_pairs={{0,1},{1,2},{2,3},{3,0},{4,5},{5,6},{6,7},{7,4},{8,9},{9,10},{10,1... | collective-permute-start | bytes 1572872 | tf_op jit(solution)/shard_map/ppermute | solution.py:51
  81.7 17.1 %collective-permute-start.4 = (bf16[128,2048]{1,0:T(8,128)(2,1)S(1)}, bf16[128,2048]{1,0:T(8,128)(2,1)S(1)}, u32[]{:S(2)}, u32[]{:S(2)}) collective-permute-start(bf16[128,2048]{1,0:T(8,128)(2,1)S(1)} %fusion.1.own), channel_id=1, source_target_pairs={{0,3},{1,0},{2,1},{3,2},{4,7},{5,4},{6,5},{7,6},{8,11},{9,8},{10,9... | collective-permute-start | bytes 1572872 | tf_op jit(solution)/shard_map/ppermute | solution.py:51
  95.3 13.4 %copy-start.7 = (bf16[128,2048]{1,0:T(8,128)(2,1)}, bf16[128,2048]{1,0:T(8,128)(2,1)S(1)}, u32[]{:S(2)}) copy-start(bf16[128,2048]{1,0:T(8,128)(2,1)S(1)} %collective-permute-done.3.before) | copy-start | bytes 1572868
  95.4 10.7 %collective-permute-start.5 = (bf16[64,2048]{1,0:T(8,128)(2,1)S(1)}, bf16[64,2048]{1,0:T(8,128)(2,1)S(1)}, u32[]{:S(2)}, u32[]{:S(2)}) collective-permute-start(bf16[64,2048]{1,0:T(8,128)(2,1)S(1)} %slice.16), channel_id=1, source_target_pairs={{0,1},{1,2},{2,3},{3,0},{4,5},{5,6},{6,7},{7,4},{8,9},{9,10},{10,1... | collective-permute-start | bytes 786440 | tf_op jit(solution)/shard_map/ppermute | solution.py:51
  98.8 3.2 %copy-start.8 = (bf16[128,2048]{1,0:T(8,128)(2,1)}, bf16[128,2048]{1,0:T(8,128)(2,1)S(1)}, u32[]{:S(2)}) copy-start(bf16[128,2048]{1,0:T(8,128)(2,1)S(1)} %collective-permute-done.4.after) | copy-start | bytes 1572868
  98.8 9.9 %collective-permute-start.6 = (bf16[64,2048]{1,0:T(8,128)(2,1)S(1)}, bf16[64,2048]{1,0:T(8,128)(2,1)}, u32[]{:S(2)}, u32[]{:S(2)}) collective-permute-start(bf16[64,2048]{1,0:T(8,128)(2,1)S(1)} %slice.17), channel_id=1, source_target_pairs={{0,3},{1,0},{2,1},{3,2},{4,7},{5,4},{6,5},{7,6},{8,11},{9,8},{10,9... | collective-permute-start | bytes 786440 | tf_op jit(solution)/shard_map/ppermute | solution.py:51
  106.1 2.7 %copy-start.11 = (bf16[64,2048]{1,0:T(8,128)(2,1)}, bf16[64,2048]{1,0:T(8,128)(2,1)S(1)}, u32[]{:S(2)}) copy-start(bf16[64,2048]{1,0:T(8,128)(2,1)S(1)} %collective-permute-done.5.far_top) | copy-start | bytes 786436
  139.8 21.0 %all-to-all-start.2 = ((bf16[128,2,128]{2,1,0:T(2,128)(2,1)}), bf16[128,2,128]{2,1,0:T(2,128)(2,1)S(1)}, u32[]{:S(2)}, u32[]{:S(2)}) async-start(bf16[128,2,128]{2,1,0:T(2,128)(2,1)} %shard_map.129), calls=%async_computation.2 | async-start | bytes 131072 | tf_op jit(solution)/shard_map/all_to_all | solution.py:460
  146.2 10.9 %collective-permute-start.8 = (bf16[8,256]{1,0:T(8,128)(2,1)S(1)}, bf16[8,256]{1,0:T(8,128)(2,1)S(1)}, u32[]{:S(2)}, u32[]{:S(2)}) collective-permute-start(bf16[8,256]{1,0:T(8,128)(2,1)S(1)} %get-tuple-element.26), channel_id=1, source_target_pairs={{0,4},{4,8},{8,12},{12,16},{16,20},{20,24},{24,28},{28,32},{32,36}... | collective-permute-start | bytes 12296 | tf_op jit(solution)/shard_map/ppermute | solution.py:57
  148.2 8.9 %collective-permute-start.9 = (bf16[8,256]{1,0:T(8,128)(2,1)S(1)}, bf16[8,256]{1,0:T(8,128)(2,1)S(1)}, u32[]{:S(2)}, u32[]{:S(2)}) collective-permute-start(bf16[8,256]{1,0:T(8,128)(2,1)S(1)} %get-tuple-element.25), channel_id=1, source_target_pairs={{4,0},{8,4},{12,8},{16,12},{20,16},{24,20},{28,24},{32,28},{36,32}... | collective-permute-start | bytes 12296 | tf_op jit(solution)/shard_map/ppermute | solution.py:57
  164.1 16.8 %collective-permute-start.10 = (bf16[128,512]{1,0:T(8,128)(2,1)}, bf16[128,512]{1,0:T(8,128)(2,1)S(1)}, u32[]{:S(2)}, u32[]{:S(2)}) collective-permute-start(bf16[128,512]{1,0:T(8,128)(2,1)} %get-tuple-element.22), channel_id=1, source_target_pairs={{0,1},{1,2},{2,3},{3,0},{4,5},{5,6},{6,7},{7,4},{8,9},{9,10},{10,1... | collective-permute-start | bytes 393224 | tf_op jit(solution)/shard_map/ppermute | solution.py:51
  167.8 13.2 %collective-permute-start.11 = (bf16[128,512]{1,0:T(8,128)(2,1)}, bf16[128,512]{1,0:T(8,128)(2,1)S(1)}, u32[]{:S(2)}, u32[]{:S(2)}) collective-permute-start(bf16[128,512]{1,0:T(8,128)(2,1)} %get-tuple-element.23), channel_id=1, source_target_pairs={{0,2},{1,3},{2,0},{3,1},{4,6},{5,7},{6,4},{7,5},{8,10},{9,11},{10,... | collective-permute-start | bytes 393224 | tf_op jit(solution)/shard_map/ppermute | solution.py:51
  172.3 8.7 %collective-permute-start.12 = (bf16[128,512]{1,0:T(8,128)(2,1)}, bf16[128,512]{1,0:T(8,128)(2,1)S(1)}, u32[]{:S(2)}, u32[]{:S(2)}) collective-permute-start(bf16[128,512]{1,0:T(8,128)(2,1)} %get-tuple-element.24), channel_id=1, source_target_pairs={{0,3},{1,0},{2,1},{3,2},{4,7},{5,4},{6,5},{7,6},{8,11},{9,8},{10,9... | collective-permute-start | bytes 393224 | tf_op jit(solution)/shard_map/ppermute | solution.py:51
  181.0 0.6 copy-start.4
  181.0 0.7 copy-start.5
  181.7 0.7 copy-start.6
  (3 other events, 1.8 us)
Sparse Core Ops, SparseCore 0:
  20.1 113.6 all-gather.1
